TPU v7x, 256 devices: a whole 4x4x8 slice. The times are simulated.
256 devices in a mesh: kv: 32 (over z, y), tp: 8 (over x, core).
Axes of the slice: x: 4, y: 4, z: 8, core: 2. Of those that a mesh axis runs over, the one named last changes fastest.
Arguments:
- tokens: bfloat16 [512, 4096], P('tp', 'kv')
- seq_pos: int32 [512], P('kv'), may hold values from 0 to 4095
- state: float32 [512, 16, 128, 256], P('kv', 'tp'), may hold values from -0.6 to 0.6
- norm_in_gain: float32 [4096], P('kv'), may hold values from 0.1 to 1.9
- query_weight: bfloat16 [4096, 2048], P('kv', 'tp'), may hold values from -0.09375 to 0.09375
- key_weight: bfloat16 [4096, 2048], P('kv', 'tp'), may hold values from -0.09375 to 0.09375
- value_weight: bfloat16 [4096, 4096], P('kv', 'tp'), may hold values from -0.09375 to 0.09375
- gate_weight: bfloat16 [4096, 4096], P('kv', 'tp'), may hold values from -0.09375 to 0.09375
- head_gain: float32 [4096], P('tp'), may hold values from 0.1 to 1.9
- out_weight: bfloat16 [4096, 4096], P('tp', 'kv'), may hold values from -0.09375 to 0.09375
- norm_mlp_gain: float32 [4096], P('kv'), may hold values from 0.1 to 1.9
- hidden_weight: bfloat16 [4096, 16384], P('kv', 'tp'), may hold values from -0.09375 to 0.09375
- down_weight: bfloat16 [16384, 4096], P('tp', 'kv'), may hold values from -0.046875 to 0.046875
Outputs:
- output: bfloat16 [512, 4096], P('tp', 'kv')
- new_state: float32 [512, 16, 128, 256], P('kv', 'tp')
All inputs are finite; a program needn't handle non-finite values.
Results may differ from a plain program's by a relative error of at most 0.03.
Values may be sent and summed in bfloat16 or wider, within the bound.
No kernel may reach another device: no remote copies, remote signals or barrier semaphores. Data moves between devices by JAX's collectives and lax.ppermute only.
A program may use at most 64 MiB of HBM per device.

v0:
```python
import jax
import jax.numpy as jnp
from jax import lax
from jax.sharding import Mesh
from jax.sharding import PartitionSpec as P

D = 4096
H = 16
DK = 128
DV = 256
KV = ("kv_0", "kv_1")


EPS = 1e-06


def copy_for_each(array, axis):
    copies = jnp.broadcast_to(array, (lax.axis_size(axis), *array.shape))
    return lax.all_to_all(copies, axis, split_axis=0, concat_axis=0, tiled=True)


def in_order(blocks, dim):
    blocks = jnp.moveaxis(blocks, 0, dim)
    shape = blocks.shape
    return blocks.reshape(*shape[:dim], shape[dim] * shape[dim + 1], *shape[dim + 2 :])


def gather_directly(array, axis, dim):
    blocks = copy_for_each(array, axis)
    return in_order(blocks, dim)


def side_by_side(arrays, axis, dim, along):
    columns = [a.reshape(*a.shape[:along], -1) for a in arrays]
    both = jnp.concatenate(columns, axis=along)
    filled, at, done = (lax.psum_scatter(both, axis, scatter_dimension=dim, tiled=True), 0, [])
    for a, column in zip(arrays, columns):
        piece = filled[..., at : at + column.shape[along]]
        done.append(piece.reshape(*piece.shape[:along], *a.shape[along:]))
        at += column.shape[along]
    return tuple(done)


def in_blocks(array, dim, devices):
    before, after = (array.shape[:dim], array.shape[dim + 1 :])
    return jnp.moveaxis(array.reshape(*before, devices, -1, *after), dim, 0)


def summed_on_arrival(array, axis, dim):
    devices = lax.axis_size(axis)
    blocks = lax.all_to_all(in_blocks(array, dim, devices), axis, 0, 0, tiled=True)
    return jnp.sum(blocks.astype(jnp.float32), axis=0)


def taken_together(array, axis):
    return copy_for_each(array, axis).sum(axis=0)


def gathered_by_axis(array, axes, dim):
    for axis in reversed(axes):
        array = lax.all_gather(array, axis, axis=dim, tiled=True)
    return array


def rotate(vectors, positions):
    half = vectors.shape[-1] // 2
    inverse = jnp.power(10000.0, -jnp.arange(half, dtype=jnp.float32) / half)
    angles = positions.astype(jnp.float32)[:, None] * inverse[None, :]
    cosine = jnp.cos(angles)[:, None, :]
    sine = jnp.sin(angles)[:, None, :]
    first, second = (vectors[..., :half], vectors[..., half:])
    return jnp.concatenate(
        [first * cosine - second * sine, first * sine + second * cosine], axis=-1
    )


def head_decay(head_ids):
    return 1.0 - jnp.exp2(-2.0 - 6.0 * head_ids / (H - 1))


def local(
    tokens,
    seq_pos,
    state,
    norm_in_gain,
    query_weight,
    key_weight,
    value_weight,
    gate_weight,
    head_gain,
    out_weight,
    norm_mlp_gain,
    hidden_weight,
    down_weight,
):
    rows_all = gather_directly(tokens, "tp", 0)
    rows_f = rows_all.astype(jnp.float32)
    squares_in = jnp.sum(rows_f * rows_f, axis=1)
    normed_in = (rows_f * norm_in_gain[None, :]).astype(jnp.bfloat16)
    term_query = jnp.dot(normed_in, query_weight, preferred_element_type=jnp.float32).astype(
        jnp.bfloat16
    )
    term_keys = jnp.dot(normed_in, key_weight, preferred_element_type=jnp.float32).astype(
        jnp.bfloat16
    )
    term_values = jnp.dot(normed_in, value_weight, preferred_element_type=jnp.float32).astype(
        jnp.bfloat16
    )
    term_gates = jnp.dot(normed_in, gate_weight, preferred_element_type=jnp.float32).astype(
        jnp.bfloat16
    )
    query, keys, values, gates, total_in = tuple(
        (
            part.astype(jnp.float32)
            for part in side_by_side(
                (
                    term_query.astype(jnp.float32).astype(jnp.bfloat16),
                    term_keys.astype(jnp.float32).astype(jnp.bfloat16),
                    term_values.astype(jnp.float32).astype(jnp.bfloat16),
                    term_gates.astype(jnp.float32).astype(jnp.bfloat16),
                    squares_in.astype(jnp.bfloat16),
                ),
                KV,
                0,
                1,
            )
        )
    )
    factor = lax.rsqrt(total_in / D + EPS)[:, None]
    query, keys, values, gates = (query * factor, keys * factor, values * factor, gates * factor)
    local_rows = query.shape[0]
    heads_dev = H // lax.axis_size("tp")
    turned_query = rotate(query.reshape(local_rows, heads_dev, DK), seq_pos)
    turned_keys = rotate(keys.reshape(local_rows, heads_dev, DK), seq_pos) * DK ** (-0.5)
    head_ids = (lax.axis_index("tp") * heads_dev + jnp.arange(heads_dev, dtype=jnp.int32)).astype(
        jnp.float32
    )
    decay = head_decay(head_ids)
    new_state = decay[None, :, None, None] * state + jnp.einsum(
        "bhk,bhv->bhkv",
        turned_keys,
        values.reshape(local_rows, heads_dev, DV),
        precision=lax.Precision.HIGHEST,
    )
    read = jnp.einsum("bhk,bhkv->bhv", turned_query, new_state, precision=lax.Precision.HIGHEST)
    read = read * lax.rsqrt(jnp.mean(read * read, axis=-1, keepdims=True) + EPS)
    mixed = (
        read.reshape(local_rows, heads_dev * DV) * head_gain[None, :] * jax.nn.silu(gates)
    ).astype(jnp.bfloat16)
    attn_terms = jnp.dot(
        gather_directly(mixed, KV, 0), out_weight, preferred_element_type=jnp.float32
    )
    attn = summed_on_arrival(attn_terms.astype(jnp.bfloat16), "tp", 0)
    resid = (tokens.astype(jnp.float32) + attn).astype(jnp.bfloat16)
    resid_all = gather_directly(resid, "tp", 0)
    resid_f = resid_all.astype(jnp.float32)
    squares_mid = jnp.sum(resid_f * resid_f, axis=1)
    normed_mid = (resid_f * norm_mlp_gain[None, :]).astype(jnp.bfloat16)
    term_hidden = jnp.dot(normed_mid, hidden_weight, preferred_element_type=jnp.float32).astype(
        jnp.bfloat16
    )
    total_mid = taken_together(squares_mid, KV)
    scale_mid = lax.rsqrt(total_mid / D + EPS)[:, None]
    hidden = summed_on_arrival(term_hidden, KV, 0)
    row_start = lax.axis_index(KV) * hidden.shape[0]
    local_scale = lax.dynamic_slice_in_dim(scale_mid, row_start, hidden.shape[0], 0)
    active = jnp.square(jax.nn.relu(hidden * local_scale)).astype(jnp.bfloat16)
    down_terms = jnp.dot(
        gathered_by_axis(active, KV, 0), down_weight, preferred_element_type=jnp.float32
    )
    down = summed_on_arrival(down_terms.astype(jnp.bfloat16), "tp", 0)
    output = (resid.astype(jnp.float32) + down).astype(jnp.bfloat16)
    return (output, new_state)


def solution(mesh):
    torus = Mesh(mesh.devices.reshape(8, 4, mesh.shape["tp"]), ("kv_0", "kv_1", "tp"))
    return jax.shard_map(
        local,
        mesh=torus,
        in_specs=(
            P("tp", KV),
            P(KV),
            P(KV, "tp", None, None),
            P(KV),
            P(KV, "tp"),
            P(KV, "tp"),
            P(KV, "tp"),
            P(KV, "tp"),
            P("tp"),
            P("tp", KV),
            P(KV),
            P(KV, "tp"),
            P("tp", KV),
        ),
        out_specs=(P("tp", KV), P(KV, "tp", None, None)),
        check_vma=False,
    )
```

profile of v0, /device:TPU:1, one launch (start us, length us, event | category | flops | bytes accessed | tf_op | source)
XLA Modules:
  0.0 414.1 jit_solution(8469200528582230642)
XLA Ops:
  7.2 0.8 broadcast_in_dim.10
  8.0 10.8 %all_to_all.36 = bf16[8,64,128]{2,1,0:T(8,128)(2,1)S(1)} all-to-all(bf16[8,64,128]{2,1,0:T(8,128)(2,1)S(1)} %broadcast_in_dim.10), channel_id=1, replica_groups=mesh['kv_0'=8,'kv_1'=4,'tp'=8] {'tp'}, dimensions={0} | all-to-all | bytes 262144 | tf_op jit(solution)/shard_map/all_to_all | solution.py:19
  18.9 0.1 multiply_reduce_fusion.1
  19.1 0.7 fusion.5
  19.8 1.1 fusion.3
  20.9 1.1 fusion.2
  22.0 1.2 fusion.1
  23.3 0.3 fusion
  23.7 2.3 copy.50
  26.2 197.0 %reduce-scatter.4.cloned.1.call-done = bf16[16,1537]{1,0:T(8,128)(2,1)} async-done(((bf16[512,1537]{1,0:T(8,128)(2,1)}), bf16[16,1537]{1,0:T(8,128)(2,1)}) %reduce-scatter.4.cloned.1.call-update) | async-done | bytes 49200 | tf_op jit(solution)/shard_map/reduce_scatter | solution.py:36
  223.2 0.7 add_rsqrt_fusion
  224.0 0.8 convert_multiply_fusion.2
  224.8 0.7 fusion.11
  226.3 2.6 multiply_add_fusion
  229.0 2.1 fusion.7
  231.3 0.8 multiply_convert_fusion.1
  232.2 19.0 %all_to_all.37 = bf16[32,16,512]{2,1,0:T(8,128)(2,1)S(1)} all-to-all(bf16[32,16,512]{2,1,0:T(8,128)(2,1)S(1)} %broadcast_in_dim.11), channel_id=1, replica_groups=mesh['kv_0'=8,'kv_1'=4,'tp'=8] {'kv_0','kv_1'}, dimensions={0} | all-to-all | bytes 1048576 | tf_op jit(solution)/shard_map/all_to_all | solution.py:19
  251.1 0.3 convolution_convert_fusion.6
  251.4 16.6 %all_to_all.38 = bf16[8,64,128]{2,1,0:T(8,128)(2,1)S(1)} all-to-all(bf16[8,64,128]{2,1,0:T(8,128)(2,1)S(1)} %bitcast.43), channel_id=1, replica_groups=mesh['kv_0'=8,'kv_1'=4,'tp'=8] {'tp'}, dimensions={0} | all-to-all | bytes 262144 | tf_op jit(solution)/shard_map/all_to_all | solution.py:51
  268.1 8.5 %all_to_all.39 = bf16[8,64,128]{2,1,0:T(8,128)(2,1)S(1)} all-to-all(bf16[8,64,128]{2,1,0:T(8,128)(2,1)S(1)} %broadcast_in_dim.12), channel_id=1, replica_groups=mesh['kv_0'=8,'kv_1'=4,'tp'=8] {'tp'}, dimensions={0} | all-to-all | bytes 262144 | tf_op jit(solution)/shard_map/all_to_all | solution.py:19
  276.8 0.7 broadcast_in_dim.14
  277.5 4.1 all-to-all-start.5
  281.6 2.0 convolution_convert_fusion
  283.7 6.7 %all-to-all-done.5 = f32[32,1,512]{2,1,0:T(1,128)S(1)} async-done(((f32[32,1,512]{2,1,0:T(1,128)}), f32[32,1,512]{2,1,0:T(1,128)S(1)}, u32[]{:S(2)}, u32[]{:S(2)}) %all-to-all-start.5) | async-done | bytes 65568 | tf_op jit(solution)/shard_map/all_to_all | solution.py:19
  290.4 4.0 all-to-all-start.4
  294.6 46.5 %all-to-all-done.4 = bf16[32,16,2048]{2,1,0:T(8,128)(2,1)S(1)} async-done(((bf16[32,16,2048]{2,1,0:T(8,128)(2,1)}), bf16[32,16,2048]{2,1,0:T(8,128)(2,1)S(1)}, u32[]{:S(2)}, u32[]{:S(2)}) %all-to-all-start.4) | async-done | bytes 2097184 | tf_op jit(solution)/shard_map/all_to_all | solution.py:51
  341.1 0.3 convert_reduce_fusion
  341.6 12.6 %all_gather.6 = bf16[64,2048]{1,0:T(8,128)(2,1)} all-gather(bf16[16,2048]{1,0:T(8,128)(2,1)S(1)} %multiply_convert_fusion), channel_id=1, replica_groups=mesh['kv_0'=8,'kv_1'=4,'tp'=8] {'kv_1'}, dimensions={0}, use_global_device_ids=true | all-gather | bytes 327680 | tf_op jit(solution)/shard_map/all_gather | solution.py:61
  354.2 36.0 %all-gather.2.cloned.1.call-done = bf16[512,2048]{1,0:T(8,128)(2,1)} async-done(((bf16[64,2048]{1,0:T(8,128)(2,1)}), bf16[512,2048]{1,0:T(8,128)(2,1)}) %all-gather.2.cloned.1.call-update) | async-done | bytes 2097168 | tf_op jit(solution)/shard_map/all_gather | solution.py:61
  390.2 2.3 convolution_convert_fusion.5
  392.5 14.2 %all_to_all.40 = bf16[8,64,128]{2,1,0:T(8,128)(2,1)S(1)} all-to-all(bf16[8,64,128]{2,1,0:T(8,128)(2,1)S(1)} %bitcast.44), channel_id=1, replica_groups=mesh['kv_0'=8,'kv_1'=4,'tp'=8] {'tp'}, dimensions={0} | all-to-all | bytes 262144 | tf_op jit(solution)/shard_map/all_to_all | solution.py:51
  406.7 0.6 add_convert_fusion
  (59 shorter events, 2.1 us)
Async XLA Ops:
  7.2 274.4 %copy-start = (bf16[128,2048]{1,0:T(8,128)(2,1)S(1)}, bf16[128,2048]{1,0:T(8,128)(2,1)}, u32[]{:S(2)}) copy-start(bf16[128,2048]{1,0:T(8,128)(2,1)} %param.24) | copy-start | bytes 1572868
  7.2 16.1 %copy-start.3 = (bf16[128,512]{1,0:T(8,128)(2,1)S(1)}, bf16[128,512]{1,0:T(8,128)(2,1)}, u32[]{:S(2)}) copy-start(bf16[128,512]{1,0:T(8,128)(2,1)} %param.20) | copy-start | bytes 393220
  7.2 216.1 %reduce-scatter.4.cloned.1.call-start = ((), (), s32[]{:S(2)}) async-start(), calls=%async_computation.9 | async-start | bytes 1757184 | tf_op jit(solution)/shard_map/reduce_scatter | solution.py:36
  23.6 2.4 copy-start.8
  228.9 2.1 copy-start.1
  228.9 2.4 copy-start.6
  228.9 22.2 %copy-start.4 = (bf16[512,128]{1,0:T(8,128)(2,1)S(1)}, bf16[512,128]{1,0:T(8,128)(2,1)}, u32[]{:S(2)}) copy-start(bf16[512,128]{1,0:T(8,128)(2,1)} %param.22) | copy-start | bytes 393220
  231.1 37.0 %copy-start.5 = (bf16[64,128]{1,0:T(8,128)(2,1)S(1)}, bf16[64,128]{1,0:T(8,128)(2,1)}, u32[]{:S(2)}) copy-start(bf16[64,128]{1,0:T(8,128)(2,1)} %param.13) | copy-start | bytes 49156
  231.1 50.5 %copy-start.7 = (f32[128]{0:T(128)S(1)}, f32[128]{0:T(128)}, u32[]{:S(2)}) copy-start(f32[128]{0:T(128)} %param.23) | copy-start | bytes 1540
  277.5 12.9 %all-to-all-start.5 = ((f32[32,1,512]{2,1,0:T(1,128)}), f32[32,1,512]{2,1,0:T(1,128)S(1)}, u32[]{:S(2)}, u32[]{:S(2)}) async-start(f32[32,1,512]{2,1,0:T(1,128)} %broadcast_in_dim.14), calls=%async_computation.5 | async-start | bytes 131072 | tf_op jit(solution)/shard_map/all_to_all | solution.py:19
  290.4 50.8 %all-to-all-start.4 = ((bf16[32,16,2048]{2,1,0:T(8,128)(2,1)}), bf16[32,16,2048]{2,1,0:T(8,128)(2,1)S(1)}, u32[]{:S(2)}, u32[]{:S(2)}) async-start(bf16[32,16,2048]{2,1,0:T(8,128)(2,1)} %bitcast.9), calls=%async_computation.4 | async-start | bytes 4194304 | tf_op jit(solution)/shard_map/all_to_all | solution.py:51
  294.4 95.8 %copy-start.2 = (bf16[2048,128]{1,0:T(8,128)(2,1)S(1)}, bf16[2048,128]{1,0:T(8,128)(2,1)}, u32[]{:S(2)}) copy-start(bf16[2048,128]{1,0:T(8,128)(2,1)} %param.25) | copy-start | bytes 1572868
  294.4 95.8 %all-gather.2.cloned.1.call-start = ((), (), s32[]{:S(2)}) async-start(), calls=%async_computation.8 | async-start | bytes 2359296 | tf_op jit(solution)/shard_map/all_gather | solution.py:61
Sparse Core Ops, SparseCore 0:
  26.1 197.0 reduce-scatter.3
  354.3 35.8 all-gather.1
where the time goes:
time: 415 us; the launch traced here: 414 us
  waiting for transfers between devices  286 us (69%)
  blocking collectives  81.6 us (20%)
  between operations  14.4 us (3%)
  matrix products  10.5 us (3%)
  starting transfers between devices  8.17 us (2%)
  other arithmetic  7.54 us (2%)
  local copies, waits for them, and re-layouts  5.57 us (1%)
    reduce_scatter x1, waiting for transfers between devices, side_by_side(): lax.psum_scatter(both, axis, scatter_dimension=dim, tiled=True)  197 us
    all_to_all x1, waiting for transfers between devices, summed_on_arrival(): lax.all_to_all(in_blocks(array, dim, devices), axis, 0, 0, tiled=True)  46.5 us
    all_to_all x3, blocking collectives, copy_for_each(): return lax.all_to_all(copies, axis, split_axis=0, concat_axis=0, tiled=True)  38.3 us
    all_gather x1, waiting for transfers between devices, gathered_by_axis(): array = lax.all_gather(array, axis, axis=dim, tiled=True)  36 us
    all_to_all x2, blocking collectives, summed_on_arrival(): lax.all_to_all(in_blocks(array, dim, devices), axis, 0, 0, tiled=True)  30.8 us
    all_gather x1, blocking collectives, gathered_by_axis(): array = lax.all_gather(array, axis, axis=dim, tiled=True)  12.6 us
  transfers between devices with their start and end apart: 4, of which 4 were waited for; matrix products, arithmetic and copies ran while one was open for 1% of the time, Pallas kernels for 0%

commit v1 on v0

--- a/solution.py
+++ b/solution.py
@@ -30,17 +30,6 @@
     return in_order(blocks, dim)
 
 
-def side_by_side(arrays, axis, dim, along):
-    columns = [a.reshape(*a.shape[:along], -1) for a in arrays]
-    both = jnp.concatenate(columns, axis=along)
-    filled, at, done = (lax.psum_scatter(both, axis, scatter_dimension=dim, tiled=True), 0, [])
-    for a, column in zip(arrays, columns):
-        piece = filled[..., at : at + column.shape[along]]
-        done.append(piece.reshape(*piece.shape[:along], *a.shape[along:]))
-        at += column.shape[along]
-    return tuple(done)
-
-
 def in_blocks(array, dim, devices):
     before, after = (array.shape[:dim], array.shape[dim + 1 :])
     return jnp.moveaxis(array.reshape(*before, devices, -1, *after), dim, 0)
@@ -54,12 +43,6 @@
 
 def taken_together(array, axis):
     return copy_for_each(array, axis).sum(axis=0)
-
-
-def gathered_by_axis(array, axes, dim):
-    for axis in reversed(axes):
-        array = lax.all_gather(array, axis, axis=dim, tiled=True)
-    return array
 
 
 def rotate(vectors, positions):
@@ -109,23 +92,15 @@
     term_gates = jnp.dot(normed_in, gate_weight, preferred_element_type=jnp.float32).astype(
         jnp.bfloat16
     )
-    query, keys, values, gates, total_in = tuple(
-        (
-            part.astype(jnp.float32)
-            for part in side_by_side(
-                (
-                    term_query.astype(jnp.float32).astype(jnp.bfloat16),
-                    term_keys.astype(jnp.float32).astype(jnp.bfloat16),
-                    term_values.astype(jnp.float32).astype(jnp.bfloat16),
-                    term_gates.astype(jnp.float32).astype(jnp.bfloat16),
-                    squares_in.astype(jnp.bfloat16),
-                ),
-                KV,
-                0,
-                1,
-            )
-        )
+    terms = jnp.concatenate(
+        [term_query, term_keys, term_values, term_gates, squares_in.astype(jnp.bfloat16)[:, None]],
+        axis=1,
     )
+    sums = summed_on_arrival(terms, KV, 0)
+    wq, wv = (query_weight.shape[1], value_weight.shape[1])
+    query, keys = (sums[:, :wq], sums[:, wq : 2 * wq])
+    values, gates = (sums[:, 2 * wq : 2 * wq + wv], sums[:, 2 * wq + wv : 2 * wq + 2 * wv])
+    total_in = sums[:, -1]
     factor = lax.rsqrt(total_in / D + EPS)[:, None]
     query, keys, values, gates = (query * factor, keys * factor, values * factor, gates * factor)
     local_rows = query.shape[0]
@@ -166,7 +141,7 @@
     local_scale = lax.dynamic_slice_in_dim(scale_mid, row_start, hidden.shape[0], 0)
     active = jnp.square(jax.nn.relu(hidden * local_scale)).astype(jnp.bfloat16)
     down_terms = jnp.dot(
-        gathered_by_axis(active, KV, 0), down_weight, preferred_element_type=jnp.float32
+        gather_directly(active, KV, 0), down_weight, preferred_element_type=jnp.float32
     )
     down = summed_on_arrival(down_terms.astype(jnp.bfloat16), "tp", 0)
     output = (resid.astype(jnp.float32) + down).astype(jnp.bfloat16)

time: 415 us -> 253 us (0.61)
  waiting for transfers between devices: 286 us -> 93.5 us
  blocking collectives: 81.6 us -> 118 us
  between operations: 14.4 us -> 0.99 us
  starting transfers between devices: 8.17 us -> 19.5 us
    reduce_scatter x1 -> x0, waiting for transfers between devices: 197 us -> none  [side_by_side(): lax.psum_scatter(both, axis, scatter_dimension=dim, tiled=True)]
    all_to_all x3 -> x4, blocking collectives: 38.3 us -> 94.7 us  [copy_for_each(): return lax.all_to_all(copies, axis, split_axis=0, concat_axis=0, tiled=True)]
    all_to_all x1 -> x2, waiting for transfers between devices: 46.5 us -> 86.8 us  [summed_on_arrival(): lax.all_to_all(in_blocks(array, dim, devices), axis, 0, 0, tiled=True)]
    all_gather x1 -> x0, waiting for transfers between devices: 36 us -> none  [gathered_by_axis(): array = lax.all_gather(array, axis, axis=dim, tiled=True)]
    all_gather x1 -> x0, blocking collectives: 12.6 us -> none  [gathered_by_axis(): array = lax.all_gather(array, axis, axis=dim, tiled=True)]
    all_to_all x1 -> x2, starting transfers between devices: 4.01 us -> 15.2 us  [summed_on_arrival(): lax.all_to_all(in_blocks(array, dim, devices), axis, 0, 0, tiled=True)]
    all_to_all x2, blocking collectives: 30.8 us -> 23.3 us  [summed_on_arrival(): lax.all_to_all(in_blocks(array, dim, devices), axis, 0, 0, tiled=True)]
  transfers between devices with their start and end apart: 4 -> 3, of which waited for: 4 -> 3; matrix products, arithmetic and copies ran while one was open for 1% -> 1% of each run, Pallas kernels for 0% -> 0%
where the time goes in v1:
time: 253 us
  blocking collectives  118 us (47%)
  waiting for transfers between devices  93.5 us (37%)
  starting transfers between devices  19.5 us (8%)
  matrix products  8.7 us (3%)
  local copies, waits for them, and re-layouts  6.18 us (2%)
  other arithmetic  5.86 us (2%)
    all_to_all x4, blocking collectives, copy_for_each(): return lax.all_to_all(copies, axis, split_axis=0, concat_axis=0, tiled=True)  94.7 us
    all_to_all x2, waiting for transfers between devices, summed_on_arrival(): lax.all_to_all(in_blocks(array, dim, devices), axis, 0, 0, tiled=True)  86.8 us
    all_to_all x2, blocking collectives, summed_on_arrival(): lax.all_to_all(in_blocks(array, dim, devices), axis, 0, 0, tiled=True)  23.3 us
    all_to_all x2, starting transfers between devices, summed_on_arrival(): lax.all_to_all(in_blocks(array, dim, devices), axis, 0, 0, tiled=True)  15.2 us
    all_to_all x1, waiting for transfers between devices, copy_for_each(): return lax.all_to_all(copies, axis, split_axis=0, concat_axis=0, tiled=True)  6.73 us
  transfers between devices with their start and end apart: 3, of which 3 were waited for; matrix products, arithmetic and copies ran while one was open for 1% of the time, Pallas kernels for 0%

profile of v1, /device:TPU:1, one launch (start us, length us, event | category | flops | bytes accessed | tf_op | source)
XLA Modules:
  0.0 252.8 jit_solution(1233224119575501240)
XLA Ops:
  0.7 0.8 broadcast_in_dim.12
  1.5 10.8 %all_to_all.46 = bf16[8,64,128]{2,1,0:T(8,128)(2,1)S(1)} all-to-all(bf16[8,64,128]{2,1,0:T(8,128)(2,1)S(1)} %broadcast_in_dim.12), channel_id=1, replica_groups=mesh['kv_0'=8,'kv_1'=4,'tp'=8] {'tp'}, dimensions={0} | all-to-all | bytes 262144 | tf_op jit(solution)/shard_map/all_to_all | solution.py:19
  12.7 0.7 fusion.1
  13.4 1.0 convolution_convert_fusion.3
  14.5 1.0 convolution_convert_fusion.4
  15.5 1.2 convolution_convert_fusion.1
  16.7 0.3 convolution_convert_fusion.2
  17.0 0.7 constant_dynamic-update-slice_fusion.4
  17.7 0.7 constant_dynamic-update-slice_fusion.3
  18.4 0.8 constant_dynamic-update-slice_fusion.2
  19.3 0.8 constant_dynamic-update-slice_fusion.1
  20.1 0.7 constant_dynamic-update-slice_fusion
  20.8 11.2 %all-to-all-start.1 = ((bf16[32,16,1537]{2,1,0:T(8,128)(2,1)}), bf16[32,16,1537]{2,1,0:T(8,128)(2,1)S(1)}, u32[]{:S(2)}, u32[]{:S(2)}) async-start(bf16[32,16,1537]{2,1,0:T(8,128)(2,1)} %constant_dynamic-update-slice_fusion), calls=%async_computation.1 | async-start | bytes 3407872 | tf_op jit(solution)/shard_map/all_to_all | solution.py:40
  32.1 40.2 %all-to-all-done.1 = bf16[32,16,1537]{2,1,0:T(8,128)(2,1)S(1)} async-done(((bf16[32,16,1537]{2,1,0:T(8,128)(2,1)}), bf16[32,16,1537]{2,1,0:T(8,128)(2,1)S(1)}, u32[]{:S(2)}, u32[]{:S(2)}) %all-to-all-start.1) | async-done | bytes 1573920 | tf_op jit(solution)/shard_map/all_to_all | solution.py:40
  72.4 0.3 convert_reduce_fusion.1
  73.3 2.6 %multiply_add_fusion = f32[16,2,128,256]{3,2,1,0:T(8,128)S(1)} fusion(f32[16,2,128,256]{3,2,1,0:T(8,128)} %param.15, f32[16,2,256]{2,1,0:T(2,128)S(1)} %reshape.141, f32[16,2,128]{2,1,0:T(2,128)S(1)} %copy.51, f32[2]{0:T(128)S(1)} %exponential_subtract_fusion), kind=kLoop, calls=%fused_computation.1 | loop fusion | flops 3145728 | bytes 8437768 | tf_op jit(solution)/shard_map/add | solution.py:114
  75.9 2.1 fusion.3
  78.4 20.7 %all_to_all.47 = bf16[32,16,512]{2,1,0:T(8,128)(2,1)S(1)} all-to-all(bf16[32,16,512]{2,1,0:T(8,128)(2,1)S(1)} %broadcast_in_dim.13), channel_id=1, replica_groups=mesh['kv_0'=8,'kv_1'=4,'tp'=8] {'kv_0','kv_1'}, dimensions={0} | all-to-all | bytes 1048576 | tf_op jit(solution)/shard_map/all_to_all | solution.py:19
  99.2 0.3 convolution_convert_fusion.6
  99.5 11.6 %all_to_all.48 = bf16[8,64,128]{2,1,0:T(8,128)(2,1)S(1)} all-to-all(bf16[8,64,128]{2,1,0:T(8,128)(2,1)S(1)} %bitcast.47), channel_id=1, replica_groups=mesh['kv_0'=8,'kv_1'=4,'tp'=8] {'tp'}, dimensions={0} | all-to-all | bytes 262144 | tf_op jit(solution)/shard_map/all_to_all | solution.py:40
  111.1 8.5 %all_to_all.49 = bf16[8,64,128]{2,1,0:T(8,128)(2,1)S(1)} all-to-all(bf16[8,64,128]{2,1,0:T(8,128)(2,1)S(1)} %broadcast_in_dim.14), channel_id=1, replica_groups=mesh['kv_0'=8,'kv_1'=4,'tp'=8] {'tp'}, dimensions={0} | all-to-all | bytes 262144 | tf_op jit(solution)/shard_map/all_to_all | solution.py:19
  119.8 0.7 broadcast_in_dim.16
  120.5 4.3 %all-to-all-start.6 = ((f32[32,1,512]{2,1,0:T(1,128)}), f32[32,1,512]{2,1,0:T(1,128)S(1)}, u32[]{:S(2)}, u32[]{:S(2)}) async-start(f32[32,1,512]{2,1,0:T(1,128)} %broadcast_in_dim.16), calls=%async_computation.6 | async-start | bytes 131072 | tf_op jit(solution)/shard_map/all_to_all | solution.py:19
  124.8 2.0 convolution_convert_fusion
  126.8 6.7 %all-to-all-done.6 = f32[32,1,512]{2,1,0:T(1,128)S(1)} async-done(((f32[32,1,512]{2,1,0:T(1,128)}), f32[32,1,512]{2,1,0:T(1,128)S(1)}, u32[]{:S(2)}, u32[]{:S(2)}) %all-to-all-start.6) | async-done | bytes 65568 | tf_op jit(solution)/shard_map/all_to_all | solution.py:19
  133.6 4.0 %all-to-all-start.5 = ((bf16[32,16,2048]{2,1,0:T(8,128)(2,1)}), bf16[32,16,2048]{2,1,0:T(8,128)(2,1)S(1)}, u32[]{:S(2)}, u32[]{:S(2)}) async-start(bf16[32,16,2048]{2,1,0:T(8,128)(2,1)} %bitcast.10), calls=%async_computation.5 | async-start | bytes 4194304 | tf_op jit(solution)/shard_map/all_to_all | solution.py:40
  137.7 46.6 %all-to-all-done.5 = bf16[32,16,2048]{2,1,0:T(8,128)(2,1)S(1)} async-done(((bf16[32,16,2048]{2,1,0:T(8,128)(2,1)}), bf16[32,16,2048]{2,1,0:T(8,128)(2,1)S(1)}, u32[]{:S(2)}, u32[]{:S(2)}) %all-to-all-start.5) | async-done | bytes 2097184 | tf_op jit(solution)/shard_map/all_to_all | solution.py:40
  184.3 0.3 convert_reduce_fusion
  185.0 54.7 %all_to_all.50 = bf16[32,16,2048]{2,1,0:T(8,128)(2,1)S(1)} all-to-all(bf16[32,16,2048]{2,1,0:T(8,128)(2,1)S(1)} %broadcast_in_dim.17), channel_id=1, replica_groups=mesh['kv_0'=8,'kv_1'=4,'tp'=8] {'kv_0','kv_1'}, dimensions={0} | all-to-all | bytes 4194304 | tf_op jit(solution)/shard_map/all_to_all | solution.py:19
  239.7 0.7 convolution_convert_fusion.5
  240.4 11.7 %all_to_all.51 = bf16[8,64,128]{2,1,0:T(8,128)(2,1)S(1)} all-to-all(bf16[8,64,128]{2,1,0:T(8,128)(2,1)S(1)} %bitcast.48), channel_id=1, replica_groups=mesh['kv_0'=8,'kv_1'=4,'tp'=8] {'tp'}, dimensions={0} | all-to-all | bytes 262144 | tf_op jit(solution)/shard_map/all_to_all | solution.py:40
  252.1 0.6 add_convert_fusion
  (53 shorter events, 2.3 us)
Async XLA Ops:
  0.6 124.1 %copy-start = (bf16[128,2048]{1,0:T(8,128)(2,1)S(1)}, bf16[128,2048]{1,0:T(8,128)(2,1)}, u32[]{:S(2)}) copy-start(bf16[128,2048]{1,0:T(8,128)(2,1)} %param.24) | copy-start | bytes 1572868
  0.6 16.1 %copy-start.3 = (bf16[128,512]{1,0:T(8,128)(2,1)S(1)}, bf16[128,512]{1,0:T(8,128)(2,1)}, u32[]{:S(2)}) copy-start(bf16[128,512]{1,0:T(8,128)(2,1)} %param.19) | copy-start | bytes 393220
  20.1 11.9 %copy-start.8 = (s32[16]{0:T(128)S(1)}, s32[16]{0:T(128)}, u32[]{:S(2)}) copy-start(s32[16]{0:T(128)} %param.14) | copy-start | bytes 196
  20.8 51.6 %all-to-all-start.1 = ((bf16[32,16,1537]{2,1,0:T(8,128)(2,1)}), bf16[32,16,1537]{2,1,0:T(8,128)(2,1)S(1)}, u32[]{:S(2)}, u32[]{:S(2)}) async-start(bf16[32,16,1537]{2,1,0:T(8,128)(2,1)} %constant_dynamic-update-slice_fusion), calls=%async_computation.1 | async-start | bytes 3407872 | tf_op jit(solution)/shard_map/all_to_all | solution.py:40
  75.9 2.1 copy-start.1
  75.9 2.4 copy-start.6
  75.9 23.2 %copy-start.4 = (bf16[512,128]{1,0:T(8,128)(2,1)S(1)}, bf16[512,128]{1,0:T(8,128)(2,1)}, u32[]{:S(2)}) copy-start(bf16[512,128]{1,0:T(8,128)(2,1)} %param.22) | copy-start | bytes 393220
  78.0 33.0 %copy-start.5 = (bf16[64,128]{1,0:T(8,128)(2,1)S(1)}, bf16[64,128]{1,0:T(8,128)(2,1)}, u32[]{:S(2)}) copy-start(bf16[64,128]{1,0:T(8,128)(2,1)} %param.13) | copy-start | bytes 49156
  78.0 46.7 %copy-start.7 = (f32[128]{0:T(128)S(1)}, f32[128]{0:T(128)}, u32[]{:S(2)}) copy-start(f32[128]{0:T(128)} %param.23) | copy-start | bytes 1540
  120.5 13.1 %all-to-all-start.6 = ((f32[32,1,512]{2,1,0:T(1,128)}), f32[32,1,512]{2,1,0:T(1,128)S(1)}, u32[]{:S(2)}, u32[]{:S(2)}) async-start(f32[32,1,512]{2,1,0:T(1,128)} %broadcast_in_dim.16), calls=%async_computation.6 | async-start | bytes 131072 | tf_op jit(solution)/shard_map/all_to_all | solution.py:19
  133.6 50.8 %all-to-all-start.5 = ((bf16[32,16,2048]{2,1,0:T(8,128)(2,1)}), bf16[32,16,2048]{2,1,0:T(8,128)(2,1)S(1)}, u32[]{:S(2)}, u32[]{:S(2)}) async-start(bf16[32,16,2048]{2,1,0:T(8,128)(2,1)} %bitcast.10), calls=%async_computation.5 | async-start | bytes 4194304 | tf_op jit(solution)/shard_map/all_to_all | solution.py:40
  185.0 54.7 %copy-start.2 = (bf16[2048,128]{1,0:T(8,128)(2,1)S(1)}, bf16[2048,128]{1,0:T(8,128)(2,1)}, u32[]{:S(2)}) copy-start(bf16[2048,128]{1,0:T(8,128)(2,1)} %param.25) | copy-start | bytes 1572868

commit v2 on v1

v2 whole, which is shorter than its diff:
```python
import jax
import jax.numpy as jnp
from jax import lax
from jax.experimental import pallas as pl
from jax.sharding import Mesh
from jax.sharding import PartitionSpec as P

D = 4096
H = 16
DK = 128
DV = 256
KV = ("z", "y")
TP = ("x", "c")
ZX = ("z", "x")
NZ, NY, NX, NC = (8, 4, 4, 2)


EPS = 1e-06


def exchanged(blocks, axis):
    return lax.all_to_all(blocks, axis, split_axis=0, concat_axis=0, tiled=True)


def copy_for_each(array, axis):
    copies = jnp.broadcast_to(array, (lax.axis_size(axis), *array.shape))
    return exchanged(copies, axis)


def summed_on_arrival(blocks, axis):
    return jnp.sum(exchanged(blocks, axis).astype(jnp.float32), axis=0)


def shifted(array, axis, by):
    size = lax.axis_size(axis)
    return lax.ppermute(array, axis, [(i, (i + by) % size) for i in range(size)])


def swapped(array):
    return lax.ppermute(array, "c", [(0, 1), (1, 0)])


def rotate(vectors, positions):
    half = vectors.shape[-1] // 2
    inverse = jnp.power(10000.0, -jnp.arange(half, dtype=jnp.float32) / half)
    angles = positions.astype(jnp.float32)[:, None] * inverse[None, :]
    cosine = jnp.cos(angles)[:, None, :]
    sine = jnp.sin(angles)[:, None, :]
    first, second = (vectors[..., :half], vectors[..., half:])
    return jnp.concatenate(
        [first * cosine - second * sine, first * sine + second * cosine], axis=-1
    )


def head_decay(head_ids):
    return 1.0 - jnp.exp2(-2.0 - 6.0 * head_ids / (H - 1))


def mixer_kernel(own_ref, other_ref, w0_ref, w1_ref, w2a_ref, w2b_ref, w3_ref, out_own_ref, out_other_ref):
    rows = own_ref.shape[1]
    half = NZ // 2

    def weights(z, low, high):
        far = w2a_ref[z, low:high] if z < half else w2b_ref[z - half, low:high]
        return [w0_ref[z, low:high], w1_ref[z, low:high], far, w3_ref[z, low:high]]

    hidden = jnp.zeros((2 * rows, 256), jnp.float32)
    squares = jnp.zeros((2 * rows, 1), jnp.float32)
    for z in range(NZ):
        left = jnp.concatenate([own_ref[z], other_ref[z]], axis=0)
        wide = left.astype(jnp.float32)
        squares = squares + jnp.sum(wide * wide, axis=1, keepdims=True)
        right = [jnp.concatenate(weights(z, 128 * j, 128 * (j + 1)), axis=0) for j in range(2)]
        right = jnp.concatenate(right, axis=1)
        hidden = hidden + jnp.dot(left, right, preferred_element_type=jnp.float32)
    scale = lax.rsqrt(squares / D + EPS)
    positive = jnp.maximum(hidden * scale, 0.0)
    active = (positive * positive).astype(jnp.bfloat16)
    for z in range(NZ):
        right = jnp.concatenate(weights(z, 256, 512), axis=1)
        out = jnp.dot(active, right, preferred_element_type=jnp.float32)
        out_own_ref[z] = out[:rows].astype(jnp.bfloat16)
        out_other_ref[z] = out[rows:].astype(jnp.bfloat16)


def ring(array):
    above = shifted(array, "y", -1)
    below = shifted(array, "y", 1)
    return above, below


def local(
    tokens,
    seq_pos,
    state,
    norm_in_gain,
    query_weight,
    key_weight,
    value_weight,
    gate_weight,
    head_gain,
    out_weight,
    norm_mlp_gain,
    hidden_weight,
    down_weight,
):
    y = lax.axis_index("y")
    weights = jnp.concatenate([query_weight, key_weight, value_weight, gate_weight], axis=1)
    weights = (weights.astype(jnp.float32) * norm_in_gain[:, None]).astype(jnp.bfloat16)
    width = weights.shape[1]
    above, below = ring(weights)
    far_a = shifted(below[:, : width // 2], "y", 1)
    far_b = shifted(above[:, width // 2 :], "y", -1)

    rows = jnp.broadcast_to(tokens.reshape(NY, 1, 16, 128), (NY, NX * NC, 16, 128))
    rows = exchanged(rows.reshape(NY * NX * NC, 16, 128), ("y", "x", "c"))
    rows = rows.reshape(NY, 128, 128)
    rows = lax.dynamic_slice_in_dim(jnp.concatenate([rows, rows], axis=0), y, NY, 0)

    scaled = (hidden_weight.astype(jnp.float32) * norm_mlp_gain[:, None]).astype(jnp.bfloat16)
    scaled = scaled.reshape(128, NZ, 2, 128).transpose(1, 2, 0, 3).reshape(NZ, 256, 128)
    mixer = jnp.concatenate([scaled, down_weight.reshape(NZ, 256, 128)], axis=1)
    mixer = exchanged(mixer, "z")

    def term(left, right):
        return jnp.dot(left, right, preferred_element_type=jnp.float32)

    near = term(rows[0], weights) + term(rows[3], below) + term(rows[1], above)
    far = jnp.concatenate([term(rows[2], far_a), term(rows[2], far_b)], axis=1)
    rows_f = rows.astype(jnp.float32)
    squares = jnp.sum(rows_f * rows_f, axis=(0, 2))[:, None]
    coarse = squares.astype(jnp.bfloat16)
    fine = (squares - coarse.astype(jnp.float32)).astype(jnp.bfloat16)
    terms = jnp.concatenate([(near + far).astype(jnp.bfloat16), coarse, fine], axis=1)
    sums = summed_on_arrival(terms.reshape(NZ, 16, width + 2), "z")
    total_in = sums[:, width] + sums[:, width + 1]
    factor = lax.rsqrt(total_in / D + EPS)[:, None]
    wq, wv = (query_weight.shape[1], value_weight.shape[1])
    query = sums[:, :wq] * factor
    keys = sums[:, wq : 2 * wq] * factor
    values = sums[:, 2 * wq : 2 * wq + wv] * factor
    gates = sums[:, 2 * wq + wv : width] * factor

    mix_above, mix_below = ring(mixer)
    out_above, out_below = ring(out_weight)
    out_far = shifted(out_weight, "y", 2)
    out_wide = jnp.concatenate([out_weight, out_above, out_far, out_below], axis=1)

    local_rows = query.shape[0]
    heads_dev = 2
    turned_query = rotate(query.reshape(local_rows, heads_dev, DK), seq_pos)
    turned_keys = rotate(keys.reshape(local_rows, heads_dev, DK), seq_pos) * DK ** (-0.5)
    head_ids = (lax.axis_index(TP) * heads_dev + jnp.arange(heads_dev, dtype=jnp.int32)).astype(
        jnp.float32
    )
    decay = head_decay(head_ids)
    new_state = decay[None, :, None, None] * state + jnp.einsum(
        "bhk,bhv->bhkv",
        turned_keys,
        values.reshape(local_rows, heads_dev, DV),
        precision=lax.Precision.HIGHEST,
    )
    read = jnp.einsum("bhk,bhkv->bhv", turned_query, new_state, precision=lax.Precision.HIGHEST)
    read = read * lax.rsqrt(jnp.mean(read * read, axis=-1, keepdims=True) + EPS)
    mixed = (
        read.reshape(local_rows, heads_dev * DV) * head_gain[None, :] * jax.nn.silu(gates)
    ).astype(jnp.bfloat16)
    mixed_all = copy_for_each(mixed, "z").reshape(128, heads_dev * DV)
    attn_terms = term(mixed_all, out_wide).astype(jnp.bfloat16)
    attn = summed_on_arrival(attn_terms.reshape(NX * NC, 16, 512), TP)
    mine = rows.reshape(NY, NX * NC, 16, 128)
    mine = lax.dynamic_index_in_dim(mine, lax.axis_index(TP), 1, keepdims=False)
    mine = mine.transpose(1, 0, 2).reshape(16, 512)
    resid = (mine.astype(jnp.float32) + attn).astype(jnp.bfloat16)

    far_low = shifted(mix_below[: NZ // 2], "y", 1)
    far_high = shifted(mix_above[NZ // 2 :], "y", -1)

    own = copy_for_each(resid, ZX).reshape(NZ, 64, 512)
    other = swapped(own)
    blocks = jax.ShapeDtypeStruct((NZ, 64, 512), jnp.bfloat16)
    out_own, out_other = pl.pallas_call(
        mixer_kernel,
        out_shape=(blocks, blocks),
        name="mixer",
    )(own, other, mixer, mix_above, far_low, far_high, mix_below)
    from_other = swapped(out_other)
    partial = (out_own.astype(jnp.float32) + from_other.astype(jnp.float32)).astype(jnp.bfloat16)
    down = summed_on_arrival(partial.reshape(NZ * NX, 16, 512), ZX)
    output = (resid.astype(jnp.float32) + down).astype(jnp.bfloat16)
    output = output.reshape(16, NY, 128).transpose(1, 0, 2)
    output = jnp.concatenate([output, output], axis=0)
    output = lax.dynamic_slice_in_dim(output, (NY - y) % NY, NY, 0)
    output = exchanged(output, "y").reshape(64, 128)
    return (output, new_state)


def solution(mesh):
    torus = Mesh(mesh.devices.reshape(NZ, NY, NX, NC), ("z", "y", "x", "c"))
    return jax.shard_map(
        local,
        mesh=torus,
        in_specs=(
            P(TP, KV),
            P(KV),
            P(KV, TP, None, None),
            P(KV),
            P(KV, TP),
            P(KV, TP),
            P(KV, TP),
            P(KV, TP),
            P(TP),
            P(TP, KV),
            P(KV),
            P(KV, TP),
            P(TP, KV),
        ),
        out_specs=(P(TP, KV), P(KV, TP, None, None)),
        check_vma=False,
    )
```

time: 253 us -> 203 us (0.80)
  blocking collectives: 118 us -> 26.2 us
  starting transfers between devices: 19.5 us -> 53.8 us
  Pallas kernels: 0 us -> 4.77 us
  matrix products: 8.7 us -> 4.1 us
    all_to_all x6 -> x2, blocking collectives: 118 us -> 26.2 us  [exchanged(): return lax.all_to_all(blocks, axis, split_axis=0, concat_axis=0, tiled=True)]
    ppermute x0 -> x13, waiting for transfers between devices: none -> 22.8 us  [the longest x11 21 us: shifted(): lax.ppermute(array, axis, [(i, (i + by) % size) for i in range(size)])]
    all_to_all x3 -> x6, waiting for transfers between devices: 93.5 us -> 71.9 us  [exchanged(): return lax.all_to_all(blocks, axis, split_axis=0, concat_axis=0, tiled=True)]
    ppermute x0 -> x13, starting transfers between devices: none -> 18 us  [the longest x11 13 us: shifted(): lax.ppermute(array, axis, [(i, (i + by) % size) for i in range(size)])]
    all_to_all x3 -> x6, starting transfers between devices: 19.5 us -> 35.8 us  [exchanged(): return lax.all_to_all(blocks, axis, split_axis=0, concat_axis=0, tiled=True)]
    pallas_call x0 -> x1, Pallas kernels: none -> 4.77 us  [local(): pl.pallas_call(mixer_kernel, out_shape=(blocks, blocks), name='mixer')]
    dot_general x7 -> x6, matrix products: 6.6 us -> 2 us  [term(): return jnp.dot(left, right, preferred_element_type=jnp.float32)]
  transfers between devices with their start and end apart: 3 -> 19, of which waited for: 3 -> 12; matrix products, arithmetic and copies ran while one was open for 1% -> 5% of each run, Pallas kernels for 0% -> 0%
where the time goes in v2:
time: 203 us; the launch traced here: 201 us
  waiting for transfers between devices  94.7 us (47%)
  starting transfers between devices  53.8 us (27%)
  blocking collectives  26.2 us (13%)
  local copies, waits for them, and re-layouts  8.34 us (4%)
  other arithmetic  8.31 us (4%)
  Pallas kernels  4.77 us (2%)
  matrix products  4.1 us (2%)
    all_to_all x6, waiting for transfers between devices, exchanged(): return lax.all_to_all(blocks, axis, split_axis=0, concat_axis=0, tiled=True)  71.9 us
    all_to_all x6, starting transfers between devices, exchanged(): return lax.all_to_all(blocks, axis, split_axis=0, concat_axis=0, tiled=True)  35.8 us
    all_to_all x2, blocking collectives, exchanged(): return lax.all_to_all(blocks, axis, split_axis=0, concat_axis=0, tiled=True)  26.2 us
    ppermute x11, waiting for transfers between devices, shifted(): lax.ppermute(array, axis, [(i, (i + by) % size) for i in range(size)])  21 us
    ppermute x11, starting transfers between devices, shifted(): lax.ppermute(array, axis, [(i, (i + by) % size) for i in range(size)])  13 us
    ppermute x2, starting transfers between devices, swapped(): return lax.ppermute(array, 'c', [(0, 1), (1, 0)])  5.02 us
    pallas_call x1, Pallas kernels, local(): pl.pallas_call(mixer_kernel, out_shape=(blocks, blocks), name='mixer')  4.77 us
    unnamed x28, local copies, waits for them, and re-layouts  4.26 us
  transfers between devices with their start and end apart: 19, of which 12 were waited for; matrix products, arithmetic and copies ran while one was open for 5% of the time, Pallas kernels for 0%

profile of v2, /device:TPU:1, one launch (start us, length us, event | category | flops | bytes accessed | tf_op | source)
XLA Modules:
  0.0 201.2 jit_solution(6724005160203984539)
XLA Ops:
  0.6 1.4 broadcast_in_dim.9
  2.0 8.6 %all-to-all-start = ((bf16[32,16,128]{2,1,0:T(8,128)(2,1)}), bf16[32,16,128]{2,1,0:T(8,128)(2,1)S(1)}, u32[]{:S(2)}, u32[]{:S(2)}) async-start(bf16[32,16,128]{2,1,0:T(8,128)(2,1)} %bitcast.1), calls=%async_computation | async-start | bytes 262144 | tf_op jit(solution)/shard_map/all_to_all | solution.py:22
  11.7 2.7 %collective-permute-start.1 = (bf16[128,1536]{1,0:T(8,128)(2,1)S(1)}, bf16[128,1536]{1,0:T(8,128)(2,1)S(1)}, u32[]{:S(2)}, u32[]{:S(2)}) collective-permute-start(bf16[128,1536]{1,0:T(8,128)(2,1)S(1)} %multiply_convert_fusion.1), channel_id=1, source_target_pairs={{0,24},{8,0},{16,8},{24,16},{1,25},{9,1},{17,9},{25,17},{2,26},{10... | collective-permute-start | bytes 1179656 | tf_op jit(solution)/shard_map/ppermute | solution.py:36
  14.4 3.9 %all-to-all-done = bf16[32,16,128]{2,1,0:T(8,128)(2,1)S(1)} async-done(((bf16[32,16,128]{2,1,0:T(8,128)(2,1)}), bf16[32,16,128]{2,1,0:T(8,128)(2,1)S(1)}, u32[]{:S(2)}, u32[]{:S(2)}) %all-to-all-start) | async-done | bytes 131104 | tf_op jit(solution)/shard_map/all_to_all | solution.py:22
  19.1 4.3 %collective-permute-done.1 = bf16[128,1536]{1,0:T(8,128)(2,1)S(1)} collective-permute-done((bf16[128,1536]{1,0:T(8,128)(2,1)S(1)}, bf16[128,1536]{1,0:T(8,128)(2,1)S(1)}, u32[]{:S(2)}, u32[]{:S(2)}) %collective-permute-start.1) | collective-permute-done | bytes 393248 | tf_op jit(solution)/shard_map/ppermute | solution.py:36
  23.4 3.1 %collective-permute-start.3 = (bf16[128,768]{1,0:T(8,128)(2,1)S(1)}, bf16[128,768]{1,0:T(8,128)(2,1)S(1)}, u32[]{:S(2)}, u32[]{:S(2)}) collective-permute-start(bf16[128,768]{1,0:T(8,128)(2,1)S(1)} %slice.78), channel_id=1, source_target_pairs={{0,24},{8,0},{16,8},{24,16},{1,25},{9,1},{17,9},{25,17},{2,26},{10... | collective-permute-start | bytes 589832 | tf_op jit(solution)/shard_map/ppermute | solution.py:36
  26.9 2.9 %collective-permute-done.3 = bf16[128,768]{1,0:T(8,128)(2,1)S(1)} collective-permute-done((bf16[128,768]{1,0:T(8,128)(2,1)S(1)}, bf16[128,768]{1,0:T(8,128)(2,1)S(1)}, u32[]{:S(2)}, u32[]{:S(2)}) %collective-permute-start.3) | collective-permute-done | bytes 196640 | tf_op jit(solution)/shard_map/ppermute | solution.py:36
  29.9 3.0 %collective-permute-done.2 = bf16[128,768]{1,0:T(8,128)(2,1)S(1)} collective-permute-done((bf16[128,768]{1,0:T(8,128)(2,1)S(1)}, bf16[128,768]{1,0:T(8,128)(2,1)S(1)}, u32[]{:S(2)}, u32[]{:S(2)}) %collective-permute-start.2) | collective-permute-done | bytes 196640 | tf_op jit(solution)/shard_map/ppermute | solution.py:36
  34.3 8.2 %all-to-all-start.1 = ((bf16[8,16,1538]{2,1,0:T(8,128)(2,1)}), bf16[8,16,1538]{2,1,0:T(8,128)(2,1)S(1)}, u32[]{:S(2)}, u32[]{:S(2)}) async-start(bf16[8,16,1538]{2,1,0:T(8,128)(2,1)} %concatenate.34), calls=%async_computation.1 | async-start | bytes 851968 | tf_op jit(solution)/shard_map/all_to_all | solution.py:22
  42.6 1.5 collective-permute-start.4
  44.3 10.9 %all-to-all-done.1 = bf16[8,16,1538]{2,1,0:T(8,128)(2,1)S(1)} async-done(((bf16[8,16,1538]{2,1,0:T(8,128)(2,1)}), bf16[8,16,1538]{2,1,0:T(8,128)(2,1)S(1)}, u32[]{:S(2)}, u32[]{:S(2)}) %all-to-all-start.1) | async-done | bytes 393760 | tf_op jit(solution)/shard_map/all_to_all | solution.py:22
  56.0 2.6 %multiply_add_fusion = f32[16,2,128,256]{3,2,1,0:T(8,128)S(1)} fusion(f32[16,2,128,256]{3,2,1,0:T(8,128)} %param.15, f32[16,2,256]{2,1,0:T(2,128)S(1)} %reshape.177, f32[16,2,128]{2,1,0:T(2,128)S(1)} %copy.53, f32[2]{0:T(128)S(1)} %exponential_subtract_fusion), kind=kLoop, calls=%fused_computation | loop fusion | flops 3145728 | bytes 8437768 | tf_op jit(solution)/shard_map/add | solution.py:157
  58.6 2.0 copy-done
  60.6 2.1 %fusion.20 = f32[16,2,1,256]{3,2,1,0:T(1,128)S(1)} fusion(f32[16,2,128,256]{3,2,1,0:T(8,128)S(1)} %multiply_add_fusion, f32[16,2,128,1]{2,0,1,3:T(8,128)S(1)} %maximum_bitcast_fusion), kind=kOutput, calls=%fused_computation.53 | convolution fusion | flops 12582912 | bytes 4243456 | tf_op jit(solution)/shard_map/bhk,bhkv->bhv/dot_general | solution.py:163
  63.7 3.4 %all-to-all-start.2 = ((bf16[8,16,512]{2,1,0:T(8,128)(2,1)}), bf16[8,16,512]{2,1,0:T(8,128)(2,1)S(1)}, u32[]{:S(2)}, u32[]{:S(2)}) async-start(bf16[8,16,512]{2,1,0:T(8,128)(2,1)} %broadcast_in_dim.10), calls=%async_computation.2 | async-start | bytes 262144 | tf_op jit(solution)/shard_map/all_to_all | solution.py:22
  67.8 7.2 %all-to-all-done.2 = bf16[8,16,512]{2,1,0:T(8,128)(2,1)S(1)} async-done(((bf16[8,16,512]{2,1,0:T(8,128)(2,1)}), bf16[8,16,512]{2,1,0:T(8,128)(2,1)S(1)}, u32[]{:S(2)}, u32[]{:S(2)}) %all-to-all-start.2) | async-done | bytes 131104 | tf_op jit(solution)/shard_map/all_to_all | solution.py:22
  75.9 8.2 %all-to-all-start.3 = ((bf16[8,16,512]{2,1,0:T(8,128)(2,1)}), bf16[8,16,512]{2,1,0:T(8,128)(2,1)S(1)}, u32[]{:S(2)}, u32[]{:S(2)}) async-start(bf16[8,16,512]{2,1,0:T(8,128)(2,1)} %bitcast.14), calls=%async_computation.3 | async-start | bytes 262144 | tf_op jit(solution)/shard_map/all_to_all | solution.py:22
  85.2 4.2 %all-to-all-done.3 = bf16[8,16,512]{2,1,0:T(8,128)(2,1)S(1)} async-done(((bf16[8,16,512]{2,1,0:T(8,128)(2,1)}), bf16[8,16,512]{2,1,0:T(8,128)(2,1)S(1)}, u32[]{:S(2)}, u32[]{:S(2)}) %all-to-all-start.3) | async-done | bytes 131104 | tf_op jit(solution)/shard_map/all_to_all | solution.py:22
  89.4 3.6 %all-to-all-start.5 = ((bf16[8,512,128]{2,1,0:T(8,128)(2,1)}), bf16[8,512,128]{2,1,0:T(8,128)(2,1)S(1)}, u32[]{:S(2)}, u32[]{:S(2)}) async-start(bf16[8,512,128]{2,1,0:T(8,128)(2,1)} %pad_maximum_fusion), calls=%async_computation.5 | async-start | bytes 2097152 | tf_op jit(solution)/shard_map/all_to_all | solution.py:22
  92.9 29.1 %all-to-all-done.5.w0_ref = bf16[8,512,128]{2,1,0:T(8,128)(2,1)S(1)} async-done(((bf16[8,512,128]{2,1,0:T(8,128)(2,1)}), bf16[8,512,128]{2,1,0:T(8,128)(2,1)S(1)}, u32[]{:S(2)}, u32[]{:S(2)}) %all-to-all-start.5) | async-done | bytes 1048608 | tf_op jit(solution)/shard_map/all_to_all | solution.py:22
  122.1 2.7 %collective-permute-start.8 = (bf16[8,512,128]{2,1,0:T(8,128)(2,1)S(1)}, bf16[8,512,128]{2,1,0:T(8,128)(2,1)S(1)}, u32[]{:S(2)}, u32[]{:S(2)}) collective-permute-start(bf16[8,512,128]{2,1,0:T(8,128)(2,1)S(1)} %all-to-all-done.5.w0_ref), channel_id=1, source_target_pairs={{0,24},{8,0},{16,8},{24,16},{1,25},{9,1},{17,9},{25,17},{2,26},{10... | collective-permute-start | bytes 3145736 | tf_op jit(solution)/shard_map/ppermute | solution.py:36
  124.8 18.8 %all_to_all.40 = bf16[32,16,512]{2,1,0:T(8,128)(2,1)S(1)} all-to-all(bf16[32,16,512]{2,1,0:T(8,128)(2,1)S(1)} %broadcast_in_dim.11), channel_id=1, replica_groups=mesh['z'=8,'y'=4,'x'=4,'c'=2] {'z','x'}, dimensions={0} | all-to-all | bytes 1048576 | tf_op jit(solution)/shard_map/all_to_all | solution.py:22
  143.6 2.8 %collective-permute-start.7 = (bf16[8,64,512]{2,1,0:T(8,128)(2,1)S(1)}, bf16[8,64,512]{2,1,0:T(8,128)(2,1)S(1)}, u32[]{:S(2)}, u32[]{:S(2)}) collective-permute-start(bf16[8,64,512]{2,1,0:T(8,128)(2,1)S(1)} %bitcast.81), channel_id=1, source_target_pairs={{0,1},{1,0},{2,3},{3,2},{4,5},{5,4},{6,7},{7,6},{8,9},{9,8},{10,11... | collective-permute-start | bytes 1572872 | tf_op jit(solution)/shard_map/ppermute | solution.py:40
  147.7 2.7 %collective-permute-start.11 = (bf16[4,512,128]{2,1,0:T(8,128)(2,1)S(1)}, bf16[4,512,128]{2,1,0:T(8,128)(2,1)}, u32[]{:S(2)}, u32[]{:S(2)}) collective-permute-start(bf16[4,512,128]{2,1,0:T(8,128)(2,1)S(1)} %slice.90), channel_id=1, source_target_pairs={{0,24},{8,0},{16,8},{24,16},{1,25},{9,1},{17,9},{25,17},{2,26},{10... | collective-permute-start | bytes 1572872 | tf_op jit(solution)/shard_map/ppermute | solution.py:36
  151.2 9.7 %collective-permute-done.10.w2a_ref = bf16[4,512,128]{2,1,0:T(8,128)(2,1)S(1)} collective-permute-done((bf16[4,512,128]{2,1,0:T(8,128)(2,1)S(1)}, bf16[4,512,128]{2,1,0:T(8,128)(2,1)S(1)}, u32[]{:S(2)}, u32[]{:S(2)}) %collective-permute-start.10) | collective-permute-done | bytes 524320 | tf_op jit(solution)/shard_map/ppermute | solution.py:36
  161.8 4.8 %mixer.1 = (bf16[8,64,512]{2,1,0:T(8,128)(2,1)}, bf16[8,64,512]{2,1,0:T(8,128)(2,1)}) custom-call(bf16[8,64,512]{2,1,0:T(8,128)(2,1)} %bitcast.82, bf16[8,64,512]{2,1,0:T(8,128)(2,1)} %copy-done.5, bf16[8,512,128]{2,1,0:T(8,128)(2,1)} %copy-done.1, bf16[8,512,128]{2,1,0:T(8,128)(2,1)} %copy-done.3, bf16[4,512,128]{2,1,0:T(8,128)(2,1)} %copy-done.6, ...), custom_call_target="tpu_custom_call" | custom-call | tf_op jit(solution)/shard_map/mixer/pallas_call | solution.py:182
  166.6 2.2 %collective-permute-start.12 = (bf16[8,64,512]{2,1,0:T(8,128)(2,1)}, bf16[8,64,512]{2,1,0:T(8,128)(2,1)S(1)}, u32[]{:S(2)}, u32[]{:S(2)}) collective-permute-start(bf16[8,64,512]{2,1,0:T(8,128)(2,1)} %get-tuple-element.5), channel_id=1, source_target_pairs={{0,1},{1,0},{2,3},{3,2},{4,5},{5,4},{6,7},{7,6},{8,9},{9,8},{10,11... | collective-permute-start | bytes 1572872 | tf_op jit(solution)/shard_map/ppermute | solution.py:40
  168.8 1.7 collective-permute-done.12
  170.5 2.0 add_convert_fusion
  172.5 3.9 %all-to-all-start.6 = ((bf16[32,16,512]{2,1,0:T(8,128)(2,1)}), bf16[32,16,512]{2,1,0:T(8,128)(2,1)S(1)}, u32[]{:S(2)}, u32[]{:S(2)}) async-start(bf16[32,16,512]{2,1,0:T(8,128)(2,1)} %bitcast.20), calls=%async_computation.6 | async-start | bytes 1048576 | tf_op jit(solution)/shard_map/all_to_all | solution.py:22
  176.4 16.6 %all-to-all-done.6 = bf16[32,16,512]{2,1,0:T(8,128)(2,1)S(1)} async-done(((bf16[32,16,512]{2,1,0:T(8,128)(2,1)}), bf16[32,16,512]{2,1,0:T(8,128)(2,1)S(1)}, u32[]{:S(2)}, u32[]{:S(2)}) %all-to-all-start.6) | async-done | bytes 524320 | tf_op jit(solution)/shard_map/all_to_all | solution.py:22
  193.2 7.4 %all_to_all.41 = bf16[4,16,128]{2,1,0:T(8,128)(2,1)S(1)} all-to-all(bf16[4,16,128]{2,1,0:T(8,128)(2,1)S(1)} %fusion.18), channel_id=1, replica_groups=mesh['z'=8,'y'=4,'x'=4,'c'=2] {'y'}, dimensions={0} | all-to-all | bytes 32768 | tf_op jit(solution)/shard_map/all_to_all | solution.py:22
  (89 shorter events, 12.1 us)
Async XLA Ops:
  2.0 16.3 %all-to-all-start = ((bf16[32,16,128]{2,1,0:T(8,128)(2,1)}), bf16[32,16,128]{2,1,0:T(8,128)(2,1)S(1)}, u32[]{:S(2)}, u32[]{:S(2)}) async-start(bf16[32,16,128]{2,1,0:T(8,128)(2,1)} %bitcast.1), calls=%async_computation | async-start | bytes 262144 | tf_op jit(solution)/shard_map/all_to_all | solution.py:22
  11.7 11.7 %collective-permute-start.1 = (bf16[128,1536]{1,0:T(8,128)(2,1)S(1)}, bf16[128,1536]{1,0:T(8,128)(2,1)S(1)}, u32[]{:S(2)}, u32[]{:S(2)}) collective-permute-start(bf16[128,1536]{1,0:T(8,128)(2,1)S(1)} %multiply_convert_fusion.1), channel_id=1, source_target_pairs={{0,24},{8,0},{16,8},{24,16},{1,25},{9,1},{17,9},{25,17},{2,26},{10... | collective-permute-start | bytes 1179656 | tf_op jit(solution)/shard_map/ppermute | solution.py:36
  14.4 12.1 %collective-permute-start = (bf16[128,1536]{1,0:T(8,128)(2,1)S(1)}, bf16[128,1536]{1,0:T(8,128)(2,1)S(1)}, u32[]{:S(2)}, u32[]{:S(2)}) collective-permute-start(bf16[128,1536]{1,0:T(8,128)(2,1)S(1)} %multiply_convert_fusion.1), channel_id=1, source_target_pairs={{0,8},{8,16},{16,24},{24,0},{1,9},{9,17},{17,25},{25,1},{2,10},{10... | collective-permute-start | bytes 1179656 | tf_op jit(solution)/shard_map/ppermute | solution.py:36
  19.1 23.4 %copy-start.11 = (bf16[512,128]{1,0:T(8,128)(2,1)S(1)}, bf16[512,128]{1,0:T(8,128)(2,1)}, u32[]{:S(2)}) copy-start(bf16[512,128]{1,0:T(8,128)(2,1)} %param.22) | copy-start | bytes 393220
  19.1 25.0 %copy-start.12 = (s32[16]{0:T(128)S(1)}, s32[16]{0:T(128)}, u32[]{:S(2)}) copy-start(s32[16]{0:T(128)} %param.14) | copy-start | bytes 196
  23.4 6.3 %collective-permute-start.3 = (bf16[128,768]{1,0:T(8,128)(2,1)S(1)}, bf16[128,768]{1,0:T(8,128)(2,1)S(1)}, u32[]{:S(2)}, u32[]{:S(2)}) collective-permute-start(bf16[128,768]{1,0:T(8,128)(2,1)S(1)} %slice.78), channel_id=1, source_target_pairs={{0,24},{8,0},{16,8},{24,16},{1,25},{9,1},{17,9},{25,17},{2,26},{10... | collective-permute-start | bytes 589832 | tf_op jit(solution)/shard_map/ppermute | solution.py:36
  26.5 6.4 %collective-permute-start.2 = (bf16[128,768]{1,0:T(8,128)(2,1)S(1)}, bf16[128,768]{1,0:T(8,128)(2,1)S(1)}, u32[]{:S(2)}, u32[]{:S(2)}) collective-permute-start(bf16[128,768]{1,0:T(8,128)(2,1)S(1)} %slice.77), channel_id=1, source_target_pairs={{0,8},{8,16},{16,24},{24,0},{1,9},{9,17},{17,25},{25,1},{2,10},{10... | collective-permute-start | bytes 589832 | tf_op jit(solution)/shard_map/ppermute | solution.py:36
  34.3 20.9 %all-to-all-start.1 = ((bf16[8,16,1538]{2,1,0:T(8,128)(2,1)}), bf16[8,16,1538]{2,1,0:T(8,128)(2,1)S(1)}, u32[]{:S(2)}, u32[]{:S(2)}) async-start(bf16[8,16,1538]{2,1,0:T(8,128)(2,1)} %concatenate.34), calls=%async_computation.1 | async-start | bytes 851968 | tf_op jit(solution)/shard_map/all_to_all | solution.py:22
  42.5 25.3 %collective-permute-start.5 = (bf16[512,128]{1,0:T(8,128)(2,1)S(1)}, bf16[512,128]{1,0:T(8,128)(2,1)S(1)}, u32[]{:S(2)}, u32[]{:S(2)}) collective-permute-start(bf16[512,128]{1,0:T(8,128)(2,1)S(1)} %copy-done.11), channel_id=1, source_target_pairs={{0,16},{8,24},{16,0},{24,8},{1,17},{9,25},{17,1},{25,9},{2,18},{10... | collective-permute-start | bytes 393224 | tf_op jit(solution)/shard_map/ppermute | solution.py:36
  42.6 25.2 %collective-permute-start.4 = (bf16[512,128]{1,0:T(8,128)(2,1)S(1)}, bf16[512,128]{1,0:T(8,128)(2,1)S(1)}, u32[]{:S(2)}, u32[]{:S(2)}) collective-permute-start(bf16[512,128]{1,0:T(8,128)(2,1)S(1)} %copy-done.11), channel_id=1, source_target_pairs={{0,24},{8,0},{16,8},{24,16},{1,25},{9,1},{17,9},{25,17},{2,26},{10... | collective-permute-start | bytes 393224 | tf_op jit(solution)/shard_map/ppermute | solution.py:36
  44.0 23.8 %collective-permute-start.6 = (bf16[512,128]{1,0:T(8,128)(2,1)S(1)}, bf16[512,128]{1,0:T(8,128)(2,1)S(1)}, u32[]{:S(2)}, u32[]{:S(2)}) collective-permute-start(bf16[512,128]{1,0:T(8,128)(2,1)S(1)} %copy-done.11), channel_id=1, source_target_pairs={{0,8},{8,16},{16,24},{24,0},{1,9},{9,17},{17,25},{25,1},{2,10},{10... | collective-permute-start | bytes 393224 | tf_op jit(solution)/shard_map/ppermute | solution.py:36
  58.6 2.0 %copy-start = (f32[16,2,128,256]{3,2,1,0:T(8,128)}, f32[16,2,128,256]{3,2,1,0:T(8,128)S(1)}, u32[]{:S(2)}) copy-start(f32[16,2,128,256]{3,2,1,0:T(8,128)S(1)} %multiply_add_fusion) | copy-start | bytes 12582916
  60.6 2.3 %copy-start.9 = (f32[512]{0:T(512)S(1)}, f32[512]{0:T(512)}, u32[]{:S(2)}) copy-start(f32[512]{0:T(512)} %param.21) | copy-start | bytes 6148
  60.6 6.5 %copy-start.7 = (bf16[128,2048]{1,0:T(8,128)(2,1)S(1)}, bf16[128,2048]{1,0:T(8,128)(2,1)}, u32[]{:S(2)}) copy-start(bf16[128,2048]{1,0:T(8,128)(2,1)} %param.24) | copy-start | bytes 1572868
  60.6 6.5 %copy-start.10 = (f32[128]{0:T(128)S(1)}, f32[128]{0:T(128)}, u32[]{:S(2)}) copy-start(f32[128]{0:T(128)} %param.23) | copy-start | bytes 1540
  60.6 23.5 %copy-start.8 = (bf16[2048,128]{1,0:T(8,128)(2,1)S(1)}, bf16[2048,128]{1,0:T(8,128)(2,1)}, u32[]{:S(2)}) copy-start(bf16[2048,128]{1,0:T(8,128)(2,1)} %param.25) | copy-start | bytes 1572868
  63.7 11.3 %all-to-all-start.2 = ((bf16[8,16,512]{2,1,0:T(8,128)(2,1)}), bf16[8,16,512]{2,1,0:T(8,128)(2,1)S(1)}, u32[]{:S(2)}, u32[]{:S(2)}) async-start(bf16[8,16,512]{2,1,0:T(8,128)(2,1)} %broadcast_in_dim.10), calls=%async_computation.2 | async-start | bytes 262144 | tf_op jit(solution)/shard_map/all_to_all | solution.py:22
  75.9 13.4 %all-to-all-start.3 = ((bf16[8,16,512]{2,1,0:T(8,128)(2,1)}), bf16[8,16,512]{2,1,0:T(8,128)(2,1)S(1)}, u32[]{:S(2)}, u32[]{:S(2)}) async-start(bf16[8,16,512]{2,1,0:T(8,128)(2,1)} %bitcast.14), calls=%async_computation.3 | async-start | bytes 262144 | tf_op jit(solution)/shard_map/all_to_all | solution.py:22
  89.4 32.7 %all-to-all-start.5 = ((bf16[8,512,128]{2,1,0:T(8,128)(2,1)}), bf16[8,512,128]{2,1,0:T(8,128)(2,1)S(1)}, u32[]{:S(2)}, u32[]{:S(2)}) async-start(bf16[8,512,128]{2,1,0:T(8,128)(2,1)} %pad_maximum_fusion), calls=%async_computation.5 | async-start | bytes 2097152 | tf_op jit(solution)/shard_map/all_to_all | solution.py:22
  122.1 39.7 %copy-start.1 = (bf16[8,512,128]{2,1,0:T(8,128)(2,1)}, bf16[8,512,128]{2,1,0:T(8,128)(2,1)S(1)}, u32[]{:S(2)}) copy-start(bf16[8,512,128]{2,1,0:T(8,128)(2,1)S(1)} %all-to-all-done.5.w0_ref) | copy-start | bytes 3145732
  122.1 25.4 %collective-permute-start.9 = (bf16[8,512,128]{2,1,0:T(8,128)(2,1)S(1)}, bf16[8,512,128]{2,1,0:T(8,128)(2,1)S(1)}, u32[]{:S(2)}, u32[]{:S(2)}) collective-permute-start(bf16[8,512,128]{2,1,0:T(8,128)(2,1)S(1)} %all-to-all-done.5.w0_ref), channel_id=1, source_target_pairs={{0,8},{8,16},{16,24},{24,0},{1,9},{9,17},{17,25},{25,1},{2,10},{10... | collective-permute-start | bytes 3145736 | tf_op jit(solution)/shard_map/ppermute | solution.py:36
  122.1 25.6 %collective-permute-start.8 = (bf16[8,512,128]{2,1,0:T(8,128)(2,1)S(1)}, bf16[8,512,128]{2,1,0:T(8,128)(2,1)S(1)}, u32[]{:S(2)}, u32[]{:S(2)}) collective-permute-start(bf16[8,512,128]{2,1,0:T(8,128)(2,1)S(1)} %all-to-all-done.5.w0_ref), channel_id=1, source_target_pairs={{0,24},{8,0},{16,8},{24,16},{1,25},{9,1},{17,9},{25,17},{2,26},{10... | collective-permute-start | bytes 3145736 | tf_op jit(solution)/shard_map/ppermute | solution.py:36
  143.6 4.0 %copy-start.4 = (bf16[32,16,512]{2,1,0:T(8,128)(2,1)}, bf16[32,16,512]{2,1,0:T(8,128)(2,1)S(1)}, u32[]{:S(2)}) copy-start(bf16[32,16,512]{2,1,0:T(8,128)(2,1)S(1)} %all_to_all.40) | copy-start | bytes 1572868
  143.6 6.8 %collective-permute-start.7 = (bf16[8,64,512]{2,1,0:T(8,128)(2,1)S(1)}, bf16[8,64,512]{2,1,0:T(8,128)(2,1)S(1)}, u32[]{:S(2)}, u32[]{:S(2)}) collective-permute-start(bf16[8,64,512]{2,1,0:T(8,128)(2,1)S(1)} %bitcast.81), channel_id=1, source_target_pairs={{0,1},{1,0},{2,3},{3,2},{4,5},{5,4},{6,7},{7,6},{8,9},{9,8},{10,11... | collective-permute-start | bytes 1572872 | tf_op jit(solution)/shard_map/ppermute | solution.py:40
  147.5 14.3 %copy-start.2 = (bf16[8,512,128]{2,1,0:T(8,128)(2,1)}, bf16[8,512,128]{2,1,0:T(8,128)(2,1)S(1)}, u32[]{:S(2)}) copy-start(bf16[8,512,128]{2,1,0:T(8,128)(2,1)S(1)} %collective-permute-done.9.w3_ref) | copy-start | bytes 3145732
  147.5 13.4 %collective-permute-start.10 = (bf16[4,512,128]{2,1,0:T(8,128)(2,1)S(1)}, bf16[4,512,128]{2,1,0:T(8,128)(2,1)S(1)}, u32[]{:S(2)}, u32[]{:S(2)}) collective-permute-start(bf16[4,512,128]{2,1,0:T(8,128)(2,1)S(1)} %slice.89), channel_id=1, source_target_pairs={{0,8},{8,16},{16,24},{24,0},{1,9},{9,17},{17,25},{25,1},{2,10},{10... | collective-permute-start | bytes 1572872 | tf_op jit(solution)/shard_map/ppermute | solution.py:36
  147.7 14.1 %copy-start.3 = (bf16[8,512,128]{2,1,0:T(8,128)(2,1)}, bf16[8,512,128]{2,1,0:T(8,128)(2,1)S(1)}, u32[]{:S(2)}) copy-start(bf16[8,512,128]{2,1,0:T(8,128)(2,1)S(1)} %collective-permute-done.8.w1_ref) | copy-start | bytes 3145732
  147.7 14.1 %collective-permute-start.11 = (bf16[4,512,128]{2,1,0:T(8,128)(2,1)S(1)}, bf16[4,512,128]{2,1,0:T(8,128)(2,1)}, u32[]{:S(2)}, u32[]{:S(2)}) collective-permute-start(bf16[4,512,128]{2,1,0:T(8,128)(2,1)S(1)} %slice.90), channel_id=1, source_target_pairs={{0,24},{8,0},{16,8},{24,16},{1,25},{9,1},{17,9},{25,17},{2,26},{10... | collective-permute-start | bytes 1572872 | tf_op jit(solution)/shard_map/ppermute | solution.py:36
  150.4 0.8 copy-start.5
  161.0 0.8 copy-start.6
  166.6 4.0 %collective-permute-start.12 = (bf16[8,64,512]{2,1,0:T(8,128)(2,1)}, bf16[8,64,512]{2,1,0:T(8,128)(2,1)S(1)}, u32[]{:S(2)}, u32[]{:S(2)}) collective-permute-start(bf16[8,64,512]{2,1,0:T(8,128)(2,1)} %get-tuple-element.5), channel_id=1, source_target_pairs={{0,1},{1,0},{2,3},{3,2},{4,5},{5,4},{6,7},{7,6},{8,9},{9,8},{10,11... | collective-permute-start | bytes 1572872 | tf_op jit(solution)/shard_map/ppermute | solution.py:40
  172.5 20.5 %all-to-all-start.6 = ((bf16[32,16,512]{2,1,0:T(8,128)(2,1)}), bf16[32,16,512]{2,1,0:T(8,128)(2,1)S(1)}, u32[]{:S(2)}, u32[]{:S(2)}) async-start(bf16[32,16,512]{2,1,0:T(8,128)(2,1)} %bitcast.20), calls=%async_computation.6 | async-start | bytes 1048576 | tf_op jit(solution)/shard_map/all_to_all | solution.py:22

commit v3 on v2

--- a/solution.py
+++ b/solution.py
@@ -2,6 +2,7 @@
 import jax.numpy as jnp
 from jax import lax
 from jax.experimental import pallas as pl
+from jax.experimental.pallas import tpu as pltpu
 from jax.sharding import Mesh
 from jax.sharding import PartitionSpec as P
 
@@ -56,31 +57,71 @@
     return 1.0 - jnp.exp2(-2.0 - 6.0 * head_ids / (H - 1))
 
 
-def mixer_kernel(own_ref, other_ref, w0_ref, w1_ref, w2a_ref, w2b_ref, w3_ref, out_own_ref, out_other_ref):
+def far_block(low_ref, high_ref, z, size):
+    half = NZ // 2
+    ref, at = (low_ref, z) if z < half else (high_ref, z - half)
+    return ref.at[pl.ds(at * size, size)]
+
+
+def hidden_kernel(own_ref, other_ref, w0_ref, w1_ref, w2a_ref, w2b_ref, w3_ref, out_ref, x_ref, w_ref, x_sem, w_sem):
+    me = lax.axis_index("c")
+    copies = []
+    for z in range(NZ):
+        parts = [
+            pltpu.make_async_copy(own_ref.at[z], x_ref.at[z, me], x_sem.at[z, 0]),
+            pltpu.make_async_copy(other_ref.at[z], x_ref.at[z, 1 - me], x_sem.at[z, 1]),
+        ]
+        far = w2a_ref.at[z] if z < NZ // 2 else w2b_ref.at[z - NZ // 2]
+        for r, ref in enumerate([w0_ref.at[z], w1_ref.at[z], far, w3_ref.at[z]]):
+            parts.append(pltpu.make_async_copy(ref, w_ref.at[z, r], w_sem.at[z, r]))
+        for copy in parts:
+            copy.start()
+        copies.append(parts)
     rows = own_ref.shape[1]
-    half = NZ // 2
-
-    def weights(z, low, high):
-        far = w2a_ref[z, low:high] if z < half else w2b_ref[z - half, low:high]
-        return [w0_ref[z, low:high], w1_ref[z, low:high], far, w3_ref[z, low:high]]
-
     hidden = jnp.zeros((2 * rows, 256), jnp.float32)
     squares = jnp.zeros((2 * rows, 1), jnp.float32)
     for z in range(NZ):
-        left = jnp.concatenate([own_ref[z], other_ref[z]], axis=0)
+        for copy in copies[z]:
+            copy.wait()
+        left = x_ref[z].reshape(2 * rows, 512)
         wide = left.astype(jnp.float32)
         squares = squares + jnp.sum(wide * wide, axis=1, keepdims=True)
-        right = [jnp.concatenate(weights(z, 128 * j, 128 * (j + 1)), axis=0) for j in range(2)]
+        right = [w_ref[z, :, 128 * j : 128 * (j + 1), :].reshape(512, 128) for j in range(2)]
         right = jnp.concatenate(right, axis=1)
         hidden = hidden + jnp.dot(left, right, preferred_element_type=jnp.float32)
     scale = lax.rsqrt(squares / D + EPS)
     positive = jnp.maximum(hidden * scale, 0.0)
     active = (positive * positive).astype(jnp.bfloat16)
     for z in range(NZ):
-        right = jnp.concatenate(weights(z, 256, 512), axis=1)
-        out = jnp.dot(active, right, preferred_element_type=jnp.float32)
-        out_own_ref[z] = out[:rows].astype(jnp.bfloat16)
-        out_other_ref[z] = out[rows:].astype(jnp.bfloat16)
+        out_ref[z] = active
+
+
+def down_kernel(act_ref, resid_ref, w0_ref, w1_ref, w2a_ref, w2b_ref, w3_ref, out_ref, a_ref, w_ref, a_sem, w_sem):
+    y, x, c = (lax.axis_index("y"), lax.axis_index("x"), lax.axis_index("c"))
+    copies = []
+    for z in range(NZ):
+        parts = [pltpu.make_async_copy(act_ref.at[z], a_ref.at[z], a_sem.at[z])]
+        near = [ref.at[pl.ds(256 * z, 256)] for ref in (w0_ref, w1_ref, w3_ref)]
+        blocks = [near[0], near[1], far_block(w2a_ref, w2b_ref, z, 256), near[2]]
+        for r, ref in enumerate(blocks):
+            parts.append(pltpu.make_async_copy(ref, w_ref.at[z, r], w_sem.at[z, r]))
+        for copy in parts:
+            copy.start()
+        copies.append(parts)
+    total = jnp.zeros((128, 512), jnp.float32)
+    for z in range(NZ):
+        for copy in copies[z]:
+            copy.wait()
+        right = jnp.concatenate([w_ref[z, r] for r in range(NY)], axis=1)
+        total = total + jnp.dot(a_ref[z], right, preferred_element_type=jnp.float32)
+    resid = resid_ref[...].astype(jnp.float32)
+    for cc in range(NC):
+        for xx in range(NX):
+            rows = total[(cc * NX + xx) * 16 : (cc * NX + xx + 1) * 16]
+            mine = jnp.logical_and(x == xx, c == cc)
+            rows = (rows + jnp.where(mine, resid, 0.0)).astype(jnp.bfloat16)
+            for r in range(NY):
+                out_ref[lax.rem(y + r, NY), xx * NC + cc] = rows[:, 128 * r : 128 * (r + 1)]
 
 
 def ring(array):
@@ -119,8 +160,7 @@
 
     scaled = (hidden_weight.astype(jnp.float32) * norm_mlp_gain[:, None]).astype(jnp.bfloat16)
     scaled = scaled.reshape(128, NZ, 2, 128).transpose(1, 2, 0, 3).reshape(NZ, 256, 128)
-    mixer = jnp.concatenate([scaled, down_weight.reshape(NZ, 256, 128)], axis=1)
-    mixer = exchanged(mixer, "z")
+    mixer = exchanged(scaled, "z")
 
     def term(left, right):
         return jnp.dot(left, right, preferred_element_type=jnp.float32)
@@ -142,9 +182,11 @@
     gates = sums[:, 2 * wq + wv : width] * factor
 
     mix_above, mix_below = ring(mixer)
+    down_above, down_below = ring(down_weight)
     out_above, out_below = ring(out_weight)
     out_far = shifted(out_weight, "y", 2)
     out_wide = jnp.concatenate([out_weight, out_above, out_far, out_below], axis=1)
+    out_wide = lax.optimization_barrier(out_wide)
 
     local_rows = query.shape[0]
     heads_dev = 2
@@ -176,22 +218,40 @@
     far_low = shifted(mix_below[: NZ // 2], "y", 1)
     far_high = shifted(mix_above[NZ // 2 :], "y", -1)
 
+    down_low = shifted(down_below[:1024], "y", 1)
+    down_high = shifted(down_above[1024:], "y", -1)
+
     own = copy_for_each(resid, ZX).reshape(NZ, 64, 512)
     other = swapped(own)
-    blocks = jax.ShapeDtypeStruct((NZ, 64, 512), jnp.bfloat16)
-    out_own, out_other = pl.pallas_call(
-        mixer_kernel,
-        out_shape=(blocks, blocks),
-        name="mixer",
+    anywhere = pl.BlockSpec(memory_space=pl.ANY)
+    active = pl.pallas_call(
+        hidden_kernel,
+        out_shape=jax.ShapeDtypeStruct((NZ, 128, 256), jnp.bfloat16),
+        in_specs=[anywhere] * 7,
+        scratch_shapes=[
+            pltpu.VMEM((NZ, NC, 64, 512), jnp.bfloat16),
+            pltpu.VMEM((NZ, NY, 256, 128), jnp.bfloat16),
+            pltpu.SemaphoreType.DMA((NZ, 2)),
+            pltpu.SemaphoreType.DMA((NZ, NY)),
+        ],
+        name="hidden",
     )(own, other, mixer, mix_above, far_low, far_high, mix_below)
-    from_other = swapped(out_other)
-    partial = (out_own.astype(jnp.float32) + from_other.astype(jnp.float32)).astype(jnp.bfloat16)
-    down = summed_on_arrival(partial.reshape(NZ * NX, 16, 512), ZX)
-    output = (resid.astype(jnp.float32) + down).astype(jnp.bfloat16)
-    output = output.reshape(16, NY, 128).transpose(1, 0, 2)
-    output = jnp.concatenate([output, output], axis=0)
-    output = lax.dynamic_slice_in_dim(output, (NY - y) % NY, NY, 0)
-    output = exchanged(output, "y").reshape(64, 128)
+    active = exchanged(active, "z")
+    partial = pl.pallas_call(
+        down_kernel,
+        out_shape=jax.ShapeDtypeStruct((NY, NX * NC, 16, 128), jnp.bfloat16),
+        in_specs=[anywhere, pl.BlockSpec(memory_space=pltpu.VMEM)] + [anywhere] * 5,
+        scratch_shapes=[
+            pltpu.VMEM((NZ, 128, 256), jnp.bfloat16),
+            pltpu.VMEM((NZ, NY, 256, 128), jnp.bfloat16),
+            pltpu.SemaphoreType.DMA((NZ,)),
+            pltpu.SemaphoreType.DMA((NZ, NY)),
+        ],
+        name="down",
+    )(active, resid, down_weight, down_above, down_low, down_high, down_below)
+    partial = exchanged(partial.reshape(NY * NX * NC, 16, 128), ("y", "x", "c"))
+    output = jnp.sum(partial.reshape(NY, NX * NC, 16, 128).astype(jnp.float32), axis=1)
+    output = output.astype(jnp.bfloat16).reshape(64, 128)
     return (output, new_state)
 
 

time: 203 us -> 197 us (0.970)
  blocking collectives: 26.2 us -> 16.4 us
  starting transfers between devices: 53.8 us -> 59.5 us
  waiting for transfers between devices: 94.7 us -> 90.5 us
  Pallas kernels: 4.77 us -> 7.67 us
  other arithmetic: 8.31 us -> 5.76 us
  local copies, waits for them, and re-layouts: 8.34 us -> 10.8 us
    all_to_all x6 -> x7, waiting for transfers between devices: 71.9 us -> 57.7 us  [exchanged(): return lax.all_to_all(blocks, axis, split_axis=0, concat_axis=0, tiled=True)]
    ppermute x11 -> x15, waiting for transfers between devices: 21 us -> 32.8 us  [shifted(): lax.ppermute(array, axis, [(i, (i + by) % size) for i in range(size)])]
    all_to_all x2 -> x1, blocking collectives: 26.2 us -> 16.4 us  [exchanged(): return lax.all_to_all(blocks, axis, split_axis=0, concat_axis=0, tiled=True)]
    ppermute x11 -> x15, starting transfers between devices: 13 us -> 18.2 us  [shifted(): lax.ppermute(array, axis, [(i, (i + by) % size) for i in range(size)])]
    all_to_all x6 -> x7, starting transfers between devices: 35.8 us -> 39.2 us  [exchanged(): return lax.all_to_all(blocks, axis, split_axis=0, concat_axis=0, tiled=True)]
    pallas_call x1 -> x2, Pallas kernels: 4.77 us -> 7.67 us  [the longest x1 3.92 us: local(): pl.pallas_call(down_kernel, out_shape=jax.ShapeDtypeStruct((NY, NX * NC,...]
    ppermute x2 -> x1, starting transfers between devices: 5.02 us -> 2.14 us  [swapped(): return lax.ppermute(array, 'c', [(0, 1), (1, 0)])]
    unnamed x28 -> x39, local copies, waits for them, and re-layouts: 4.26 us -> 5.05 us
  transfers between devices with their start and end apart: 19 -> 23, of which waited for: 12 -> 12; matrix products, arithmetic and copies ran while one was open for 5% -> 5% of each run, Pallas kernels for 0% -> 0%
where the time goes in v3:
time: 197 us; the launch traced here: 196 us
  waiting for transfers between devices  90.5 us (46%)
  starting transfers between devices  59.5 us (30%)
  blocking collectives  16.4 us (8%)
  local copies, waits for them, and re-layouts  10.8 us (5%)
  Pallas kernels  7.67 us (4%)
  other arithmetic  5.76 us (3%)
  matrix products  4.1 us (2%)
    all_to_all x7, waiting for transfers between devices, exchanged(): return lax.all_to_all(blocks, axis, split_axis=0, concat_axis=0, tiled=True)  57.7 us
    all_to_all x7, starting transfers between devices, exchanged(): return lax.all_to_all(blocks, axis, split_axis=0, concat_axis=0, tiled=True)  39.2 us
    ppermute x15, waiting for transfers between devices, shifted(): lax.ppermute(array, axis, [(i, (i + by) % size) for i in range(size)])  32.8 us
    ppermute x15, starting transfers between devices, shifted(): lax.ppermute(array, axis, [(i, (i + by) % size) for i in range(size)])  18.2 us
    all_to_all x1, blocking collectives, exchanged(): return lax.all_to_all(blocks, axis, split_axis=0, concat_axis=0, tiled=True)  16.4 us
    unnamed x39, local copies, waits for them, and re-layouts  5.05 us
  transfers between devices with their start and end apart: 23, of which 12 were waited for; matrix products, arithmetic and copies ran while one was open for 5% of the time, Pallas kernels for 0%

profile of v3, /device:TPU:1, one launch (start us, length us, event | category | flops | bytes accessed | tf_op | source)
XLA Modules:
  0.0 195.9 jit_solution(7431195639271256170)
XLA Ops:
  2.0 8.6 %all-to-all-start = ((bf16[32,16,128]{2,1,0:T(8,128)(2,1)}), bf16[32,16,128]{2,1,0:T(8,128)(2,1)S(1)}, u32[]{:S(2)}, u32[]{:S(2)}) async-start(bf16[32,16,128]{2,1,0:T(8,128)(2,1)} %bitcast.1), calls=%async_computation | async-start | bytes 262144 | tf_op jit(solution)/shard_map/all_to_all | solution.py:23
  11.7 1.4 collective-permute-start
  14.5 3.7 %all-to-all-done = bf16[32,16,128]{2,1,0:T(8,128)(2,1)S(1)} async-done(((bf16[32,16,128]{2,1,0:T(8,128)(2,1)}), bf16[32,16,128]{2,1,0:T(8,128)(2,1)S(1)}, u32[]{:S(2)}, u32[]{:S(2)}) %all-to-all-start) | async-done | bytes 131104 | tf_op jit(solution)/shard_map/all_to_all | solution.py:23
  19.0 5.0 %collective-permute-done.1 = bf16[128,1536]{1,0:T(8,128)(2,1)S(1)} collective-permute-done((bf16[128,1536]{1,0:T(8,128)(2,1)S(1)}, bf16[128,1536]{1,0:T(8,128)(2,1)S(1)}, u32[]{:S(2)}, u32[]{:S(2)}) %collective-permute-start.1) | collective-permute-done | bytes 393248 | tf_op jit(solution)/shard_map/ppermute | solution.py:37
  24.0 2.5 %collective-permute-start.3 = (bf16[128,768]{1,0:T(8,128)(2,1)S(1)}, bf16[128,768]{1,0:T(8,128)(2,1)S(1)}, u32[]{:S(2)}, u32[]{:S(2)}) collective-permute-start(bf16[128,768]{1,0:T(8,128)(2,1)S(1)} %slice.86), channel_id=1, source_target_pairs={{0,24},{8,0},{16,8},{24,16},{1,25},{9,1},{17,9},{25,17},{2,26},{10... | collective-permute-start | bytes 589832 | tf_op jit(solution)/shard_map/ppermute | solution.py:37
  26.9 2.8 %collective-permute-done.3 = bf16[128,768]{1,0:T(8,128)(2,1)S(1)} collective-permute-done((bf16[128,768]{1,0:T(8,128)(2,1)S(1)}, bf16[128,768]{1,0:T(8,128)(2,1)S(1)}, u32[]{:S(2)}, u32[]{:S(2)}) %collective-permute-start.3) | collective-permute-done | bytes 196640 | tf_op jit(solution)/shard_map/ppermute | solution.py:37
  29.9 3.0 %collective-permute-done.2 = bf16[128,768]{1,0:T(8,128)(2,1)S(1)} collective-permute-done((bf16[128,768]{1,0:T(8,128)(2,1)S(1)}, bf16[128,768]{1,0:T(8,128)(2,1)S(1)}, u32[]{:S(2)}, u32[]{:S(2)}) %collective-permute-start.2) | collective-permute-done | bytes 196640 | tf_op jit(solution)/shard_map/ppermute | solution.py:37
  34.2 8.2 %all-to-all-start.1 = ((bf16[8,16,1538]{2,1,0:T(8,128)(2,1)}), bf16[8,16,1538]{2,1,0:T(8,128)(2,1)S(1)}, u32[]{:S(2)}, u32[]{:S(2)}) async-start(bf16[8,16,1538]{2,1,0:T(8,128)(2,1)} %concatenate.28), calls=%async_computation.1 | async-start | bytes 851968 | tf_op jit(solution)/shard_map/all_to_all | solution.py:23
  44.1 11.0 %all-to-all-done.1 = bf16[8,16,1538]{2,1,0:T(8,128)(2,1)S(1)} async-done(((bf16[8,16,1538]{2,1,0:T(8,128)(2,1)}), bf16[8,16,1538]{2,1,0:T(8,128)(2,1)S(1)}, u32[]{:S(2)}, u32[]{:S(2)}) %all-to-all-start.1) | async-done | bytes 393760 | tf_op jit(solution)/shard_map/all_to_all | solution.py:23
  55.9 2.6 %multiply_add_fusion = f32[16,2,128,256]{3,2,1,0:T(8,128)S(1)} fusion(f32[16,2,128,256]{3,2,1,0:T(8,128)} %param.15, f32[16,2,256]{2,1,0:T(2,128)S(1)} %reshape.172, f32[16,2,128]{2,1,0:T(2,128)S(1)} %copy.59, f32[2]{0:T(128)S(1)} %exponential_subtract_fusion), kind=kLoop, calls=%fused_computation | loop fusion | flops 3145728 | bytes 8437768 | tf_op jit(solution)/shard_map/add | solution.py:199
  58.5 2.0 %copy-done = f32[16,2,128,256]{3,2,1,0:T(8,128)} copy-done((f32[16,2,128,256]{3,2,1,0:T(8,128)}, f32[16,2,128,256]{3,2,1,0:T(8,128)S(1)}, u32[]{:S(2)}) %copy-start) | copy-done | bytes 4194328
  60.5 2.1 %fusion.8 = f32[16,2,1,256]{3,2,1,0:T(1,128)S(1)} fusion(f32[16,2,128,256]{3,2,1,0:T(8,128)S(1)} %multiply_add_fusion, f32[16,2,128,1]{2,0,1,3:T(8,128)S(1)} %maximum_bitcast_fusion), kind=kOutput, calls=%fused_computation.36 | convolution fusion | flops 12582912 | bytes 4243456 | tf_op jit(solution)/shard_map/bhk,bhkv->bhv/dot_general | solution.py:205
  63.6 3.4 %all-to-all-start.2 = ((bf16[8,16,512]{2,1,0:T(8,128)(2,1)}), bf16[8,16,512]{2,1,0:T(8,128)(2,1)S(1)}, u32[]{:S(2)}, u32[]{:S(2)}) async-start(bf16[8,16,512]{2,1,0:T(8,128)(2,1)} %broadcast_in_dim.10), calls=%async_computation.2 | async-start | bytes 262144 | tf_op jit(solution)/shard_map/all_to_all | solution.py:23
  67.1 7.8 %all-to-all-done.2 = bf16[8,16,512]{2,1,0:T(8,128)(2,1)S(1)} async-done(((bf16[8,16,512]{2,1,0:T(8,128)(2,1)}), bf16[8,16,512]{2,1,0:T(8,128)(2,1)S(1)}, u32[]{:S(2)}, u32[]{:S(2)}) %all-to-all-start.2) | async-done | bytes 131104 | tf_op jit(solution)/shard_map/all_to_all | solution.py:23
  75.7 8.0 %all-to-all-start.3 = ((bf16[8,16,512]{2,1,0:T(8,128)(2,1)}), bf16[8,16,512]{2,1,0:T(8,128)(2,1)S(1)}, u32[]{:S(2)}, u32[]{:S(2)}) async-start(bf16[8,16,512]{2,1,0:T(8,128)(2,1)} %bitcast.14), calls=%async_computation.3 | async-start | bytes 262144 | tf_op jit(solution)/shard_map/all_to_all | solution.py:23
  85.2 3.8 %all-to-all-done.3 = bf16[8,16,512]{2,1,0:T(8,128)(2,1)S(1)} async-done(((bf16[8,16,512]{2,1,0:T(8,128)(2,1)}), bf16[8,16,512]{2,1,0:T(8,128)(2,1)S(1)}, u32[]{:S(2)}, u32[]{:S(2)}) %all-to-all-start.3) | async-done | bytes 131104 | tf_op jit(solution)/shard_map/all_to_all | solution.py:23
  89.0 3.6 %all-to-all-start.5 = ((bf16[8,256,128]{2,1,0:T(8,128)(2,1)}), bf16[8,256,128]{2,1,0:T(8,128)(2,1)S(1)}, u32[]{:S(2)}, u32[]{:S(2)}) async-start(bf16[8,256,128]{2,1,0:T(8,128)(2,1)} %bitcast.17), calls=%async_computation.5 | async-start | bytes 1048576 | tf_op jit(solution)/shard_map/all_to_all | solution.py:23
  92.7 17.8 %all-to-all-done.5.w0_ref = bf16[8,256,128]{2,1,0:T(8,128)(2,1)S(1)} async-done(((bf16[8,256,128]{2,1,0:T(8,128)(2,1)}), bf16[8,256,128]{2,1,0:T(8,128)(2,1)S(1)}, u32[]{:S(2)}, u32[]{:S(2)}) %all-to-all-start.5) | async-done | bytes 524320 | tf_op jit(solution)/shard_map/all_to_all | solution.py:23
  111.4 3.9 %all-to-all-start.4 = ((bf16[32,16,512]{2,1,0:T(8,128)(2,1)}), bf16[32,16,512]{2,1,0:T(8,128)(2,1)S(1)}, u32[]{:S(2)}, u32[]{:S(2)}) async-start(bf16[32,16,512]{2,1,0:T(8,128)(2,1)} %broadcast_in_dim.11), calls=%async_computation.4 | async-start | bytes 1048576 | tf_op jit(solution)/shard_map/all_to_all | solution.py:23
  115.6 2.7 %collective-permute-start.8 = (bf16[8,256,128]{2,1,0:T(8,128)(2,1)S(1)}, bf16[8,256,128]{2,1,0:T(8,128)(2,1)S(1)}, u32[]{:S(2)}, u32[]{:S(2)}) collective-permute-start(bf16[8,256,128]{2,1,0:T(8,128)(2,1)S(1)} %all-to-all-done.5.w0_ref), channel_id=1, source_target_pairs={{0,24},{8,0},{16,8},{24,16},{1,25},{9,1},{17,9},{25,17},{2,26},{10... | collective-permute-start | bytes 1572872 | tf_op jit(solution)/shard_map/ppermute | solution.py:37
  118.3 13.7 %all-to-all-done.4 = bf16[32,16,512]{2,1,0:T(8,128)(2,1)S(1)} async-done(((bf16[32,16,512]{2,1,0:T(8,128)(2,1)}), bf16[32,16,512]{2,1,0:T(8,128)(2,1)S(1)}, u32[]{:S(2)}, u32[]{:S(2)}) %all-to-all-start.4) | async-done | bytes 524320 | tf_op jit(solution)/shard_map/all_to_all | solution.py:23
  131.9 2.1 %collective-permute-start.7 = (bf16[8,64,512]{2,1,0:T(8,128)(2,1)S(1)}, bf16[8,64,512]{2,1,0:T(8,128)(2,1)S(1)}, u32[]{:S(2)}, u32[]{:S(2)}) collective-permute-start(bf16[8,64,512]{2,1,0:T(8,128)(2,1)S(1)} %bitcast.57), channel_id=1, source_target_pairs={{0,1},{1,0},{2,3},{3,2},{4,5},{5,4},{6,7},{7,6},{8,9},{9,8},{10,11... | collective-permute-start | bytes 1572872 | tf_op jit(solution)/shard_map/ppermute | solution.py:41
  134.3 2.7 %collective-permute-start.11 = (bf16[4,256,128]{2,1,0:T(8,128)(2,1)S(1)}, bf16[4,256,128]{2,1,0:T(8,128)(2,1)}, u32[]{:S(2)}, u32[]{:S(2)}) collective-permute-start(bf16[4,256,128]{2,1,0:T(8,128)(2,1)S(1)} %slice.98), channel_id=1, source_target_pairs={{0,24},{8,0},{16,8},{24,16},{1,25},{9,1},{17,9},{25,17},{2,26},{10... | collective-permute-start | bytes 786440 | tf_op jit(solution)/shard_map/ppermute | solution.py:37
  137.0 6.3 %collective-permute-done.10.w2a_ref = bf16[4,256,128]{2,1,0:T(8,128)(2,1)S(1)} collective-permute-done((bf16[4,256,128]{2,1,0:T(8,128)(2,1)S(1)}, bf16[4,256,128]{2,1,0:T(8,128)(2,1)S(1)}, u32[]{:S(2)}, u32[]{:S(2)}) %collective-permute-start.10) | collective-permute-done | bytes 262176 | tf_op jit(solution)/shard_map/ppermute | solution.py:37
  144.7 3.8 %hidden.1 = bf16[8,128,256]{2,1,0:T(8,128)(2,1)} custom-call(bf16[8,64,512]{2,1,0:T(8,128)(2,1)} %bitcast.58, bf16[8,64,512]{2,1,0:T(8,128)(2,1)} %copy-done.8, bf16[8,256,128]{2,1,0:T(8,128)(2,1)} %copy-done.1, bf16[8,256,128]{2,1,0:T(8,128)(2,1)} %copy-done.5, bf16[4,256,128]{2,1,0:T(8,128)(2,1)} %copy-done.11, ...), custom_call_target="tpu_custom_call" | custom-call | tf_op jit(solution)/shard_map/hidden/pallas_call | solution.py:227
  148.5 3.5 %all-to-all-start.6 = ((bf16[8,128,256]{2,1,0:T(8,128)(2,1)}), bf16[8,128,256]{2,1,0:T(8,128)(2,1)S(1)}, u32[]{:S(2)}, u32[]{:S(2)}) async-start(bf16[8,128,256]{2,1,0:T(8,128)(2,1)} %hidden.1), calls=%async_computation.6 | async-start | bytes 1048576 | tf_op jit(solution)/shard_map/all_to_all | solution.py:23
  152.1 2.7 %collective-permute-start.12 = (bf16[2048,128]{1,0:T(8,128)(2,1)S(1)}, bf16[2048,128]{1,0:T(8,128)(2,1)S(1)}, u32[]{:S(2)}, u32[]{:S(2)}) collective-permute-start(bf16[2048,128]{1,0:T(8,128)(2,1)S(1)} %copy-done.10), channel_id=1, source_target_pairs={{0,24},{8,0},{16,8},{24,16},{1,25},{9,1},{17,9},{25,17},{2,26},{10... | collective-permute-start | bytes 1572872 | tf_op jit(solution)/shard_map/ppermute | solution.py:37
  154.8 11.1 %collective-permute-done.13.w3_ref = bf16[2048,128]{1,0:T(8,128)(2,1)S(1)} collective-permute-done((bf16[2048,128]{1,0:T(8,128)(2,1)S(1)}, bf16[2048,128]{1,0:T(8,128)(2,1)S(1)}, u32[]{:S(2)}, u32[]{:S(2)}) %collective-permute-start.13) | collective-permute-done | bytes 524320 | tf_op jit(solution)/shard_map/ppermute | solution.py:37
  166.1 2.7 %collective-permute-start.15 = (bf16[1024,128]{1,0:T(8,128)(2,1)S(1)}, bf16[1024,128]{1,0:T(8,128)(2,1)S(1)}, u32[]{:S(2)}, u32[]{:S(2)}) collective-permute-start(bf16[1024,128]{1,0:T(8,128)(2,1)S(1)} %slice.100), channel_id=1, source_target_pairs={{0,24},{8,0},{16,8},{24,16},{1,25},{9,1},{17,9},{25,17},{2,26},{10... | collective-permute-start | bytes 786440 | tf_op jit(solution)/shard_map/ppermute | solution.py:37
  168.8 4.6 %collective-permute-done.14.w2a_ref = bf16[1024,128]{1,0:T(8,128)(2,1)S(1)} collective-permute-done((bf16[1024,128]{1,0:T(8,128)(2,1)S(1)}, bf16[1024,128]{1,0:T(8,128)(2,1)S(1)}, u32[]{:S(2)}, u32[]{:S(2)}) %collective-permute-start.14) | collective-permute-done | bytes 262176 | tf_op jit(solution)/shard_map/ppermute | solution.py:37
  174.9 3.9 %down.1 = bf16[4,8,16,128]{3,2,1,0:T(8,128)(2,1)} custom-call(bf16[8,128,256]{2,1,0:T(8,128)(2,1)} %copy-done.3, bf16[16,512]{1,0:T(8,128)(2,1)} %copy-done.14, bf16[2048,128]{1,0:T(8,128)(2,1)} %w0_ref.1, bf16[2048,128]{1,0:T(8,128)(2,1)} %copy-done.7, bf16[1024,128]{1,0:T(8,128)(2,1)} %copy-done.12, bf16[1024,128]{1,0:T(8,128)(2,1)} %copy-done.13, ...), custom_call_target="tpu_custom_call" | custom-call | tf_op jit(solution)/shard_map/down/pallas_call | solution.py:240
  178.9 16.4 %all_to_all.40 = bf16[32,16,128]{2,1,0:T(8,128)(2,1)S(1)} all-to-all(bf16[32,16,128]{2,1,0:T(8,128)(2,1)} %bitcast.63), channel_id=1, replica_groups=mesh['z'=8,'y'=4,'x'=4,'c'=2] {'y','x','c'}, dimensions={0} | all-to-all | bytes 262144 | tf_op jit(solution)/shard_map/all_to_all | solution.py:23
  (107 shorter events, 17.5 us)
Async XLA Ops:
  2.0 16.2 %all-to-all-start = ((bf16[32,16,128]{2,1,0:T(8,128)(2,1)}), bf16[32,16,128]{2,1,0:T(8,128)(2,1)S(1)}, u32[]{:S(2)}, u32[]{:S(2)}) async-start(bf16[32,16,128]{2,1,0:T(8,128)(2,1)} %bitcast.1), calls=%async_computation | async-start | bytes 262144 | tf_op jit(solution)/shard_map/all_to_all | solution.py:23
  11.7 14.8 %collective-permute-start = (bf16[128,1536]{1,0:T(8,128)(2,1)S(1)}, bf16[128,1536]{1,0:T(8,128)(2,1)S(1)}, u32[]{:S(2)}, u32[]{:S(2)}) collective-permute-start(bf16[128,1536]{1,0:T(8,128)(2,1)S(1)} %multiply_convert_fusion.1), channel_id=1, source_target_pairs={{0,8},{8,16},{16,24},{24,0},{1,9},{9,17},{17,25},{25,1},{2,10},{10... | collective-permute-start | bytes 1179656 | tf_op jit(solution)/shard_map/ppermute | solution.py:37
  13.2 10.8 %collective-permute-start.1 = (bf16[128,1536]{1,0:T(8,128)(2,1)S(1)}, bf16[128,1536]{1,0:T(8,128)(2,1)S(1)}, u32[]{:S(2)}, u32[]{:S(2)}) collective-permute-start(bf16[128,1536]{1,0:T(8,128)(2,1)S(1)} %multiply_convert_fusion.1), channel_id=1, source_target_pairs={{0,24},{8,0},{16,8},{24,16},{1,25},{9,1},{17,9},{25,17},{2,26},{10... | collective-permute-start | bytes 1179656 | tf_op jit(solution)/shard_map/ppermute | solution.py:37
  19.0 23.4 %copy-start.15 = (bf16[512,128]{1,0:T(8,128)(2,1)S(1)}, bf16[512,128]{1,0:T(8,128)(2,1)}, u32[]{:S(2)}) copy-start(bf16[512,128]{1,0:T(8,128)(2,1)} %param.22) | copy-start | bytes 393220
  19.0 25.0 %copy-start.18 = (s32[16]{0:T(128)S(1)}, s32[16]{0:T(128)}, u32[]{:S(2)}) copy-start(s32[16]{0:T(128)} %param.14) | copy-start | bytes 196
  24.0 5.7 %collective-permute-start.3 = (bf16[128,768]{1,0:T(8,128)(2,1)S(1)}, bf16[128,768]{1,0:T(8,128)(2,1)S(1)}, u32[]{:S(2)}, u32[]{:S(2)}) collective-permute-start(bf16[128,768]{1,0:T(8,128)(2,1)S(1)} %slice.86), channel_id=1, source_target_pairs={{0,24},{8,0},{16,8},{24,16},{1,25},{9,1},{17,9},{25,17},{2,26},{10... | collective-permute-start | bytes 589832 | tf_op jit(solution)/shard_map/ppermute | solution.py:37
  26.5 6.4 %collective-permute-start.2 = (bf16[128,768]{1,0:T(8,128)(2,1)S(1)}, bf16[128,768]{1,0:T(8,128)(2,1)S(1)}, u32[]{:S(2)}, u32[]{:S(2)}) collective-permute-start(bf16[128,768]{1,0:T(8,128)(2,1)S(1)} %slice.85), channel_id=1, source_target_pairs={{0,8},{8,16},{16,24},{24,0},{1,9},{9,17},{17,25},{25,1},{2,10},{10... | collective-permute-start | bytes 589832 | tf_op jit(solution)/shard_map/ppermute | solution.py:37
  34.2 20.9 %all-to-all-start.1 = ((bf16[8,16,1538]{2,1,0:T(8,128)(2,1)}), bf16[8,16,1538]{2,1,0:T(8,128)(2,1)S(1)}, u32[]{:S(2)}, u32[]{:S(2)}) async-start(bf16[8,16,1538]{2,1,0:T(8,128)(2,1)} %concatenate.28), calls=%async_computation.1 | async-start | bytes 851968 | tf_op jit(solution)/shard_map/all_to_all | solution.py:23
  42.4 24.5 %collective-permute-start.4 = (bf16[512,128]{1,0:T(8,128)(2,1)S(1)}, bf16[512,128]{1,0:T(8,128)(2,1)S(1)}, u32[]{:S(2)}, u32[]{:S(2)}) collective-permute-start(bf16[512,128]{1,0:T(8,128)(2,1)S(1)} %copy-done.15), channel_id=1, source_target_pairs={{0,24},{8,0},{16,8},{24,16},{1,25},{9,1},{17,9},{25,17},{2,26},{10... | collective-permute-start | bytes 393224 | tf_op jit(solution)/shard_map/ppermute | solution.py:37
  42.9 24.1 %collective-permute-start.5 = (bf16[512,128]{1,0:T(8,128)(2,1)S(1)}, bf16[512,128]{1,0:T(8,128)(2,1)S(1)}, u32[]{:S(2)}, u32[]{:S(2)}) collective-permute-start(bf16[512,128]{1,0:T(8,128)(2,1)S(1)} %copy-done.15), channel_id=1, source_target_pairs={{0,16},{8,24},{16,0},{24,8},{1,17},{9,25},{17,1},{25,9},{2,18},{10... | collective-permute-start | bytes 393224 | tf_op jit(solution)/shard_map/ppermute | solution.py:37
  43.4 23.6 %collective-permute-start.6 = (bf16[512,128]{1,0:T(8,128)(2,1)S(1)}, bf16[512,128]{1,0:T(8,128)(2,1)S(1)}, u32[]{:S(2)}, u32[]{:S(2)}) collective-permute-start(bf16[512,128]{1,0:T(8,128)(2,1)S(1)} %copy-done.15), channel_id=1, source_target_pairs={{0,8},{8,16},{16,24},{24,0},{1,9},{9,17},{17,25},{25,1},{2,10},{10... | collective-permute-start | bytes 393224 | tf_op jit(solution)/shard_map/ppermute | solution.py:37
  60.5 23.3 %copy-start.9 = (bf16[128,2048]{1,0:T(8,128)(2,1)S(1)}, bf16[128,2048]{1,0:T(8,128)(2,1)}, u32[]{:S(2)}) copy-start(bf16[128,2048]{1,0:T(8,128)(2,1)} %param.24) | copy-start | bytes 1572868
  60.5 23.3 %copy-start.17 = (f32[128]{0:T(128)S(1)}, f32[128]{0:T(128)}, u32[]{:S(2)}) copy-start(f32[128]{0:T(128)} %param.23) | copy-start | bytes 1540
  63.6 11.3 %all-to-all-start.2 = ((bf16[8,16,512]{2,1,0:T(8,128)(2,1)}), bf16[8,16,512]{2,1,0:T(8,128)(2,1)S(1)}, u32[]{:S(2)}, u32[]{:S(2)}) async-start(bf16[8,16,512]{2,1,0:T(8,128)(2,1)} %broadcast_in_dim.10), calls=%async_computation.2 | async-start | bytes 262144 | tf_op jit(solution)/shard_map/all_to_all | solution.py:23
  75.7 13.3 %all-to-all-start.3 = ((bf16[8,16,512]{2,1,0:T(8,128)(2,1)}), bf16[8,16,512]{2,1,0:T(8,128)(2,1)S(1)}, u32[]{:S(2)}, u32[]{:S(2)}) async-start(bf16[8,16,512]{2,1,0:T(8,128)(2,1)} %bitcast.14), calls=%async_computation.3 | async-start | bytes 262144 | tf_op jit(solution)/shard_map/all_to_all | solution.py:23
  89.0 63.0 %copy-start.10 = (bf16[2048,128]{1,0:T(8,128)(2,1)S(1)}, bf16[2048,128]{1,0:T(8,128)(2,1)}, u32[]{:S(2)}) copy-start(bf16[2048,128]{1,0:T(8,128)(2,1)} %w0_ref.1) | copy-start | bytes 1572868
  89.0 21.5 %all-to-all-start.5 = ((bf16[8,256,128]{2,1,0:T(8,128)(2,1)}), bf16[8,256,128]{2,1,0:T(8,128)(2,1)S(1)}, u32[]{:S(2)}, u32[]{:S(2)}) async-start(bf16[8,256,128]{2,1,0:T(8,128)(2,1)} %bitcast.17), calls=%async_computation.5 | async-start | bytes 1048576 | tf_op jit(solution)/shard_map/all_to_all | solution.py:23
  92.7 73.4 %copy-start.14 = (bf16[16,512]{1,0:T(8,128)(2,1)}, bf16[16,512]{1,0:T(8,128)(2,1)S(1)}, u32[]{:S(2)}) copy-start(bf16[16,512]{1,0:T(8,128)(2,1)S(1)} %fusion.3.resid_ref) | copy-start | bytes 49156
  110.5 32.7 %copy-start.1 = (bf16[8,256,128]{2,1,0:T(8,128)(2,1)}, bf16[8,256,128]{2,1,0:T(8,128)(2,1)S(1)}, u32[]{:S(2)}) copy-start(bf16[8,256,128]{2,1,0:T(8,128)(2,1)S(1)} %all-to-all-done.5.w0_ref) | copy-start | bytes 1572868
  111.4 20.5 %all-to-all-start.4 = ((bf16[32,16,512]{2,1,0:T(8,128)(2,1)}), bf16[32,16,512]{2,1,0:T(8,128)(2,1)S(1)}, u32[]{:S(2)}, u32[]{:S(2)}) async-start(bf16[32,16,512]{2,1,0:T(8,128)(2,1)} %broadcast_in_dim.11), calls=%async_computation.4 | async-start | bytes 1048576 | tf_op jit(solution)/shard_map/all_to_all | solution.py:23
  115.3 18.7 %collective-permute-start.9 = (bf16[8,256,128]{2,1,0:T(8,128)(2,1)S(1)}, bf16[8,256,128]{2,1,0:T(8,128)(2,1)S(1)}, u32[]{:S(2)}, u32[]{:S(2)}) collective-permute-start(bf16[8,256,128]{2,1,0:T(8,128)(2,1)S(1)} %all-to-all-done.5.w0_ref), channel_id=1, source_target_pairs={{0,8},{8,16},{16,24},{24,0},{1,9},{9,17},{17,25},{25,1},{2,10},{10... | collective-permute-start | bytes 1572872 | tf_op jit(solution)/shard_map/ppermute | solution.py:37
  115.6 18.6 %collective-permute-start.8 = (bf16[8,256,128]{2,1,0:T(8,128)(2,1)S(1)}, bf16[8,256,128]{2,1,0:T(8,128)(2,1)S(1)}, u32[]{:S(2)}, u32[]{:S(2)}) collective-permute-start(bf16[8,256,128]{2,1,0:T(8,128)(2,1)S(1)} %all-to-all-done.5.w0_ref), channel_id=1, source_target_pairs={{0,24},{8,0},{16,8},{24,16},{1,25},{9,1},{17,9},{25,17},{2,26},{10... | collective-permute-start | bytes 1572872 | tf_op jit(solution)/shard_map/ppermute | solution.py:37
  131.9 11.3 %copy-start.2 = (bf16[32,16,512]{2,1,0:T(8,128)(2,1)}, bf16[32,16,512]{2,1,0:T(8,128)(2,1)S(1)}, u32[]{:S(2)}) copy-start(bf16[32,16,512]{2,1,0:T(8,128)(2,1)S(1)} %all-to-all-done.4) | copy-start | bytes 1572868
  131.9 11.3 %collective-permute-start.7 = (bf16[8,64,512]{2,1,0:T(8,128)(2,1)S(1)}, bf16[8,64,512]{2,1,0:T(8,128)(2,1)S(1)}, u32[]{:S(2)}, u32[]{:S(2)}) collective-permute-start(bf16[8,64,512]{2,1,0:T(8,128)(2,1)S(1)} %bitcast.57), channel_id=1, source_target_pairs={{0,1},{1,0},{2,3},{3,2},{4,5},{5,4},{6,7},{7,6},{8,9},{9,8},{10,11... | collective-permute-start | bytes 1572872 | tf_op jit(solution)/shard_map/ppermute | solution.py:41
  134.1 9.2 %copy-start.4 = (bf16[8,256,128]{2,1,0:T(8,128)(2,1)}, bf16[8,256,128]{2,1,0:T(8,128)(2,1)S(1)}, u32[]{:S(2)}) copy-start(bf16[8,256,128]{2,1,0:T(8,128)(2,1)S(1)} %collective-permute-done.9.w3_ref) | copy-start | bytes 1572868
  134.1 9.1 %collective-permute-start.10 = (bf16[4,256,128]{2,1,0:T(8,128)(2,1)S(1)}, bf16[4,256,128]{2,1,0:T(8,128)(2,1)S(1)}, u32[]{:S(2)}, u32[]{:S(2)}) collective-permute-start(bf16[4,256,128]{2,1,0:T(8,128)(2,1)S(1)} %slice.97), channel_id=1, source_target_pairs={{0,8},{8,16},{16,24},{24,0},{1,9},{9,17},{17,25},{25,1},{2,10},{10... | collective-permute-start | bytes 786440 | tf_op jit(solution)/shard_map/ppermute | solution.py:37
  134.3 9.0 %collective-permute-start.11 = (bf16[4,256,128]{2,1,0:T(8,128)(2,1)S(1)}, bf16[4,256,128]{2,1,0:T(8,128)(2,1)}, u32[]{:S(2)}, u32[]{:S(2)}) collective-permute-start(bf16[4,256,128]{2,1,0:T(8,128)(2,1)S(1)} %slice.98), channel_id=1, source_target_pairs={{0,24},{8,0},{16,8},{24,16},{1,25},{9,1},{17,9},{25,17},{2,26},{10... | collective-permute-start | bytes 786440 | tf_op jit(solution)/shard_map/ppermute | solution.py:37
  148.5 24.9 %all-to-all-start.6 = ((bf16[8,128,256]{2,1,0:T(8,128)(2,1)}), bf16[8,128,256]{2,1,0:T(8,128)(2,1)S(1)}, u32[]{:S(2)}, u32[]{:S(2)}) async-start(bf16[8,128,256]{2,1,0:T(8,128)(2,1)} %hidden.1), calls=%async_computation.6 | async-start | bytes 1048576 | tf_op jit(solution)/shard_map/all_to_all | solution.py:23
  152.0 13.9 %collective-permute-start.13 = (bf16[2048,128]{1,0:T(8,128)(2,1)S(1)}, bf16[2048,128]{1,0:T(8,128)(2,1)S(1)}, u32[]{:S(2)}, u32[]{:S(2)}) collective-permute-start(bf16[2048,128]{1,0:T(8,128)(2,1)S(1)} %copy-done.10), channel_id=1, source_target_pairs={{0,8},{8,16},{16,24},{24,0},{1,9},{9,17},{17,25},{25,1},{2,10},{10... | collective-permute-start | bytes 1572872 | tf_op jit(solution)/shard_map/ppermute | solution.py:37
  152.1 13.9 %collective-permute-start.12 = (bf16[2048,128]{1,0:T(8,128)(2,1)S(1)}, bf16[2048,128]{1,0:T(8,128)(2,1)S(1)}, u32[]{:S(2)}, u32[]{:S(2)}) collective-permute-start(bf16[2048,128]{1,0:T(8,128)(2,1)S(1)} %copy-done.10), channel_id=1, source_target_pairs={{0,24},{8,0},{16,8},{24,16},{1,25},{9,1},{17,9},{25,17},{2,26},{10... | collective-permute-start | bytes 1572872 | tf_op jit(solution)/shard_map/ppermute | solution.py:37
  165.9 7.4 %collective-permute-start.14 = (bf16[1024,128]{1,0:T(8,128)(2,1)S(1)}, bf16[1024,128]{1,0:T(8,128)(2,1)S(1)}, u32[]{:S(2)}, u32[]{:S(2)}) collective-permute-start(bf16[1024,128]{1,0:T(8,128)(2,1)S(1)} %slice.99), channel_id=1, source_target_pairs={{0,8},{8,16},{16,24},{24,0},{1,9},{9,17},{17,25},{25,1},{2,10},{10... | collective-permute-start | bytes 786440 | tf_op jit(solution)/shard_map/ppermute | solution.py:37
  166.1 7.3 %collective-permute-start.15 = (bf16[1024,128]{1,0:T(8,128)(2,1)S(1)}, bf16[1024,128]{1,0:T(8,128)(2,1)S(1)}, u32[]{:S(2)}, u32[]{:S(2)}) collective-permute-start(bf16[1024,128]{1,0:T(8,128)(2,1)S(1)} %slice.100), channel_id=1, source_target_pairs={{0,24},{8,0},{16,8},{24,16},{1,25},{9,1},{17,9},{25,17},{2,26},{10... | collective-permute-start | bytes 786440 | tf_op jit(solution)/shard_map/ppermute | solution.py:37
  (10 other events, 32.0 us)

commit v4 on v3

--- a/solution.py
+++ b/solution.py
@@ -64,12 +64,13 @@
 
 
 def hidden_kernel(own_ref, other_ref, w0_ref, w1_ref, w2a_ref, w2b_ref, w3_ref, out_ref, x_ref, w_ref, x_sem, w_sem):
-    me = lax.axis_index("c")
+    me, my_z = (lax.axis_index("c"), lax.axis_index("z"))
     copies = []
     for z in range(NZ):
+        at = lax.rem(my_z + NZ - z, NZ)
         parts = [
-            pltpu.make_async_copy(own_ref.at[z], x_ref.at[z, me], x_sem.at[z, 0]),
-            pltpu.make_async_copy(other_ref.at[z], x_ref.at[z, 1 - me], x_sem.at[z, 1]),
+            pltpu.make_async_copy(own_ref.at[at], x_ref.at[z, me], x_sem.at[z, 0]),
+            pltpu.make_async_copy(other_ref.at[at], x_ref.at[z, 1 - me], x_sem.at[z, 1]),
         ]
         far = w2a_ref.at[z] if z < NZ // 2 else w2b_ref.at[z - NZ // 2]
         for r, ref in enumerate([w0_ref.at[z], w1_ref.at[z], far, w3_ref.at[z]]):
@@ -160,7 +161,18 @@
 
     scaled = (hidden_weight.astype(jnp.float32) * norm_mlp_gain[:, None]).astype(jnp.bfloat16)
     scaled = scaled.reshape(128, NZ, 2, 128).transpose(1, 2, 0, 3).reshape(NZ, 256, 128)
-    mixer = exchanged(scaled, "z")
+    z = lax.axis_index("z")
+    mixer = [lax.dynamic_index_in_dim(scaled, z, 0, keepdims=False)]
+    for s in range(1, NZ):
+        block = lax.dynamic_index_in_dim(scaled, (z + s) % NZ, 0, keepdims=False)
+        mixer.append(shifted(block, "z", s))
+    mixer = jnp.stack(mixer)
+
+    heads_dev = 2
+    head_ids = (lax.axis_index(TP) * heads_dev + jnp.arange(heads_dev, dtype=jnp.int32)).astype(
+        jnp.float32
+    )
+    decayed = lax.optimization_barrier(head_decay(head_ids)[None, :, None, None] * state)
 
     def term(left, right):
         return jnp.dot(left, right, preferred_element_type=jnp.float32)
@@ -189,14 +201,9 @@
     out_wide = lax.optimization_barrier(out_wide)
 
     local_rows = query.shape[0]
-    heads_dev = 2
     turned_query = rotate(query.reshape(local_rows, heads_dev, DK), seq_pos)
     turned_keys = rotate(keys.reshape(local_rows, heads_dev, DK), seq_pos) * DK ** (-0.5)
-    head_ids = (lax.axis_index(TP) * heads_dev + jnp.arange(heads_dev, dtype=jnp.int32)).astype(
-        jnp.float32
-    )
-    decay = head_decay(head_ids)
-    new_state = decay[None, :, None, None] * state + jnp.einsum(
+    new_state = decayed + jnp.einsum(
         "bhk,bhv->bhkv",
         turned_keys,
         values.reshape(local_rows, heads_dev, DV),

time: 197 us -> 188 us (0.954)
  waiting for transfers between devices: 90.5 us -> 57.7 us
  starting transfers between devices: 59.5 us -> 76.1 us
  other arithmetic: 5.76 us -> 11.6 us
    all_to_all x7 -> x6, waiting for transfers between devices: 57.7 us -> 25.5 us  [exchanged(): return lax.all_to_all(blocks, axis, split_axis=0, concat_axis=0, tiled=True)]
    ppermute x15 -> x22, starting transfers between devices: 18.2 us -> 37.5 us  [shifted(): lax.ppermute(array, axis, [(i, (i + by) % size) for i in range(size)])]
    mul x0 -> x1, other arithmetic: none -> 4.81 us  [local(): head_decay(head_ids)[None, :, None, None] * state]
    all_to_all x7 -> x6, starting transfers between devices: 39.2 us -> 35.4 us  [exchanged(): return lax.all_to_all(blocks, axis, split_axis=0, concat_axis=0, tiled=True)]
    unnamed x39 -> x47, local copies, waits for them, and re-layouts: 5.05 us -> 6.05 us
    ppermute x15 -> x22, waiting for transfers between devices: 32.8 us -> 32.2 us  [shifted(): lax.ppermute(array, axis, [(i, (i + by) % size) for i in range(size)])]
  transfers between devices with their start and end apart: 23 -> 29, of which waited for: 12 -> 9; matrix products, arithmetic and copies ran while one was open for 5% -> 11% of each run, Pallas kernels for 0% -> 0%
where the time goes in v4:
time: 188 us; the launch traced here: 187 us
  starting transfers between devices  76.1 us (40%)
  waiting for transfers between devices  57.7 us (31%)
  blocking collectives  16.4 us (9%)
  local copies, waits for them, and re-layouts  11.7 us (6%)
  other arithmetic  11.6 us (6%)
  Pallas kernels  7.67 us (4%)
  matrix products  4.11 us (2%)
    ppermute x22, starting transfers between devices, shifted(): lax.ppermute(array, axis, [(i, (i + by) % size) for i in range(size)])  37.5 us
    all_to_all x6, starting transfers between devices, exchanged(): return lax.all_to_all(blocks, axis, split_axis=0, concat_axis=0, tiled=True)  35.4 us
    ppermute x22, waiting for transfers between devices, shifted(): lax.ppermute(array, axis, [(i, (i + by) % size) for i in range(size)])  32.2 us
    all_to_all x6, waiting for transfers between devices, exchanged(): return lax.all_to_all(blocks, axis, split_axis=0, concat_axis=0, tiled=True)  25.5 us
    all_to_all x1, blocking collectives, exchanged(): return lax.all_to_all(blocks, axis, split_axis=0, concat_axis=0, tiled=True)  16.4 us
    unnamed x47, local copies, waits for them, and re-layouts  6.05 us
    mul x1, other arithmetic, local(): head_decay(head_ids)[None, :, None, None] * state  4.81 us
    pallas_call x1, Pallas kernels, local(): pl.pallas_call(down_kernel, out_shape=jax.ShapeDtypeStruct((NY, NX * NC,...  3.91 us
  transfers between devices with their start and end apart: 29, of which 9 were waited for; matrix products, arithmetic and copies ran while one was open for 11% of the time, Pallas kernels for 0%

profile of v4, /device:TPU:1, one launch (start us, length us, event | category | flops | bytes accessed | tf_op | source)
XLA Modules:
  0.0 186.6 jit_solution(4245036614489031945)
XLA Ops:
  1.8 2.2 %collective-permute-start = (bf16[128,1536]{1,0:T(8,128)(2,1)S(1)}, bf16[128,1536]{1,0:T(8,128)(2,1)S(1)}, u32[]{:S(2)}, u32[]{:S(2)}) collective-permute-start(bf16[128,1536]{1,0:T(8,128)(2,1)S(1)} %multiply_convert_fusion.1), channel_id=1, source_target_pairs={{0,8},{8,16},{16,24},{24,0},{1,9},{9,17},{17,25},{25,1},{2,10},{10... | collective-permute-start | bytes 1179656 | tf_op jit(solution)/shard_map/ppermute | solution.py:37
  5.5 2.6 %collective-permute-start.5 = (bf16[512,128]{1,0:T(8,128)(2,1)}, bf16[512,128]{1,0:T(8,128)(2,1)S(1)}, u32[]{:S(2)}, u32[]{:S(2)}) collective-permute-start(bf16[512,128]{1,0:T(8,128)(2,1)} %param.22), channel_id=1, source_target_pairs={{0,16},{8,24},{16,0},{24,8},{1,17},{9,25},{17,1},{25,9},{2,18},{10... | collective-permute-start | bytes 393224 | tf_op jit(solution)/shard_map/ppermute | solution.py:37
  10.5 7.5 %all-to-all-start = ((bf16[32,16,128]{2,1,0:T(8,128)(2,1)}), bf16[32,16,128]{2,1,0:T(8,128)(2,1)S(1)}, u32[]{:S(2)}, u32[]{:S(2)}) async-start(bf16[32,16,128]{2,1,0:T(8,128)(2,1)} %bitcast.1), calls=%async_computation | async-start | bytes 262144 | tf_op jit(solution)/shard_map/all_to_all | solution.py:23
  20.7 5.0 %all-to-all-done = bf16[32,16,128]{2,1,0:T(8,128)(2,1)S(1)} async-done(((bf16[32,16,128]{2,1,0:T(8,128)(2,1)}), bf16[32,16,128]{2,1,0:T(8,128)(2,1)S(1)}, u32[]{:S(2)}, u32[]{:S(2)}) %all-to-all-start) | async-done | bytes 131104 | tf_op jit(solution)/shard_map/all_to_all | solution.py:23
  29.4 4.6 %collective-permute-done.3 = bf16[128,768]{1,0:T(8,128)(2,1)S(1)} collective-permute-done((bf16[128,768]{1,0:T(8,128)(2,1)S(1)}, bf16[128,768]{1,0:T(8,128)(2,1)S(1)}, u32[]{:S(2)}, u32[]{:S(2)}) %collective-permute-start.3) | collective-permute-done | bytes 196640 | tf_op jit(solution)/shard_map/ppermute | solution.py:37
  34.6 5.6 %collective-permute-done.2 = bf16[128,768]{1,0:T(8,128)(2,1)S(1)} collective-permute-done((bf16[128,768]{1,0:T(8,128)(2,1)S(1)}, bf16[128,768]{1,0:T(8,128)(2,1)S(1)}, u32[]{:S(2)}, u32[]{:S(2)}) %collective-permute-start.2) | collective-permute-done | bytes 196640 | tf_op jit(solution)/shard_map/ppermute | solution.py:37
  40.1 3.0 %collective-permute-start.9 = (bf16[256,128]{1,0:T(8,128)(2,1)S(1)}, bf16[256,128]{1,0:T(8,128)(2,1)S(1)}, u32[]{:S(2)}, u32[]{:S(2)}) collective-permute-start(bf16[256,128]{1,0:T(8,128)(2,1)S(1)} %copy-done.17), channel_id=1, source_target_pairs={{0,64},{32,96},{64,128},{96,160},{128,192},{160,224},{192,0},{224,... | collective-permute-start | bytes 196616 | tf_op jit(solution)/shard_map/ppermute | solution.py:37
  44.4 5.5 %all-to-all-start.1 = ((bf16[8,16,1538]{2,1,0:T(8,128)(2,1)}), bf16[8,16,1538]{2,1,0:T(8,128)(2,1)S(1)}, u32[]{:S(2)}, u32[]{:S(2)}) async-start(bf16[8,16,1538]{2,1,0:T(8,128)(2,1)} %concatenate.28), calls=%async_computation.1 | async-start | bytes 851968 | tf_op jit(solution)/shard_map/all_to_all | solution.py:23
  49.9 4.8 %broadcast_multiply_fusion = f32[16,2,128,256]{3,2,1,0:T(8,128)} fusion(f32[16,2,128,256]{3,2,1,0:T(8,128)} %param.15, f32[2]{0:T(128)S(1)} %exponential_subtract_fusion), kind=kLoop, calls=%fused_computation.5 | loop fusion | flops 1048576 | bytes 8388616 | tf_op jit(solution)/shard_map/mul | solution.py:175
  54.9 3.5 %collective-permute-start.10 = (bf16[256,128]{1,0:T(8,128)(2,1)S(1)}, bf16[256,128]{1,0:T(8,128)(2,1)S(1)}, u32[]{:S(2)}, u32[]{:S(2)}) collective-permute-start(bf16[256,128]{1,0:T(8,128)(2,1)S(1)} %copy-done.16), channel_id=1, source_target_pairs={{0,96},{32,128},{64,160},{96,192},{128,224},{160,0},{192,32},{224,... | collective-permute-start | bytes 196616 | tf_op jit(solution)/shard_map/ppermute | solution.py:37
  59.3 2.7 %all-to-all-done.1 = bf16[8,16,1538]{2,1,0:T(8,128)(2,1)S(1)} async-done(((bf16[8,16,1538]{2,1,0:T(8,128)(2,1)}), bf16[8,16,1538]{2,1,0:T(8,128)(2,1)S(1)}, u32[]{:S(2)}, u32[]{:S(2)}) %all-to-all-start.1) | async-done | bytes 393760 | tf_op jit(solution)/shard_map/all_to_all | solution.py:23
  62.7 2.6 %multiply_add_fusion = f32[16,2,128,256]{3,2,1,0:T(8,128)S(1)} fusion(f32[16,2,128,256]{3,2,1,0:T(8,128)} %broadcast_multiply_fusion, f32[16,2,256]{2,1,0:T(2,128)S(1)} %reshape.172, f32[16,2,128]{2,1,0:T(2,128)S(1)} %copy.59), kind=kLoop, calls=%fused_computation | loop fusion | flops 2097152 | bytes 8437760 | tf_op jit(solution)/shard_map/add | solution.py:206
  67.3 2.1 %fusion.8 = f32[16,2,1,256]{3,2,1,0:T(1,128)S(1)} fusion(f32[16,2,128,256]{3,2,1,0:T(8,128)S(1)} %multiply_add_fusion, f32[16,2,128,1]{2,0,1,3:T(8,128)S(1)} %maximum_bitcast_fusion), kind=kOutput, calls=%fused_computation.52 | convolution fusion | flops 12582912 | bytes 4243456 | tf_op jit(solution)/shard_map/bhk,bhkv->bhv/dot_general | solution.py:212
  70.4 3.4 %all-to-all-start.2 = ((bf16[8,16,512]{2,1,0:T(8,128)(2,1)}), bf16[8,16,512]{2,1,0:T(8,128)(2,1)S(1)}, u32[]{:S(2)}, u32[]{:S(2)}) async-start(bf16[8,16,512]{2,1,0:T(8,128)(2,1)} %broadcast_in_dim.10), calls=%async_computation.2 | async-start | bytes 262144 | tf_op jit(solution)/shard_map/all_to_all | solution.py:23
  73.8 5.4 %collective-permute-start.11 = (bf16[256,128]{1,0:T(8,128)(2,1)S(1)}, bf16[256,128]{1,0:T(8,128)(2,1)S(1)}, u32[]{:S(2)}, u32[]{:S(2)}) collective-permute-start(bf16[256,128]{1,0:T(8,128)(2,1)S(1)} %copy-done.15), channel_id=1, source_target_pairs={{0,128},{32,160},{64,192},{96,224},{128,0},{160,32},{192,64},{224,... | collective-permute-start | bytes 196616 | tf_op jit(solution)/shard_map/ppermute | solution.py:37
  79.6 2.4 %collective-permute-start.13 = (bf16[256,128]{1,0:T(8,128)(2,1)S(1)}, bf16[256,128]{1,0:T(8,128)(2,1)S(1)}, u32[]{:S(2)}, u32[]{:S(2)}) collective-permute-start(bf16[256,128]{1,0:T(8,128)(2,1)S(1)} %get-tuple-element.7), channel_id=1, source_target_pairs={{0,192},{32,224},{64,0},{96,32},{128,64},{160,96},{192,128},{224,1... | collective-permute-start | bytes 196616 | tf_op jit(solution)/shard_map/ppermute | solution.py:37
  84.1 11.2 %all-to-all-start.3 = ((bf16[8,16,512]{2,1,0:T(8,128)(2,1)}), bf16[8,16,512]{2,1,0:T(8,128)(2,1)S(1)}, u32[]{:S(2)}, u32[]{:S(2)}) async-start(bf16[8,16,512]{2,1,0:T(8,128)(2,1)} %bitcast.14), calls=%async_computation.3 | async-start | bytes 262144 | tf_op jit(solution)/shard_map/all_to_all | solution.py:23
  95.3 5.2 %all-to-all-done.3 = bf16[8,16,512]{2,1,0:T(8,128)(2,1)S(1)} async-done(((bf16[8,16,512]{2,1,0:T(8,128)(2,1)}), bf16[8,16,512]{2,1,0:T(8,128)(2,1)S(1)}, u32[]{:S(2)}, u32[]{:S(2)}) %all-to-all-start.3) | async-done | bytes 131104 | tf_op jit(solution)/shard_map/all_to_all | solution.py:23
  101.5 4.3 %all-to-all-start.4 = ((bf16[32,16,512]{2,1,0:T(8,128)(2,1)}), bf16[32,16,512]{2,1,0:T(8,128)(2,1)S(1)}, u32[]{:S(2)}, u32[]{:S(2)}) async-start(bf16[32,16,512]{2,1,0:T(8,128)(2,1)} %broadcast_in_dim.11), calls=%async_computation.4 | async-start | bytes 1048576 | tf_op jit(solution)/shard_map/all_to_all | solution.py:23
  106.1 2.7 %collective-permute-start.15 = (bf16[8,256,128]{2,1,0:T(8,128)(2,1)S(1)}, bf16[8,256,128]{2,1,0:T(8,128)(2,1)S(1)}, u32[]{:S(2)}, u32[]{:S(2)}) collective-permute-start(bf16[8,256,128]{2,1,0:T(8,128)(2,1)S(1)} %bitcast_dynamic-update-slice_fusion.w0_ref), channel_id=1, source_target_pairs={{0,24},{8,0},{16,8},{24,16},{1,25},{9,1},{17,9},{25,17},{2,26},{10... | collective-permute-start | bytes 1572872 | tf_op jit(solution)/shard_map/ppermute | solution.py:37
  108.7 12.6 %all-to-all-done.4 = bf16[32,16,512]{2,1,0:T(8,128)(2,1)S(1)} async-done(((bf16[32,16,512]{2,1,0:T(8,128)(2,1)}), bf16[32,16,512]{2,1,0:T(8,128)(2,1)S(1)}, u32[]{:S(2)}, u32[]{:S(2)}) %all-to-all-start.4) | async-done | bytes 524320 | tf_op jit(solution)/shard_map/all_to_all | solution.py:23
  121.3 3.2 %collective-permute-start.7 = (bf16[8,64,512]{2,1,0:T(8,128)(2,1)S(1)}, bf16[8,64,512]{2,1,0:T(8,128)(2,1)S(1)}, u32[]{:S(2)}, u32[]{:S(2)}) collective-permute-start(bf16[8,64,512]{2,1,0:T(8,128)(2,1)S(1)} %bitcast.85), channel_id=1, source_target_pairs={{0,1},{1,0},{2,3},{3,2},{4,5},{5,4},{6,7},{7,6},{8,9},{9,8},{10,11... | collective-permute-start | bytes 1572872 | tf_op jit(solution)/shard_map/ppermute | solution.py:41
  124.7 2.7 %collective-permute-start.18 = (bf16[4,256,128]{2,1,0:T(8,128)(2,1)S(1)}, bf16[4,256,128]{2,1,0:T(8,128)(2,1)}, u32[]{:S(2)}, u32[]{:S(2)}) collective-permute-start(bf16[4,256,128]{2,1,0:T(8,128)(2,1)S(1)} %slice.98), channel_id=1, source_target_pairs={{0,24},{8,0},{16,8},{24,16},{1,25},{9,1},{17,9},{25,17},{2,26},{10... | collective-permute-start | bytes 786440 | tf_op jit(solution)/shard_map/ppermute | solution.py:37
  127.4 6.3 %collective-permute-done.17.w2a_ref = bf16[4,256,128]{2,1,0:T(8,128)(2,1)S(1)} collective-permute-done((bf16[4,256,128]{2,1,0:T(8,128)(2,1)S(1)}, bf16[4,256,128]{2,1,0:T(8,128)(2,1)S(1)}, u32[]{:S(2)}, u32[]{:S(2)}) %collective-permute-start.17) | collective-permute-done | bytes 262176 | tf_op jit(solution)/shard_map/ppermute | solution.py:37
  135.2 3.8 %hidden.1 = bf16[8,128,256]{2,1,0:T(8,128)(2,1)} custom-call(bf16[8,64,512]{2,1,0:T(8,128)(2,1)} %bitcast.86, bf16[8,64,512]{2,1,0:T(8,128)(2,1)} %copy-done.8, bf16[8,256,128]{2,1,0:T(8,128)(2,1)} %copy-done.7, bf16[8,256,128]{2,1,0:T(8,128)(2,1)} %copy-done.4, bf16[4,256,128]{2,1,0:T(8,128)(2,1)} %copy-done.10, ...), custom_call_target="tpu_custom_call" | custom-call | tf_op jit(solution)/shard_map/hidden/pallas_call | solution.py:234
  139.0 3.5 %all-to-all-start.5 = ((bf16[8,128,256]{2,1,0:T(8,128)(2,1)}), bf16[8,128,256]{2,1,0:T(8,128)(2,1)S(1)}, u32[]{:S(2)}, u32[]{:S(2)}) async-start(bf16[8,128,256]{2,1,0:T(8,128)(2,1)} %hidden.1), calls=%async_computation.5 | async-start | bytes 1048576 | tf_op jit(solution)/shard_map/all_to_all | solution.py:23
  142.8 2.7 %collective-permute-start.19 = (bf16[2048,128]{1,0:T(8,128)(2,1)S(1)}, bf16[2048,128]{1,0:T(8,128)(2,1)S(1)}, u32[]{:S(2)}, u32[]{:S(2)}) collective-permute-start(bf16[2048,128]{1,0:T(8,128)(2,1)S(1)} %copy-done.9), channel_id=1, source_target_pairs={{0,24},{8,0},{16,8},{24,16},{1,25},{9,1},{17,9},{25,17},{2,26},{10... | collective-permute-start | bytes 1572872 | tf_op jit(solution)/shard_map/ppermute | solution.py:37
  145.5 11.1 %collective-permute-done.20.w3_ref = bf16[2048,128]{1,0:T(8,128)(2,1)S(1)} collective-permute-done((bf16[2048,128]{1,0:T(8,128)(2,1)S(1)}, bf16[2048,128]{1,0:T(8,128)(2,1)S(1)}, u32[]{:S(2)}, u32[]{:S(2)}) %collective-permute-start.20) | collective-permute-done | bytes 524320 | tf_op jit(solution)/shard_map/ppermute | solution.py:37
  156.8 2.7 %collective-permute-start.22 = (bf16[1024,128]{1,0:T(8,128)(2,1)S(1)}, bf16[1024,128]{1,0:T(8,128)(2,1)S(1)}, u32[]{:S(2)}, u32[]{:S(2)}) collective-permute-start(bf16[1024,128]{1,0:T(8,128)(2,1)S(1)} %slice.100), channel_id=1, source_target_pairs={{0,24},{8,0},{16,8},{24,16},{1,25},{9,1},{17,9},{25,17},{2,26},{10... | collective-permute-start | bytes 786440 | tf_op jit(solution)/shard_map/ppermute | solution.py:37
  159.5 4.6 %collective-permute-done.21.w2a_ref = bf16[1024,128]{1,0:T(8,128)(2,1)S(1)} collective-permute-done((bf16[1024,128]{1,0:T(8,128)(2,1)S(1)}, bf16[1024,128]{1,0:T(8,128)(2,1)S(1)}, u32[]{:S(2)}, u32[]{:S(2)}) %collective-permute-start.21) | collective-permute-done | bytes 262176 | tf_op jit(solution)/shard_map/ppermute | solution.py:37
  165.7 3.9 %down.1 = bf16[4,8,16,128]{3,2,1,0:T(8,128)(2,1)} custom-call(bf16[8,128,256]{2,1,0:T(8,128)(2,1)} %copy-done.2, bf16[16,512]{1,0:T(8,128)(2,1)} %copy-done.13, bf16[2048,128]{1,0:T(8,128)(2,1)} %w0_ref.1, bf16[2048,128]{1,0:T(8,128)(2,1)} %copy-done.6, bf16[1024,128]{1,0:T(8,128)(2,1)} %copy-done.11, bf16[1024,128]{1,0:T(8,128)(2,1)} %copy-done.12, ...), custom_call_target="tpu_custom_call" | custom-call | tf_op jit(solution)/shard_map/down/pallas_call | solution.py:247
  169.6 16.4 %all_to_all.35 = bf16[32,16,128]{2,1,0:T(8,128)(2,1)S(1)} all-to-all(bf16[32,16,128]{2,1,0:T(8,128)(2,1)} %bitcast.92), channel_id=1, replica_groups=mesh['z'=8,'y'=4,'x'=4,'c'=2] {'y','x','c'}, dimensions={0} | all-to-all | bytes 262144 | tf_op jit(solution)/shard_map/all_to_all | solution.py:23
  (130 shorter events, 25.7 us)
Async XLA Ops:
  1.8 26.4 %collective-permute-start = (bf16[128,1536]{1,0:T(8,128)(2,1)S(1)}, bf16[128,1536]{1,0:T(8,128)(2,1)S(1)}, u32[]{:S(2)}, u32[]{:S(2)}) collective-permute-start(bf16[128,1536]{1,0:T(8,128)(2,1)S(1)} %multiply_convert_fusion.1), channel_id=1, source_target_pairs={{0,8},{8,16},{16,24},{24,0},{1,9},{9,17},{17,25},{25,1},{2,10},{10... | collective-permute-start | bytes 1179656 | tf_op jit(solution)/shard_map/ppermute | solution.py:37
  4.0 22.4 %collective-permute-start.1 = (bf16[128,1536]{1,0:T(8,128)(2,1)S(1)}, bf16[128,1536]{1,0:T(8,128)(2,1)S(1)}, u32[]{:S(2)}, u32[]{:S(2)}) collective-permute-start(bf16[128,1536]{1,0:T(8,128)(2,1)S(1)} %multiply_convert_fusion.1), channel_id=1, source_target_pairs={{0,24},{8,0},{16,8},{24,16},{1,25},{9,1},{17,9},{25,17},{2,26},{10... | collective-permute-start | bytes 1179656 | tf_op jit(solution)/shard_map/ppermute | solution.py:37
  5.5 73.7 %collective-permute-start.6 = (bf16[512,128]{1,0:T(8,128)(2,1)}, bf16[512,128]{1,0:T(8,128)(2,1)S(1)}, u32[]{:S(2)}, u32[]{:S(2)}) collective-permute-start(bf16[512,128]{1,0:T(8,128)(2,1)} %param.22), channel_id=1, source_target_pairs={{0,8},{8,16},{16,24},{24,0},{1,9},{9,17},{17,25},{25,1},{2,10},{10... | collective-permute-start | bytes 393224 | tf_op jit(solution)/shard_map/ppermute | solution.py:37
  5.5 74.1 %collective-permute-start.5 = (bf16[512,128]{1,0:T(8,128)(2,1)}, bf16[512,128]{1,0:T(8,128)(2,1)S(1)}, u32[]{:S(2)}, u32[]{:S(2)}) collective-permute-start(bf16[512,128]{1,0:T(8,128)(2,1)} %param.22), channel_id=1, source_target_pairs={{0,16},{8,24},{16,0},{24,8},{1,17},{9,25},{17,1},{25,9},{2,18},{10... | collective-permute-start | bytes 393224 | tf_op jit(solution)/shard_map/ppermute | solution.py:37
  8.0 73.9 %collective-permute-start.4 = (bf16[512,128]{1,0:T(8,128)(2,1)}, bf16[512,128]{1,0:T(8,128)(2,1)S(1)}, u32[]{:S(2)}, u32[]{:S(2)}) collective-permute-start(bf16[512,128]{1,0:T(8,128)(2,1)} %param.22), channel_id=1, source_target_pairs={{0,24},{8,0},{16,8},{24,16},{1,25},{9,1},{17,9},{25,17},{2,26},{10... | collective-permute-start | bytes 393224 | tf_op jit(solution)/shard_map/ppermute | solution.py:37
  10.5 15.1 %all-to-all-start = ((bf16[32,16,128]{2,1,0:T(8,128)(2,1)}), bf16[32,16,128]{2,1,0:T(8,128)(2,1)S(1)}, u32[]{:S(2)}, u32[]{:S(2)}) async-start(bf16[32,16,128]{2,1,0:T(8,128)(2,1)} %bitcast.1), calls=%async_computation | async-start | bytes 262144 | tf_op jit(solution)/shard_map/all_to_all | solution.py:23
  26.4 28.5 %collective-permute-start.8 = (bf16[256,128]{1,0:T(8,128)(2,1)}, bf16[256,128]{1,0:T(8,128)(2,1)}, u32[]{:S(2)}, u32[]{:S(2)}) collective-permute-start(bf16[256,128]{1,0:T(8,128)(2,1)} %get-tuple-element.12), channel_id=1, source_target_pairs={{0,32},{32,64},{64,96},{96,128},{128,160},{160,192},{192,224},{224... | collective-permute-start | bytes 196616 | tf_op jit(solution)/shard_map/ppermute | solution.py:37
  28.2 5.8 %collective-permute-start.3 = (bf16[128,768]{1,0:T(8,128)(2,1)S(1)}, bf16[128,768]{1,0:T(8,128)(2,1)S(1)}, u32[]{:S(2)}, u32[]{:S(2)}) collective-permute-start(bf16[128,768]{1,0:T(8,128)(2,1)S(1)} %slice.86), channel_id=1, source_target_pairs={{0,24},{8,0},{16,8},{24,16},{1,25},{9,1},{17,9},{25,17},{2,26},{10... | collective-permute-start | bytes 589832 | tf_op jit(solution)/shard_map/ppermute | solution.py:37
  34.0 6.1 %collective-permute-start.2 = (bf16[128,768]{1,0:T(8,128)(2,1)S(1)}, bf16[128,768]{1,0:T(8,128)(2,1)S(1)}, u32[]{:S(2)}, u32[]{:S(2)}) collective-permute-start(bf16[128,768]{1,0:T(8,128)(2,1)S(1)} %slice.85), channel_id=1, source_target_pairs={{0,8},{8,16},{16,24},{24,0},{1,9},{9,17},{17,25},{25,1},{2,10},{10... | collective-permute-start | bytes 589832 | tf_op jit(solution)/shard_map/ppermute | solution.py:37
  40.1 33.7 %collective-permute-start.9 = (bf16[256,128]{1,0:T(8,128)(2,1)S(1)}, bf16[256,128]{1,0:T(8,128)(2,1)S(1)}, u32[]{:S(2)}, u32[]{:S(2)}) collective-permute-start(bf16[256,128]{1,0:T(8,128)(2,1)S(1)} %copy-done.17), channel_id=1, source_target_pairs={{0,64},{32,96},{64,128},{96,160},{128,192},{160,224},{192,0},{224,... | collective-permute-start | bytes 196616 | tf_op jit(solution)/shard_map/ppermute | solution.py:37
  44.4 17.5 %all-to-all-start.1 = ((bf16[8,16,1538]{2,1,0:T(8,128)(2,1)}), bf16[8,16,1538]{2,1,0:T(8,128)(2,1)S(1)}, u32[]{:S(2)}, u32[]{:S(2)}) async-start(bf16[8,16,1538]{2,1,0:T(8,128)(2,1)} %concatenate.28), calls=%async_computation.1 | async-start | bytes 851968 | tf_op jit(solution)/shard_map/all_to_all | solution.py:23
  54.9 40.4 %collective-permute-start.10 = (bf16[256,128]{1,0:T(8,128)(2,1)S(1)}, bf16[256,128]{1,0:T(8,128)(2,1)S(1)}, u32[]{:S(2)}, u32[]{:S(2)}) collective-permute-start(bf16[256,128]{1,0:T(8,128)(2,1)S(1)} %copy-done.16), channel_id=1, source_target_pairs={{0,96},{32,128},{64,160},{96,192},{128,224},{160,0},{192,32},{224,... | collective-permute-start | bytes 196616 | tf_op jit(solution)/shard_map/ppermute | solution.py:37
  70.4 12.8 %all-to-all-start.2 = ((bf16[8,16,512]{2,1,0:T(8,128)(2,1)}), bf16[8,16,512]{2,1,0:T(8,128)(2,1)S(1)}, u32[]{:S(2)}, u32[]{:S(2)}) async-start(bf16[8,16,512]{2,1,0:T(8,128)(2,1)} %broadcast_in_dim.10), calls=%async_computation.2 | async-start | bytes 262144 | tf_op jit(solution)/shard_map/all_to_all | solution.py:23
  73.8 32.0 %collective-permute-start.11 = (bf16[256,128]{1,0:T(8,128)(2,1)S(1)}, bf16[256,128]{1,0:T(8,128)(2,1)S(1)}, u32[]{:S(2)}, u32[]{:S(2)}) collective-permute-start(bf16[256,128]{1,0:T(8,128)(2,1)S(1)} %copy-done.15), channel_id=1, source_target_pairs={{0,128},{32,160},{64,192},{96,224},{128,0},{160,32},{192,64},{224,... | collective-permute-start | bytes 196616 | tf_op jit(solution)/shard_map/ppermute | solution.py:37
  79.2 26.7 %collective-permute-start.12 = (bf16[256,128]{1,0:T(8,128)(2,1)S(1)}, bf16[256,128]{1,0:T(8,128)(2,1)S(1)}, u32[]{:S(2)}, u32[]{:S(2)}) collective-permute-start(bf16[256,128]{1,0:T(8,128)(2,1)S(1)} %get-tuple-element.8), channel_id=1, source_target_pairs={{0,160},{32,192},{64,224},{96,0},{128,32},{160,64},{192,96},{224,1... | collective-permute-start | bytes 196616 | tf_op jit(solution)/shard_map/ppermute | solution.py:37
  79.6 26.3 %collective-permute-start.13 = (bf16[256,128]{1,0:T(8,128)(2,1)S(1)}, bf16[256,128]{1,0:T(8,128)(2,1)S(1)}, u32[]{:S(2)}, u32[]{:S(2)}) collective-permute-start(bf16[256,128]{1,0:T(8,128)(2,1)S(1)} %get-tuple-element.7), channel_id=1, source_target_pairs={{0,192},{32,224},{64,0},{96,32},{128,64},{160,96},{192,128},{224,1... | collective-permute-start | bytes 196616 | tf_op jit(solution)/shard_map/ppermute | solution.py:37
  82.0 23.9 %collective-permute-start.14 = (bf16[256,128]{1,0:T(8,128)(2,1)S(1)}, bf16[256,128]{1,0:T(8,128)(2,1)S(1)}, u32[]{:S(2)}, u32[]{:S(2)}) collective-permute-start(bf16[256,128]{1,0:T(8,128)(2,1)S(1)} %get-tuple-element.6), channel_id=1, source_target_pairs={{0,224},{32,0},{64,32},{96,64},{128,96},{160,128},{192,160},{224,1... | collective-permute-start | bytes 196616 | tf_op jit(solution)/shard_map/ppermute | solution.py:37
  84.1 58.4 %copy-start.9 = (bf16[2048,128]{1,0:T(8,128)(2,1)S(1)}, bf16[2048,128]{1,0:T(8,128)(2,1)}, u32[]{:S(2)}) copy-start(bf16[2048,128]{1,0:T(8,128)(2,1)} %w0_ref.1) | copy-start | bytes 1572868
  84.1 16.4 %all-to-all-start.3 = ((bf16[8,16,512]{2,1,0:T(8,128)(2,1)}), bf16[8,16,512]{2,1,0:T(8,128)(2,1)S(1)}, u32[]{:S(2)}, u32[]{:S(2)}) async-start(bf16[8,16,512]{2,1,0:T(8,128)(2,1)} %bitcast.14), calls=%async_computation.3 | async-start | bytes 262144 | tf_op jit(solution)/shard_map/all_to_all | solution.py:23
  100.6 56.0 %copy-start.13 = (bf16[16,512]{1,0:T(8,128)(2,1)}, bf16[16,512]{1,0:T(8,128)(2,1)S(1)}, u32[]{:S(2)}) copy-start(bf16[16,512]{1,0:T(8,128)(2,1)S(1)} %fusion.3.resid_ref) | copy-start | bytes 49156
  101.5 19.8 %all-to-all-start.4 = ((bf16[32,16,512]{2,1,0:T(8,128)(2,1)}), bf16[32,16,512]{2,1,0:T(8,128)(2,1)S(1)}, u32[]{:S(2)}, u32[]{:S(2)}) async-start(bf16[32,16,512]{2,1,0:T(8,128)(2,1)} %broadcast_in_dim.11), calls=%async_computation.4 | async-start | bytes 1048576 | tf_op jit(solution)/shard_map/all_to_all | solution.py:23
  106.0 27.7 %copy-start.7 = (bf16[8,256,128]{2,1,0:T(8,128)(2,1)}, bf16[8,256,128]{2,1,0:T(8,128)(2,1)S(1)}, u32[]{:S(2)}) copy-start(bf16[8,256,128]{2,1,0:T(8,128)(2,1)S(1)} %bitcast_dynamic-update-slice_fusion.w0_ref) | copy-start | bytes 1572868
  106.0 18.6 %collective-permute-start.16 = (bf16[8,256,128]{2,1,0:T(8,128)(2,1)S(1)}, bf16[8,256,128]{2,1,0:T(8,128)(2,1)S(1)}, u32[]{:S(2)}, u32[]{:S(2)}) collective-permute-start(bf16[8,256,128]{2,1,0:T(8,128)(2,1)S(1)} %bitcast_dynamic-update-slice_fusion.w0_ref), channel_id=1, source_target_pairs={{0,8},{8,16},{16,24},{24,0},{1,9},{9,17},{17,25},{25,1},{2,10},{10... | collective-permute-start | bytes 1572872 | tf_op jit(solution)/shard_map/ppermute | solution.py:37
  106.1 18.6 %collective-permute-start.15 = (bf16[8,256,128]{2,1,0:T(8,128)(2,1)S(1)}, bf16[8,256,128]{2,1,0:T(8,128)(2,1)S(1)}, u32[]{:S(2)}, u32[]{:S(2)}) collective-permute-start(bf16[8,256,128]{2,1,0:T(8,128)(2,1)S(1)} %bitcast_dynamic-update-slice_fusion.w0_ref), channel_id=1, source_target_pairs={{0,24},{8,0},{16,8},{24,16},{1,25},{9,1},{17,9},{25,17},{2,26},{10... | collective-permute-start | bytes 1572872 | tf_op jit(solution)/shard_map/ppermute | solution.py:37
  121.3 12.3 %collective-permute-start.7 = (bf16[8,64,512]{2,1,0:T(8,128)(2,1)S(1)}, bf16[8,64,512]{2,1,0:T(8,128)(2,1)S(1)}, u32[]{:S(2)}, u32[]{:S(2)}) collective-permute-start(bf16[8,64,512]{2,1,0:T(8,128)(2,1)S(1)} %bitcast.85), channel_id=1, source_target_pairs={{0,1},{1,0},{2,3},{3,2},{4,5},{5,4},{6,7},{7,6},{8,9},{9,8},{10,11... | collective-permute-start | bytes 1572872 | tf_op jit(solution)/shard_map/ppermute | solution.py:41
  124.5 9.1 %collective-permute-start.17 = (bf16[4,256,128]{2,1,0:T(8,128)(2,1)S(1)}, bf16[4,256,128]{2,1,0:T(8,128)(2,1)S(1)}, u32[]{:S(2)}, u32[]{:S(2)}) collective-permute-start(bf16[4,256,128]{2,1,0:T(8,128)(2,1)S(1)} %slice.97), channel_id=1, source_target_pairs={{0,8},{8,16},{16,24},{24,0},{1,9},{9,17},{17,25},{25,1},{2,10},{10... | collective-permute-start | bytes 786440 | tf_op jit(solution)/shard_map/ppermute | solution.py:37
  124.7 9.0 %collective-permute-start.18 = (bf16[4,256,128]{2,1,0:T(8,128)(2,1)S(1)}, bf16[4,256,128]{2,1,0:T(8,128)(2,1)}, u32[]{:S(2)}, u32[]{:S(2)}) collective-permute-start(bf16[4,256,128]{2,1,0:T(8,128)(2,1)S(1)} %slice.98), channel_id=1, source_target_pairs={{0,24},{8,0},{16,8},{24,16},{1,25},{9,1},{17,9},{25,17},{2,26},{10... | collective-permute-start | bytes 786440 | tf_op jit(solution)/shard_map/ppermute | solution.py:37
  139.0 25.1 %all-to-all-start.5 = ((bf16[8,128,256]{2,1,0:T(8,128)(2,1)}), bf16[8,128,256]{2,1,0:T(8,128)(2,1)S(1)}, u32[]{:S(2)}, u32[]{:S(2)}) async-start(bf16[8,128,256]{2,1,0:T(8,128)(2,1)} %hidden.1), calls=%async_computation.5 | async-start | bytes 1048576 | tf_op jit(solution)/shard_map/all_to_all | solution.py:23
  142.5 14.1 %collective-permute-start.20 = (bf16[2048,128]{1,0:T(8,128)(2,1)S(1)}, bf16[2048,128]{1,0:T(8,128)(2,1)S(1)}, u32[]{:S(2)}, u32[]{:S(2)}) collective-permute-start(bf16[2048,128]{1,0:T(8,128)(2,1)S(1)} %copy-done.9), channel_id=1, source_target_pairs={{0,8},{8,16},{16,24},{24,0},{1,9},{9,17},{17,25},{25,1},{2,10},{10... | collective-permute-start | bytes 1572872 | tf_op jit(solution)/shard_map/ppermute | solution.py:37
  142.8 13.9 %collective-permute-start.19 = (bf16[2048,128]{1,0:T(8,128)(2,1)S(1)}, bf16[2048,128]{1,0:T(8,128)(2,1)S(1)}, u32[]{:S(2)}, u32[]{:S(2)}) collective-permute-start(bf16[2048,128]{1,0:T(8,128)(2,1)S(1)} %copy-done.9), channel_id=1, source_target_pairs={{0,24},{8,0},{16,8},{24,16},{1,25},{9,1},{17,9},{25,17},{2,26},{10... | collective-permute-start | bytes 1572872 | tf_op jit(solution)/shard_map/ppermute | solution.py:37
  156.6 7.4 %collective-permute-start.21 = (bf16[1024,128]{1,0:T(8,128)(2,1)S(1)}, bf16[1024,128]{1,0:T(8,128)(2,1)S(1)}, u32[]{:S(2)}, u32[]{:S(2)}) collective-permute-start(bf16[1024,128]{1,0:T(8,128)(2,1)S(1)} %slice.99), channel_id=1, source_target_pairs={{0,8},{8,16},{16,24},{24,0},{1,9},{9,17},{17,25},{25,1},{2,10},{10... | collective-permute-start | bytes 786440 | tf_op jit(solution)/shard_map/ppermute | solution.py:37
  156.8 7.3 %collective-permute-start.22 = (bf16[1024,128]{1,0:T(8,128)(2,1)S(1)}, bf16[1024,128]{1,0:T(8,128)(2,1)S(1)}, u32[]{:S(2)}, u32[]{:S(2)}) collective-permute-start(bf16[1024,128]{1,0:T(8,128)(2,1)S(1)} %slice.100), channel_id=1, source_target_pairs={{0,24},{8,0},{16,8},{24,16},{1,25},{9,1},{17,9},{25,17},{2,26},{10... | collective-permute-start | bytes 786440 | tf_op jit(solution)/shard_map/ppermute | solution.py:37
  (17 other events, 105.2 us)

commit v5 on v3

--- a/solution.py
+++ b/solution.py
@@ -195,18 +195,16 @@
     head_ids = (lax.axis_index(TP) * heads_dev + jnp.arange(heads_dev, dtype=jnp.int32)).astype(
         jnp.float32
     )
-    decay = head_decay(head_ids)
-    new_state = decay[None, :, None, None] * state + jnp.einsum(
-        "bhk,bhv->bhkv",
-        turned_keys,
-        values.reshape(local_rows, heads_dev, DV),
-        precision=lax.Precision.HIGHEST,
-    )
-    read = jnp.einsum("bhk,bhkv->bhv", turned_query, new_state, precision=lax.Precision.HIGHEST)
+    decay = head_decay(head_ids)[None, :, None]
+    values = values.reshape(local_rows, heads_dev, DV)
+    along = jnp.sum(turned_query * turned_keys, axis=-1, keepdims=True)
+    read = decay * jnp.sum(turned_query[..., None] * state, axis=2) + along * values
     read = read * lax.rsqrt(jnp.mean(read * read, axis=-1, keepdims=True) + EPS)
     mixed = (
         read.reshape(local_rows, heads_dev * DV) * head_gain[None, :] * jax.nn.silu(gates)
     ).astype(jnp.bfloat16)
+    mixed, old, left, right = lax.optimization_barrier((mixed, state, turned_keys, values))
+    new_state = decay[..., None] * old + left[..., None] * right[:, :, None, :]
     mixed_all = copy_for_each(mixed, "z").reshape(128, heads_dev * DV)
     attn_terms = term(mixed_all, out_wide).astype(jnp.bfloat16)
     attn = summed_on_arrival(attn_terms.reshape(NX * NC, 16, 512), TP)

time: 197 us -> 194 us (0.985)
  blocking collectives: 16.4 us -> 0 us
  starting transfers between devices: 59.5 us -> 69.5 us
  other arithmetic: 5.76 us -> 9.73 us
  waiting for transfers between devices: 90.5 us -> 93 us
  matrix products: 4.1 us -> 2.01 us
    all_to_all x1 -> x0, blocking collectives: 16.4 us -> none  [exchanged(): return lax.all_to_all(blocks, axis, split_axis=0, concat_axis=0, tiled=True)]
    all_to_all x7 -> x8, starting transfers between devices: 39.2 us -> 48 us  [exchanged(): return lax.all_to_all(blocks, axis, split_axis=0, concat_axis=0, tiled=True)]
    reduce_sum x0 -> x2, other arithmetic: none -> 2.77 us  [the longest x1 2.61 us: local(): jnp.sum(turned_query[..., None] * state, axis=2)]
    all_to_all x7 -> x8, waiting for transfers between devices: 57.7 us -> 60.2 us  [exchanged(): return lax.all_to_all(blocks, axis, split_axis=0, concat_axis=0, tiled=True)]
    dot_general x1 -> x0, matrix products: 2.1 us -> none  [local(): jnp.einsum('bhk,bhkv->bhv', turned_query, new_state, precision=lax.Precis...]
    unnamed x39 -> x44, local copies, waits for them, and re-layouts: 5.05 us -> 3.99 us
  transfers between devices with their start and end apart: 23 -> 24, of which waited for: 12 -> 13; matrix products, arithmetic and copies ran while one was open for 5% -> 7% of each run, Pallas kernels for 0% -> 0%
where the time goes in v5:
time: 194 us; the launch traced here: 193 us
  waiting for transfers between devices  93 us (48%)
  starting transfers between devices  69.5 us (36%)
  local copies, waits for them, and re-layouts  9.92 us (5%)
  other arithmetic  9.73 us (5%)
  Pallas kernels  7.67 us (4%)
  matrix products  2.01 us (1%)
    all_to_all x8, waiting for transfers between devices, exchanged(): return lax.all_to_all(blocks, axis, split_axis=0, concat_axis=0, tiled=True)  60.2 us
    all_to_all x8, starting transfers between devices, exchanged(): return lax.all_to_all(blocks, axis, split_axis=0, concat_axis=0, tiled=True)  48 us
    ppermute x15, waiting for transfers between devices, shifted(): lax.ppermute(array, axis, [(i, (i + by) % size) for i in range(size)])  32.8 us
    ppermute x15, starting transfers between devices, shifted(): lax.ppermute(array, axis, [(i, (i + by) % size) for i in range(size)])  19.4 us
    unnamed x44, local copies, waits for them, and re-layouts  3.99 us
    add x1, other arithmetic, local(): new_state = decay[..., None] * old + left[..., None] * right[:, :, None, :]  3.96 us
    pallas_call x1, Pallas kernels, local(): pl.pallas_call(down_kernel, out_shape=jax.ShapeDtypeStruct((NY, NX * NC,...  3.91 us
  transfers between devices with their start and end apart: 24, of which 13 were waited for; matrix products, arithmetic and copies ran while one was open for 7% of the time, Pallas kernels for 0%

profile of v5, /device:TPU:1, one launch (start us, length us, event | category | flops | bytes accessed | tf_op | source)
XLA Modules:
  0.0 193.0 jit_solution(13758141912662818424)
XLA Ops:
  2.0 8.6 %all-to-all-start = ((bf16[32,16,128]{2,1,0:T(8,128)(2,1)}), bf16[32,16,128]{2,1,0:T(8,128)(2,1)S(1)}, u32[]{:S(2)}, u32[]{:S(2)}) async-start(bf16[32,16,128]{2,1,0:T(8,128)(2,1)} %bitcast.1), calls=%async_computation | async-start | bytes 262144 | tf_op jit(solution)/shard_map/all_to_all | solution.py:23
  14.5 3.7 %all-to-all-done = bf16[32,16,128]{2,1,0:T(8,128)(2,1)S(1)} async-done(((bf16[32,16,128]{2,1,0:T(8,128)(2,1)}), bf16[32,16,128]{2,1,0:T(8,128)(2,1)S(1)}, u32[]{:S(2)}, u32[]{:S(2)}) %all-to-all-start) | async-done | bytes 131104 | tf_op jit(solution)/shard_map/all_to_all | solution.py:23
  19.0 5.0 %collective-permute-done.1 = bf16[128,1536]{1,0:T(8,128)(2,1)S(1)} collective-permute-done((bf16[128,1536]{1,0:T(8,128)(2,1)S(1)}, bf16[128,1536]{1,0:T(8,128)(2,1)S(1)}, u32[]{:S(2)}, u32[]{:S(2)}) %collective-permute-start.1) | collective-permute-done | bytes 393248 | tf_op jit(solution)/shard_map/ppermute | solution.py:37
  24.0 2.5 %collective-permute-start.3 = (bf16[128,768]{1,0:T(8,128)(2,1)S(1)}, bf16[128,768]{1,0:T(8,128)(2,1)S(1)}, u32[]{:S(2)}, u32[]{:S(2)}) collective-permute-start(bf16[128,768]{1,0:T(8,128)(2,1)S(1)} %slice.86), channel_id=1, source_target_pairs={{0,24},{8,0},{16,8},{24,16},{1,25},{9,1},{17,9},{25,17},{2,26},{10... | collective-permute-start | bytes 589832 | tf_op jit(solution)/shard_map/ppermute | solution.py:37
  26.9 2.8 %collective-permute-done.3 = bf16[128,768]{1,0:T(8,128)(2,1)S(1)} collective-permute-done((bf16[128,768]{1,0:T(8,128)(2,1)S(1)}, bf16[128,768]{1,0:T(8,128)(2,1)S(1)}, u32[]{:S(2)}, u32[]{:S(2)}) %collective-permute-start.3) | collective-permute-done | bytes 196640 | tf_op jit(solution)/shard_map/ppermute | solution.py:37
  29.9 3.0 %collective-permute-done.2 = bf16[128,768]{1,0:T(8,128)(2,1)S(1)} collective-permute-done((bf16[128,768]{1,0:T(8,128)(2,1)S(1)}, bf16[128,768]{1,0:T(8,128)(2,1)S(1)}, u32[]{:S(2)}, u32[]{:S(2)}) %collective-permute-start.2) | collective-permute-done | bytes 196640 | tf_op jit(solution)/shard_map/ppermute | solution.py:37
  34.2 8.2 %all-to-all-start.1 = ((bf16[8,16,1538]{2,1,0:T(8,128)(2,1)}), bf16[8,16,1538]{2,1,0:T(8,128)(2,1)S(1)}, u32[]{:S(2)}, u32[]{:S(2)}) async-start(bf16[8,16,1538]{2,1,0:T(8,128)(2,1)} %concatenate.28), calls=%async_computation.1 | async-start | bytes 851968 | tf_op jit(solution)/shard_map/all_to_all | solution.py:23
  42.5 1.6 collective-permute-start.5
  45.5 9.7 %all-to-all-done.1 = bf16[8,16,1538]{2,1,0:T(8,128)(2,1)S(1)} async-done(((bf16[8,16,1538]{2,1,0:T(8,128)(2,1)}), bf16[8,16,1538]{2,1,0:T(8,128)(2,1)S(1)}, u32[]{:S(2)}, u32[]{:S(2)}) %all-to-all-start.1) | async-done | bytes 393760 | tf_op jit(solution)/shard_map/all_to_all | solution.py:23
  56.0 2.6 %multiply_reduce_fusion = f32[16,2,256]{2,1,0:T(2,128)S(1)} fusion(f32[16,2,128,256]{3,2,1,0:T(8,128)} %param.15, f32[16,2,128]{2,1,0:T(2,128)S(1)} %copy.59), kind=kLoop, calls=%fused_computation.1 | loop fusion | flops 2088960 | bytes 4243456 | tf_op jit(solution)/shard_map/reduce_sum | solution.py:201
  59.8 3.4 %all-to-all-start.2 = ((bf16[8,16,512]{2,1,0:T(8,128)(2,1)}), bf16[8,16,512]{2,1,0:T(8,128)(2,1)S(1)}, u32[]{:S(2)}, u32[]{:S(2)}) async-start(bf16[8,16,512]{2,1,0:T(8,128)(2,1)} %broadcast_in_dim.10), calls=%async_computation.2 | async-start | bytes 262144 | tf_op jit(solution)/shard_map/all_to_all | solution.py:23
  63.3 7.8 %all-to-all-done.2 = bf16[8,16,512]{2,1,0:T(8,128)(2,1)S(1)} async-done(((bf16[8,16,512]{2,1,0:T(8,128)(2,1)}), bf16[8,16,512]{2,1,0:T(8,128)(2,1)S(1)}, u32[]{:S(2)}, u32[]{:S(2)}) %all-to-all-start.2) | async-done | bytes 131104 | tf_op jit(solution)/shard_map/all_to_all | solution.py:23
  71.9 8.1 %all-to-all-start.3 = ((bf16[8,16,512]{2,1,0:T(8,128)(2,1)}), bf16[8,16,512]{2,1,0:T(8,128)(2,1)S(1)}, u32[]{:S(2)}, u32[]{:S(2)}) async-start(bf16[8,16,512]{2,1,0:T(8,128)(2,1)} %bitcast.12), calls=%async_computation.3 | async-start | bytes 262144 | tf_op jit(solution)/shard_map/all_to_all | solution.py:23
  81.4 3.8 %all-to-all-done.3 = bf16[8,16,512]{2,1,0:T(8,128)(2,1)S(1)} async-done(((bf16[8,16,512]{2,1,0:T(8,128)(2,1)}), bf16[8,16,512]{2,1,0:T(8,128)(2,1)S(1)}, u32[]{:S(2)}, u32[]{:S(2)}) %all-to-all-start.3) | async-done | bytes 131104 | tf_op jit(solution)/shard_map/all_to_all | solution.py:23
  85.2 3.6 %all-to-all-start.5 = ((bf16[8,256,128]{2,1,0:T(8,128)(2,1)}), bf16[8,256,128]{2,1,0:T(8,128)(2,1)S(1)}, u32[]{:S(2)}, u32[]{:S(2)}) async-start(bf16[8,256,128]{2,1,0:T(8,128)(2,1)} %bitcast.15), calls=%async_computation.5 | async-start | bytes 1048576 | tf_op jit(solution)/shard_map/all_to_all | solution.py:23
  88.9 17.8 %all-to-all-done.5.w0_ref = bf16[8,256,128]{2,1,0:T(8,128)(2,1)S(1)} async-done(((bf16[8,256,128]{2,1,0:T(8,128)(2,1)}), bf16[8,256,128]{2,1,0:T(8,128)(2,1)S(1)}, u32[]{:S(2)}, u32[]{:S(2)}) %all-to-all-start.5) | async-done | bytes 524320 | tf_op jit(solution)/shard_map/all_to_all | solution.py:23
  107.7 3.9 %all-to-all-start.4 = ((bf16[32,16,512]{2,1,0:T(8,128)(2,1)}), bf16[32,16,512]{2,1,0:T(8,128)(2,1)S(1)}, u32[]{:S(2)}, u32[]{:S(2)}) async-start(bf16[32,16,512]{2,1,0:T(8,128)(2,1)} %broadcast_in_dim.11), calls=%async_computation.4 | async-start | bytes 1048576 | tf_op jit(solution)/shard_map/all_to_all | solution.py:23
  111.7 2.7 %collective-permute-start.8 = (bf16[8,256,128]{2,1,0:T(8,128)(2,1)S(1)}, bf16[8,256,128]{2,1,0:T(8,128)(2,1)S(1)}, u32[]{:S(2)}, u32[]{:S(2)}) collective-permute-start(bf16[8,256,128]{2,1,0:T(8,128)(2,1)S(1)} %all-to-all-done.5.w0_ref), channel_id=1, source_target_pairs={{0,24},{8,0},{16,8},{24,16},{1,25},{9,1},{17,9},{25,17},{2,26},{10... | collective-permute-start | bytes 1572872 | tf_op jit(solution)/shard_map/ppermute | solution.py:37
  114.3 13.8 %all-to-all-done.4 = bf16[32,16,512]{2,1,0:T(8,128)(2,1)S(1)} async-done(((bf16[32,16,512]{2,1,0:T(8,128)(2,1)}), bf16[32,16,512]{2,1,0:T(8,128)(2,1)S(1)}, u32[]{:S(2)}, u32[]{:S(2)}) %all-to-all-start.4) | async-done | bytes 524320 | tf_op jit(solution)/shard_map/all_to_all | solution.py:23
  128.2 2.1 %collective-permute-start.7 = (bf16[8,64,512]{2,1,0:T(8,128)(2,1)S(1)}, bf16[8,64,512]{2,1,0:T(8,128)(2,1)S(1)}, u32[]{:S(2)}, u32[]{:S(2)}) collective-permute-start(bf16[8,64,512]{2,1,0:T(8,128)(2,1)S(1)} %bitcast.56), channel_id=1, source_target_pairs={{0,1},{1,0},{2,3},{3,2},{4,5},{5,4},{6,7},{7,6},{8,9},{9,8},{10,11... | collective-permute-start | bytes 1572872 | tf_op jit(solution)/shard_map/ppermute | solution.py:41
  130.7 2.7 %collective-permute-start.11 = (bf16[4,256,128]{2,1,0:T(8,128)(2,1)S(1)}, bf16[4,256,128]{2,1,0:T(8,128)(2,1)S(1)}, u32[]{:S(2)}, u32[]{:S(2)}) collective-permute-start(bf16[4,256,128]{2,1,0:T(8,128)(2,1)S(1)} %slice.98), channel_id=1, source_target_pairs={{0,24},{8,0},{16,8},{24,16},{1,25},{9,1},{17,9},{25,17},{2,26},{10... | collective-permute-start | bytes 786440 | tf_op jit(solution)/shard_map/ppermute | solution.py:37
  133.4 6.3 %collective-permute-done.10.w2a_ref = bf16[4,256,128]{2,1,0:T(8,128)(2,1)S(1)} collective-permute-done((bf16[4,256,128]{2,1,0:T(8,128)(2,1)S(1)}, bf16[4,256,128]{2,1,0:T(8,128)(2,1)S(1)}, u32[]{:S(2)}, u32[]{:S(2)}) %collective-permute-start.10) | collective-permute-done | bytes 262176 | tf_op jit(solution)/shard_map/ppermute | solution.py:37
  141.9 3.8 %hidden.1 = bf16[8,128,256]{2,1,0:T(8,128)(2,1)} custom-call(bf16[8,64,512]{2,1,0:T(8,128)(2,1)} %bitcast.57, bf16[8,64,512]{2,1,0:T(8,128)(2,1)} %copy-done.7, bf16[8,256,128]{2,1,0:T(8,128)(2,1)} %copy-done, bf16[8,256,128]{2,1,0:T(8,128)(2,1)} %copy-done.4, bf16[4,256,128]{2,1,0:T(8,128)(2,1)} %copy-done.10, bf16[4,256,128]{2,1,0:T(8,128)(2,1)} %copy-done.11, ...), custom_call_target="tpu_custom_call" | custom-call | tf_op jit(solution)/shard_map/hidden/pallas_call | solution.py:225
  145.7 3.5 %all-to-all-start.6 = ((bf16[8,128,256]{2,1,0:T(8,128)(2,1)}), bf16[8,128,256]{2,1,0:T(8,128)(2,1)S(1)}, u32[]{:S(2)}, u32[]{:S(2)}) async-start(bf16[8,128,256]{2,1,0:T(8,128)(2,1)} %hidden.1), calls=%async_computation.6 | async-start | bytes 1048576 | tf_op jit(solution)/shard_map/all_to_all | solution.py:23
  149.3 2.7 %collective-permute-start.12 = (bf16[2048,128]{1,0:T(8,128)(2,1)S(1)}, bf16[2048,128]{1,0:T(8,128)(2,1)S(1)}, u32[]{:S(2)}, u32[]{:S(2)}) collective-permute-start(bf16[2048,128]{1,0:T(8,128)(2,1)S(1)} %copy-done.9), channel_id=1, source_target_pairs={{0,24},{8,0},{16,8},{24,16},{1,25},{9,1},{17,9},{25,17},{2,26},{10... | collective-permute-start | bytes 1572872 | tf_op jit(solution)/shard_map/ppermute | solution.py:37
  151.9 11.1 %collective-permute-done.13.w3_ref = bf16[2048,128]{1,0:T(8,128)(2,1)S(1)} collective-permute-done((bf16[2048,128]{1,0:T(8,128)(2,1)S(1)}, bf16[2048,128]{1,0:T(8,128)(2,1)S(1)}, u32[]{:S(2)}, u32[]{:S(2)}) %collective-permute-start.13) | collective-permute-done | bytes 524320 | tf_op jit(solution)/shard_map/ppermute | solution.py:37
  163.2 2.7 %collective-permute-start.15 = (bf16[1024,128]{1,0:T(8,128)(2,1)S(1)}, bf16[1024,128]{1,0:T(8,128)(2,1)S(1)}, u32[]{:S(2)}, u32[]{:S(2)}) collective-permute-start(bf16[1024,128]{1,0:T(8,128)(2,1)S(1)} %slice.100), channel_id=1, source_target_pairs={{0,24},{8,0},{16,8},{24,16},{1,25},{9,1},{17,9},{25,17},{2,26},{10... | collective-permute-start | bytes 786440 | tf_op jit(solution)/shard_map/ppermute | solution.py:37
  166.0 4.5 %collective-permute-done.14.w2a_ref = bf16[1024,128]{1,0:T(8,128)(2,1)S(1)} collective-permute-done((bf16[1024,128]{1,0:T(8,128)(2,1)S(1)}, bf16[1024,128]{1,0:T(8,128)(2,1)S(1)}, u32[]{:S(2)}, u32[]{:S(2)}) %collective-permute-start.14) | collective-permute-done | bytes 262176 | tf_op jit(solution)/shard_map/ppermute | solution.py:37
  172.1 3.9 %down.1 = bf16[4,8,16,128]{3,2,1,0:T(8,128)(2,1)} custom-call(bf16[8,128,256]{2,1,0:T(8,128)(2,1)} %copy-done.2, bf16[16,512]{1,0:T(8,128)(2,1)} %copy-done.14, bf16[2048,128]{1,0:T(8,128)(2,1)} %w0_ref.1, bf16[2048,128]{1,0:T(8,128)(2,1)} %copy-done.6, bf16[1024,128]{1,0:T(8,128)(2,1)} %copy-done.12, bf16[1024,128]{1,0:T(8,128)(2,1)} %copy-done.13, ...), custom_call_target="tpu_custom_call" | custom-call | tf_op jit(solution)/shard_map/down/pallas_call | solution.py:238
  176.0 8.8 %all-to-all-start.7 = ((bf16[32,16,128]{2,1,0:T(8,128)(2,1)}), bf16[32,16,128]{2,1,0:T(8,128)(2,1)S(1)}, u32[]{:S(2)}, u32[]{:S(2)}) async-start(bf16[32,16,128]{2,1,0:T(8,128)(2,1)} %bitcast.62), calls=%async_computation.7 | async-start | bytes 262144 | tf_op jit(solution)/shard_map/all_to_all | solution.py:23
  184.8 4.0 %multiply_add_fusion = f32[16,2,128,256]{3,2,1,0:T(8,128)} fusion(f32[16,2,128,256]{3,2,1,0:T(8,128)} %param.15, f32[16,2,256]{2,1,0:T(2,128)S(1)} %reshape.188, f32[16,2,128]{2,1,0:T(2,128)S(1)} %copy.64, f32[2]{0:T(128)S(1)} %exponential_subtract_fusion), kind=kLoop, calls=%fused_computation | loop fusion | flops 3145728 | bytes 8437768 | tf_op jit(solution)/shard_map/add | solution.py:207
  188.8 3.6 %all-to-all-done.7 = bf16[32,16,128]{2,1,0:T(8,128)(2,1)S(1)} async-done(((bf16[32,16,128]{2,1,0:T(8,128)(2,1)}), bf16[32,16,128]{2,1,0:T(8,128)(2,1)S(1)}, u32[]{:S(2)}, u32[]{:S(2)}) %all-to-all-start.7) | async-done | bytes 131104 | tf_op jit(solution)/shard_map/all_to_all | solution.py:23
  (114 shorter events, 19.7 us)
Async XLA Ops:
  2.0 16.2 %all-to-all-start = ((bf16[32,16,128]{2,1,0:T(8,128)(2,1)}), bf16[32,16,128]{2,1,0:T(8,128)(2,1)S(1)}, u32[]{:S(2)}, u32[]{:S(2)}) async-start(bf16[32,16,128]{2,1,0:T(8,128)(2,1)} %bitcast.1), calls=%async_computation | async-start | bytes 262144 | tf_op jit(solution)/shard_map/all_to_all | solution.py:23
  11.7 14.8 %collective-permute-start = (bf16[128,1536]{1,0:T(8,128)(2,1)S(1)}, bf16[128,1536]{1,0:T(8,128)(2,1)S(1)}, u32[]{:S(2)}, u32[]{:S(2)}) collective-permute-start(bf16[128,1536]{1,0:T(8,128)(2,1)S(1)} %multiply_convert_fusion.1), channel_id=1, source_target_pairs={{0,8},{8,16},{16,24},{24,0},{1,9},{9,17},{17,25},{25,1},{2,10},{10... | collective-permute-start | bytes 1179656 | tf_op jit(solution)/shard_map/ppermute | solution.py:37
  13.2 10.8 %collective-permute-start.1 = (bf16[128,1536]{1,0:T(8,128)(2,1)S(1)}, bf16[128,1536]{1,0:T(8,128)(2,1)S(1)}, u32[]{:S(2)}, u32[]{:S(2)}) collective-permute-start(bf16[128,1536]{1,0:T(8,128)(2,1)S(1)} %multiply_convert_fusion.1), channel_id=1, source_target_pairs={{0,24},{8,0},{16,8},{24,16},{1,25},{9,1},{17,9},{25,17},{2,26},{10... | collective-permute-start | bytes 1179656 | tf_op jit(solution)/shard_map/ppermute | solution.py:37
  19.0 23.4 %copy-start.15 = (bf16[512,128]{1,0:T(8,128)(2,1)S(1)}, bf16[512,128]{1,0:T(8,128)(2,1)}, u32[]{:S(2)}) copy-start(bf16[512,128]{1,0:T(8,128)(2,1)} %param.22) | copy-start | bytes 393220
  19.0 26.2 %copy-start.18 = (s32[16]{0:T(128)S(1)}, s32[16]{0:T(128)}, u32[]{:S(2)}) copy-start(s32[16]{0:T(128)} %param.14) | copy-start | bytes 196
  24.0 5.7 %collective-permute-start.3 = (bf16[128,768]{1,0:T(8,128)(2,1)S(1)}, bf16[128,768]{1,0:T(8,128)(2,1)S(1)}, u32[]{:S(2)}, u32[]{:S(2)}) collective-permute-start(bf16[128,768]{1,0:T(8,128)(2,1)S(1)} %slice.86), channel_id=1, source_target_pairs={{0,24},{8,0},{16,8},{24,16},{1,25},{9,1},{17,9},{25,17},{2,26},{10... | collective-permute-start | bytes 589832 | tf_op jit(solution)/shard_map/ppermute | solution.py:37
  26.5 6.4 %collective-permute-start.2 = (bf16[128,768]{1,0:T(8,128)(2,1)S(1)}, bf16[128,768]{1,0:T(8,128)(2,1)S(1)}, u32[]{:S(2)}, u32[]{:S(2)}) collective-permute-start(bf16[128,768]{1,0:T(8,128)(2,1)S(1)} %slice.85), channel_id=1, source_target_pairs={{0,8},{8,16},{16,24},{24,0},{1,9},{9,17},{17,25},{25,1},{2,10},{10... | collective-permute-start | bytes 589832 | tf_op jit(solution)/shard_map/ppermute | solution.py:37
  33.4 25.6 %copy-start.16 = (f32[512]{0:T(512)S(1)}, f32[512]{0:T(512)}, u32[]{:S(2)}) copy-start(f32[512]{0:T(512)} %param.21) | copy-start | bytes 6148
  34.2 20.9 %all-to-all-start.1 = ((bf16[8,16,1538]{2,1,0:T(8,128)(2,1)}), bf16[8,16,1538]{2,1,0:T(8,128)(2,1)S(1)}, u32[]{:S(2)}, u32[]{:S(2)}) async-start(bf16[8,16,1538]{2,1,0:T(8,128)(2,1)} %concatenate.28), calls=%async_computation.1 | async-start | bytes 851968 | tf_op jit(solution)/shard_map/all_to_all | solution.py:23
  42.4 20.7 %collective-permute-start.6 = (bf16[512,128]{1,0:T(8,128)(2,1)S(1)}, bf16[512,128]{1,0:T(8,128)(2,1)S(1)}, u32[]{:S(2)}, u32[]{:S(2)}) collective-permute-start(bf16[512,128]{1,0:T(8,128)(2,1)S(1)} %copy-done.15), channel_id=1, source_target_pairs={{0,8},{8,16},{16,24},{24,0},{1,9},{9,17},{17,25},{25,1},{2,10},{10... | collective-permute-start | bytes 393224 | tf_op jit(solution)/shard_map/ppermute | solution.py:37
  42.5 20.6 %collective-permute-start.5 = (bf16[512,128]{1,0:T(8,128)(2,1)S(1)}, bf16[512,128]{1,0:T(8,128)(2,1)S(1)}, u32[]{:S(2)}, u32[]{:S(2)}) collective-permute-start(bf16[512,128]{1,0:T(8,128)(2,1)S(1)} %copy-done.15), channel_id=1, source_target_pairs={{0,16},{8,24},{16,0},{24,8},{1,17},{9,25},{17,1},{25,9},{2,18},{10... | collective-permute-start | bytes 393224 | tf_op jit(solution)/shard_map/ppermute | solution.py:37
  44.1 19.1 %collective-permute-start.4 = (bf16[512,128]{1,0:T(8,128)(2,1)S(1)}, bf16[512,128]{1,0:T(8,128)(2,1)S(1)}, u32[]{:S(2)}, u32[]{:S(2)}) collective-permute-start(bf16[512,128]{1,0:T(8,128)(2,1)S(1)} %copy-done.15), channel_id=1, source_target_pairs={{0,24},{8,0},{16,8},{24,16},{1,25},{9,1},{17,9},{25,17},{2,26},{10... | collective-permute-start | bytes 393224 | tf_op jit(solution)/shard_map/ppermute | solution.py:37
  45.4 34.5 %copy-start.8 = (bf16[128,2048]{1,0:T(8,128)(2,1)S(1)}, bf16[128,2048]{1,0:T(8,128)(2,1)}, u32[]{:S(2)}) copy-start(bf16[128,2048]{1,0:T(8,128)(2,1)} %param.24) | copy-start | bytes 1572868
  45.4 34.5 %copy-start.17 = (f32[128]{0:T(128)S(1)}, f32[128]{0:T(128)}, u32[]{:S(2)}) copy-start(f32[128]{0:T(128)} %param.23) | copy-start | bytes 1540
  59.8 11.3 %all-to-all-start.2 = ((bf16[8,16,512]{2,1,0:T(8,128)(2,1)}), bf16[8,16,512]{2,1,0:T(8,128)(2,1)S(1)}, u32[]{:S(2)}, u32[]{:S(2)}) async-start(bf16[8,16,512]{2,1,0:T(8,128)(2,1)} %broadcast_in_dim.10), calls=%async_computation.2 | async-start | bytes 262144 | tf_op jit(solution)/shard_map/all_to_all | solution.py:23
  71.9 13.3 %all-to-all-start.3 = ((bf16[8,16,512]{2,1,0:T(8,128)(2,1)}), bf16[8,16,512]{2,1,0:T(8,128)(2,1)S(1)}, u32[]{:S(2)}, u32[]{:S(2)}) async-start(bf16[8,16,512]{2,1,0:T(8,128)(2,1)} %bitcast.12), calls=%async_computation.3 | async-start | bytes 262144 | tf_op jit(solution)/shard_map/all_to_all | solution.py:23
  85.2 64.0 %copy-start.9 = (bf16[2048,128]{1,0:T(8,128)(2,1)S(1)}, bf16[2048,128]{1,0:T(8,128)(2,1)}, u32[]{:S(2)}) copy-start(bf16[2048,128]{1,0:T(8,128)(2,1)} %w0_ref.1) | copy-start | bytes 1572868
  85.2 21.5 %all-to-all-start.5 = ((bf16[8,256,128]{2,1,0:T(8,128)(2,1)}), bf16[8,256,128]{2,1,0:T(8,128)(2,1)S(1)}, u32[]{:S(2)}, u32[]{:S(2)}) async-start(bf16[8,256,128]{2,1,0:T(8,128)(2,1)} %bitcast.15), calls=%async_computation.5 | async-start | bytes 1048576 | tf_op jit(solution)/shard_map/all_to_all | solution.py:23
  88.9 74.3 %copy-start.14 = (bf16[16,512]{1,0:T(8,128)(2,1)}, bf16[16,512]{1,0:T(8,128)(2,1)S(1)}, u32[]{:S(2)}) copy-start(bf16[16,512]{1,0:T(8,128)(2,1)S(1)} %fusion.3.resid_ref) | copy-start | bytes 49156
  106.7 34.3 %copy-start = (bf16[8,256,128]{2,1,0:T(8,128)(2,1)}, bf16[8,256,128]{2,1,0:T(8,128)(2,1)S(1)}, u32[]{:S(2)}) copy-start(bf16[8,256,128]{2,1,0:T(8,128)(2,1)S(1)} %all-to-all-done.5.w0_ref) | copy-start | bytes 1572868
  107.7 20.5 %all-to-all-start.4 = ((bf16[32,16,512]{2,1,0:T(8,128)(2,1)}), bf16[32,16,512]{2,1,0:T(8,128)(2,1)S(1)}, u32[]{:S(2)}, u32[]{:S(2)}) async-start(bf16[32,16,512]{2,1,0:T(8,128)(2,1)} %broadcast_in_dim.11), calls=%async_computation.4 | async-start | bytes 1048576 | tf_op jit(solution)/shard_map/all_to_all | solution.py:23
  111.6 18.7 %collective-permute-start.9 = (bf16[8,256,128]{2,1,0:T(8,128)(2,1)S(1)}, bf16[8,256,128]{2,1,0:T(8,128)(2,1)S(1)}, u32[]{:S(2)}, u32[]{:S(2)}) collective-permute-start(bf16[8,256,128]{2,1,0:T(8,128)(2,1)S(1)} %all-to-all-done.5.w0_ref), channel_id=1, source_target_pairs={{0,8},{8,16},{16,24},{24,0},{1,9},{9,17},{17,25},{25,1},{2,10},{10... | collective-permute-start | bytes 1572872 | tf_op jit(solution)/shard_map/ppermute | solution.py:37
  111.7 18.9 %collective-permute-start.8 = (bf16[8,256,128]{2,1,0:T(8,128)(2,1)S(1)}, bf16[8,256,128]{2,1,0:T(8,128)(2,1)S(1)}, u32[]{:S(2)}, u32[]{:S(2)}) collective-permute-start(bf16[8,256,128]{2,1,0:T(8,128)(2,1)S(1)} %all-to-all-done.5.w0_ref), channel_id=1, source_target_pairs={{0,24},{8,0},{16,8},{24,16},{1,25},{9,1},{17,9},{25,17},{2,26},{10... | collective-permute-start | bytes 1572872 | tf_op jit(solution)/shard_map/ppermute | solution.py:37
  128.2 12.9 %collective-permute-start.7 = (bf16[8,64,512]{2,1,0:T(8,128)(2,1)S(1)}, bf16[8,64,512]{2,1,0:T(8,128)(2,1)S(1)}, u32[]{:S(2)}, u32[]{:S(2)}) collective-permute-start(bf16[8,64,512]{2,1,0:T(8,128)(2,1)S(1)} %bitcast.56), channel_id=1, source_target_pairs={{0,1},{1,0},{2,3},{3,2},{4,5},{5,4},{6,7},{7,6},{8,9},{9,8},{10,11... | collective-permute-start | bytes 1572872 | tf_op jit(solution)/shard_map/ppermute | solution.py:41
  130.3 9.3 %collective-permute-start.10 = (bf16[4,256,128]{2,1,0:T(8,128)(2,1)S(1)}, bf16[4,256,128]{2,1,0:T(8,128)(2,1)S(1)}, u32[]{:S(2)}, u32[]{:S(2)}) collective-permute-start(bf16[4,256,128]{2,1,0:T(8,128)(2,1)S(1)} %slice.97), channel_id=1, source_target_pairs={{0,8},{8,16},{16,24},{24,0},{1,9},{9,17},{17,25},{25,1},{2,10},{10... | collective-permute-start | bytes 786440 | tf_op jit(solution)/shard_map/ppermute | solution.py:37
  130.7 9.7 %collective-permute-start.11 = (bf16[4,256,128]{2,1,0:T(8,128)(2,1)S(1)}, bf16[4,256,128]{2,1,0:T(8,128)(2,1)S(1)}, u32[]{:S(2)}, u32[]{:S(2)}) collective-permute-start(bf16[4,256,128]{2,1,0:T(8,128)(2,1)S(1)} %slice.98), channel_id=1, source_target_pairs={{0,24},{8,0},{16,8},{24,16},{1,25},{9,1},{17,9},{25,17},{2,26},{10... | collective-permute-start | bytes 786440 | tf_op jit(solution)/shard_map/ppermute | solution.py:37
  145.7 24.9 %all-to-all-start.6 = ((bf16[8,128,256]{2,1,0:T(8,128)(2,1)}), bf16[8,128,256]{2,1,0:T(8,128)(2,1)S(1)}, u32[]{:S(2)}, u32[]{:S(2)}) async-start(bf16[8,128,256]{2,1,0:T(8,128)(2,1)} %hidden.1), calls=%async_computation.6 | async-start | bytes 1048576 | tf_op jit(solution)/shard_map/all_to_all | solution.py:23
  149.2 13.9 %collective-permute-start.13 = (bf16[2048,128]{1,0:T(8,128)(2,1)S(1)}, bf16[2048,128]{1,0:T(8,128)(2,1)S(1)}, u32[]{:S(2)}, u32[]{:S(2)}) collective-permute-start(bf16[2048,128]{1,0:T(8,128)(2,1)S(1)} %copy-done.9), channel_id=1, source_target_pairs={{0,8},{8,16},{16,24},{24,0},{1,9},{9,17},{17,25},{25,1},{2,10},{10... | collective-permute-start | bytes 1572872 | tf_op jit(solution)/shard_map/ppermute | solution.py:37
  149.3 13.9 %collective-permute-start.12 = (bf16[2048,128]{1,0:T(8,128)(2,1)S(1)}, bf16[2048,128]{1,0:T(8,128)(2,1)S(1)}, u32[]{:S(2)}, u32[]{:S(2)}) collective-permute-start(bf16[2048,128]{1,0:T(8,128)(2,1)S(1)} %copy-done.9), channel_id=1, source_target_pairs={{0,24},{8,0},{16,8},{24,16},{1,25},{9,1},{17,9},{25,17},{2,26},{10... | collective-permute-start | bytes 1572872 | tf_op jit(solution)/shard_map/ppermute | solution.py:37
  163.1 7.4 %collective-permute-start.14 = (bf16[1024,128]{1,0:T(8,128)(2,1)S(1)}, bf16[1024,128]{1,0:T(8,128)(2,1)S(1)}, u32[]{:S(2)}, u32[]{:S(2)}) collective-permute-start(bf16[1024,128]{1,0:T(8,128)(2,1)S(1)} %slice.99), channel_id=1, source_target_pairs={{0,8},{8,16},{16,24},{24,0},{1,9},{9,17},{17,25},{25,1},{2,10},{10... | collective-permute-start | bytes 786440 | tf_op jit(solution)/shard_map/ppermute | solution.py:37
  163.2 7.3 %collective-permute-start.15 = (bf16[1024,128]{1,0:T(8,128)(2,1)S(1)}, bf16[1024,128]{1,0:T(8,128)(2,1)S(1)}, u32[]{:S(2)}, u32[]{:S(2)}) collective-permute-start(bf16[1024,128]{1,0:T(8,128)(2,1)S(1)} %slice.100), channel_id=1, source_target_pairs={{0,24},{8,0},{16,8},{24,16},{1,25},{9,1},{17,9},{25,17},{2,26},{10... | collective-permute-start | bytes 786440 | tf_op jit(solution)/shard_map/ppermute | solution.py:37
  176.0 16.4 %all-to-all-start.7 = ((bf16[32,16,128]{2,1,0:T(8,128)(2,1)}), bf16[32,16,128]{2,1,0:T(8,128)(2,1)S(1)}, u32[]{:S(2)}, u32[]{:S(2)}) async-start(bf16[32,16,128]{2,1,0:T(8,128)(2,1)} %bitcast.62), calls=%async_computation.7 | async-start | bytes 262144 | tf_op jit(solution)/shard_map/all_to_all | solution.py:23
  (11 other events, 53.5 us)

commit v6 on v5

--- a/solution.py
+++ b/solution.py
@@ -57,23 +57,22 @@
     return 1.0 - jnp.exp2(-2.0 - 6.0 * head_ids / (H - 1))
 
 
-def far_block(low_ref, high_ref, z, size):
-    half = NZ // 2
-    ref, at = (low_ref, z) if z < half else (high_ref, z - half)
-    return ref.at[pl.ds(at * size, size)]
+STEP = 2
 
 
 def hidden_kernel(own_ref, other_ref, w0_ref, w1_ref, w2a_ref, w2b_ref, w3_ref, out_ref, x_ref, w_ref, x_sem, w_sem):
     me = lax.axis_index("c")
     copies = []
-    for z in range(NZ):
+    for k in range(NZ // STEP):
+        at = pl.ds(STEP * k, STEP)
         parts = [
-            pltpu.make_async_copy(own_ref.at[z], x_ref.at[z, me], x_sem.at[z, 0]),
-            pltpu.make_async_copy(other_ref.at[z], x_ref.at[z, 1 - me], x_sem.at[z, 1]),
+            pltpu.make_async_copy(own_ref.at[at], x_ref.at[me, at], x_sem.at[k, 0]),
+            pltpu.make_async_copy(other_ref.at[at], x_ref.at[1 - me, at], x_sem.at[k, 1]),
         ]
-        far = w2a_ref.at[z] if z < NZ // 2 else w2b_ref.at[z - NZ // 2]
-        for r, ref in enumerate([w0_ref.at[z], w1_ref.at[z], far, w3_ref.at[z]]):
-            parts.append(pltpu.make_async_copy(ref, w_ref.at[z, r], w_sem.at[z, r]))
+        half = NZ // STEP // 2
+        far = w2a_ref.at[at] if k < half else w2b_ref.at[pl.ds(STEP * (k - half), STEP)]
+        for r, ref in enumerate([w0_ref.at[at], w1_ref.at[at], far, w3_ref.at[at]]):
+            parts.append(pltpu.make_async_copy(ref, w_ref.at[r, at], w_sem.at[k, r]))
         for copy in parts:
             copy.start()
         copies.append(parts)
@@ -81,12 +80,13 @@
     hidden = jnp.zeros((2 * rows, 256), jnp.float32)
     squares = jnp.zeros((2 * rows, 1), jnp.float32)
     for z in range(NZ):
-        for copy in copies[z]:
-            copy.wait()
-        left = x_ref[z].reshape(2 * rows, 512)
+        if z % STEP == 0:
+            for copy in copies[z // STEP]:
+                copy.wait()
+        left = x_ref[:, z].reshape(2 * rows, 512)
         wide = left.astype(jnp.float32)
         squares = squares + jnp.sum(wide * wide, axis=1, keepdims=True)
-        right = [w_ref[z, :, 128 * j : 128 * (j + 1), :].reshape(512, 128) for j in range(2)]
+        right = [w_ref[:, z, 128 * j : 128 * (j + 1), :].reshape(512, 128) for j in range(2)]
         right = jnp.concatenate(right, axis=1)
         hidden = hidden + jnp.dot(left, right, preferred_element_type=jnp.float32)
     scale = lax.rsqrt(squares / D + EPS)
@@ -99,20 +99,25 @@
 def down_kernel(act_ref, resid_ref, w0_ref, w1_ref, w2a_ref, w2b_ref, w3_ref, out_ref, a_ref, w_ref, a_sem, w_sem):
     y, x, c = (lax.axis_index("y"), lax.axis_index("x"), lax.axis_index("c"))
     copies = []
-    for z in range(NZ):
-        parts = [pltpu.make_async_copy(act_ref.at[z], a_ref.at[z], a_sem.at[z])]
-        near = [ref.at[pl.ds(256 * z, 256)] for ref in (w0_ref, w1_ref, w3_ref)]
-        blocks = [near[0], near[1], far_block(w2a_ref, w2b_ref, z, 256), near[2]]
-        for r, ref in enumerate(blocks):
-            parts.append(pltpu.make_async_copy(ref, w_ref.at[z, r], w_sem.at[z, r]))
+    size = 256 * STEP
+    for k in range(NZ // STEP):
+        at = pl.ds(STEP * k, STEP)
+        parts = [pltpu.make_async_copy(act_ref.at[at], a_ref.at[at], a_sem.at[k])]
+        half = NZ // STEP // 2
+        lines = pl.ds(size * k, size)
+        far = w2a_ref.at[lines] if k < half else w2b_ref.at[pl.ds(size * (k - half), size)]
+        for r, ref in enumerate([w0_ref.at[lines], w1_ref.at[lines], far, w3_ref.at[lines]]):
+            parts.append(pltpu.make_async_copy(ref, w_ref.at[r, lines], w_sem.at[k, r]))
         for copy in parts:
             copy.start()
         copies.append(parts)
     total = jnp.zeros((128, 512), jnp.float32)
     for z in range(NZ):
-        for copy in copies[z]:
-            copy.wait()
-        right = jnp.concatenate([w_ref[z, r] for r in range(NY)], axis=1)
+        if z % STEP == 0:
+            for copy in copies[z // STEP]:
+                copy.wait()
+        right = [w_ref[r, 256 * z : 256 * (z + 1)] for r in range(NY)]
+        right = jnp.concatenate(right, axis=1)
         total = total + jnp.dot(a_ref[z], right, preferred_element_type=jnp.float32)
     resid = resid_ref[...].astype(jnp.float32)
     for cc in range(NC):
@@ -227,10 +232,10 @@
         out_shape=jax.ShapeDtypeStruct((NZ, 128, 256), jnp.bfloat16),
         in_specs=[anywhere] * 7,
         scratch_shapes=[
-            pltpu.VMEM((NZ, NC, 64, 512), jnp.bfloat16),
-            pltpu.VMEM((NZ, NY, 256, 128), jnp.bfloat16),
-            pltpu.SemaphoreType.DMA((NZ, 2)),
-            pltpu.SemaphoreType.DMA((NZ, NY)),
+            pltpu.VMEM((NC, NZ, 64, 512), jnp.bfloat16),
+            pltpu.VMEM((NY, NZ, 256, 128), jnp.bfloat16),
+            pltpu.SemaphoreType.DMA((NZ // STEP, 2)),
+            pltpu.SemaphoreType.DMA((NZ // STEP, NY)),
         ],
         name="hidden",
     )(own, other, mixer, mix_above, far_low, far_high, mix_below)
@@ -241,9 +246,9 @@
         in_specs=[anywhere, pl.BlockSpec(memory_space=pltpu.VMEM)] + [anywhere] * 5,
         scratch_shapes=[
             pltpu.VMEM((NZ, 128, 256), jnp.bfloat16),
-            pltpu.VMEM((NZ, NY, 256, 128), jnp.bfloat16),
-            pltpu.SemaphoreType.DMA((NZ,)),
-            pltpu.SemaphoreType.DMA((NZ, NY)),
+            pltpu.VMEM((NY, NZ * 256, 128), jnp.bfloat16),
+            pltpu.SemaphoreType.DMA((NZ // STEP,)),
+            pltpu.SemaphoreType.DMA((NZ // STEP, NY)),
         ],
         name="down",
     )(active, resid, down_weight, down_above, down_low, down_high, down_below)

time: 194 us -> 193 us (level)
  no operation moved by 1% of the time
where the time goes in v6:
time: 193 us; the launch traced here: 192 us
  waiting for transfers between devices  93 us (48%)
  starting transfers between devices  69.5 us (36%)
  local copies, waits for them, and re-layouts  9.92 us (5%)
  other arithmetic  9.73 us (5%)
  Pallas kernels  7.03 us (4%)
  matrix products  2.01 us (1%)
    all_to_all x8, waiting for transfers between devices, exchanged(): return lax.all_to_all(blocks, axis, split_axis=0, concat_axis=0, tiled=True)  60.2 us
    all_to_all x8, starting transfers between devices, exchanged(): return lax.all_to_all(blocks, axis, split_axis=0, concat_axis=0, tiled=True)  48 us
    ppermute x15, waiting for transfers between devices, shifted(): lax.ppermute(array, axis, [(i, (i + by) % size) for i in range(size)])  32.8 us
    ppermute x15, starting transfers between devices, shifted(): lax.ppermute(array, axis, [(i, (i + by) % size) for i in range(size)])  19.4 us
    unnamed x44, local copies, waits for them, and re-layouts  3.99 us
    add x1, other arithmetic, local(): new_state = decay[..., None] * old + left[..., None] * right[:, :, None, :]  3.96 us
  transfers between devices with their start and end apart: 24, of which 13 were waited for; matrix products, arithmetic and copies ran while one was open for 7% of the time, Pallas kernels for 0%

profile of v6, /device:TPU:1, one launch (start us, length us, event | category | flops | bytes accessed | tf_op | source)
XLA Modules:
  0.0 192.4 jit_solution(13954380981128608550)
XLA Ops:
  2.0 8.6 %all-to-all-start = ((bf16[32,16,128]{2,1,0:T(8,128)(2,1)}), bf16[32,16,128]{2,1,0:T(8,128)(2,1)S(1)}, u32[]{:S(2)}, u32[]{:S(2)}) async-start(bf16[32,16,128]{2,1,0:T(8,128)(2,1)} %bitcast.1), calls=%async_computation | async-start | bytes 262144 | tf_op jit(solution)/shard_map/all_to_all | solution.py:23
  14.5 3.7 %all-to-all-done = bf16[32,16,128]{2,1,0:T(8,128)(2,1)S(1)} async-done(((bf16[32,16,128]{2,1,0:T(8,128)(2,1)}), bf16[32,16,128]{2,1,0:T(8,128)(2,1)S(1)}, u32[]{:S(2)}, u32[]{:S(2)}) %all-to-all-start) | async-done | bytes 131104 | tf_op jit(solution)/shard_map/all_to_all | solution.py:23
  19.0 5.0 %collective-permute-done.1 = bf16[128,1536]{1,0:T(8,128)(2,1)S(1)} collective-permute-done((bf16[128,1536]{1,0:T(8,128)(2,1)S(1)}, bf16[128,1536]{1,0:T(8,128)(2,1)S(1)}, u32[]{:S(2)}, u32[]{:S(2)}) %collective-permute-start.1) | collective-permute-done | bytes 393248 | tf_op jit(solution)/shard_map/ppermute | solution.py:37
  24.0 2.5 %collective-permute-start.3 = (bf16[128,768]{1,0:T(8,128)(2,1)S(1)}, bf16[128,768]{1,0:T(8,128)(2,1)S(1)}, u32[]{:S(2)}, u32[]{:S(2)}) collective-permute-start(bf16[128,768]{1,0:T(8,128)(2,1)S(1)} %slice.86), channel_id=1, source_target_pairs={{0,24},{8,0},{16,8},{24,16},{1,25},{9,1},{17,9},{25,17},{2,26},{10... | collective-permute-start | bytes 589832 | tf_op jit(solution)/shard_map/ppermute | solution.py:37
  26.9 2.8 %collective-permute-done.3 = bf16[128,768]{1,0:T(8,128)(2,1)S(1)} collective-permute-done((bf16[128,768]{1,0:T(8,128)(2,1)S(1)}, bf16[128,768]{1,0:T(8,128)(2,1)S(1)}, u32[]{:S(2)}, u32[]{:S(2)}) %collective-permute-start.3) | collective-permute-done | bytes 196640 | tf_op jit(solution)/shard_map/ppermute | solution.py:37
  29.9 3.0 %collective-permute-done.2 = bf16[128,768]{1,0:T(8,128)(2,1)S(1)} collective-permute-done((bf16[128,768]{1,0:T(8,128)(2,1)S(1)}, bf16[128,768]{1,0:T(8,128)(2,1)S(1)}, u32[]{:S(2)}, u32[]{:S(2)}) %collective-permute-start.2) | collective-permute-done | bytes 196640 | tf_op jit(solution)/shard_map/ppermute | solution.py:37
  34.2 8.2 %all-to-all-start.1 = ((bf16[8,16,1538]{2,1,0:T(8,128)(2,1)}), bf16[8,16,1538]{2,1,0:T(8,128)(2,1)S(1)}, u32[]{:S(2)}, u32[]{:S(2)}) async-start(bf16[8,16,1538]{2,1,0:T(8,128)(2,1)} %concatenate.28), calls=%async_computation.1 | async-start | bytes 851968 | tf_op jit(solution)/shard_map/all_to_all | solution.py:23
  42.5 1.6 collective-permute-start.5
  45.5 9.7 %all-to-all-done.1 = bf16[8,16,1538]{2,1,0:T(8,128)(2,1)S(1)} async-done(((bf16[8,16,1538]{2,1,0:T(8,128)(2,1)}), bf16[8,16,1538]{2,1,0:T(8,128)(2,1)S(1)}, u32[]{:S(2)}, u32[]{:S(2)}) %all-to-all-start.1) | async-done | bytes 393760 | tf_op jit(solution)/shard_map/all_to_all | solution.py:23
  56.0 2.6 %multiply_reduce_fusion = f32[16,2,256]{2,1,0:T(2,128)S(1)} fusion(f32[16,2,128,256]{3,2,1,0:T(8,128)} %param.15, f32[16,2,128]{2,1,0:T(2,128)S(1)} %copy.59), kind=kLoop, calls=%fused_computation.1 | loop fusion | flops 2088960 | bytes 4243456 | tf_op jit(solution)/shard_map/reduce_sum | solution.py:206
  59.8 3.4 %all-to-all-start.2 = ((bf16[8,16,512]{2,1,0:T(8,128)(2,1)}), bf16[8,16,512]{2,1,0:T(8,128)(2,1)S(1)}, u32[]{:S(2)}, u32[]{:S(2)}) async-start(bf16[8,16,512]{2,1,0:T(8,128)(2,1)} %broadcast_in_dim.10), calls=%async_computation.2 | async-start | bytes 262144 | tf_op jit(solution)/shard_map/all_to_all | solution.py:23
  63.3 7.8 %all-to-all-done.2 = bf16[8,16,512]{2,1,0:T(8,128)(2,1)S(1)} async-done(((bf16[8,16,512]{2,1,0:T(8,128)(2,1)}), bf16[8,16,512]{2,1,0:T(8,128)(2,1)S(1)}, u32[]{:S(2)}, u32[]{:S(2)}) %all-to-all-start.2) | async-done | bytes 131104 | tf_op jit(solution)/shard_map/all_to_all | solution.py:23
  71.9 8.1 %all-to-all-start.3 = ((bf16[8,16,512]{2,1,0:T(8,128)(2,1)}), bf16[8,16,512]{2,1,0:T(8,128)(2,1)S(1)}, u32[]{:S(2)}, u32[]{:S(2)}) async-start(bf16[8,16,512]{2,1,0:T(8,128)(2,1)} %bitcast.12), calls=%async_computation.3 | async-start | bytes 262144 | tf_op jit(solution)/shard_map/all_to_all | solution.py:23
  81.4 3.8 %all-to-all-done.3 = bf16[8,16,512]{2,1,0:T(8,128)(2,1)S(1)} async-done(((bf16[8,16,512]{2,1,0:T(8,128)(2,1)}), bf16[8,16,512]{2,1,0:T(8,128)(2,1)S(1)}, u32[]{:S(2)}, u32[]{:S(2)}) %all-to-all-start.3) | async-done | bytes 131104 | tf_op jit(solution)/shard_map/all_to_all | solution.py:23
  85.2 3.6 %all-to-all-start.5 = ((bf16[8,256,128]{2,1,0:T(8,128)(2,1)}), bf16[8,256,128]{2,1,0:T(8,128)(2,1)S(1)}, u32[]{:S(2)}, u32[]{:S(2)}) async-start(bf16[8,256,128]{2,1,0:T(8,128)(2,1)} %bitcast.15), calls=%async_computation.5 | async-start | bytes 1048576 | tf_op jit(solution)/shard_map/all_to_all | solution.py:23
  88.9 17.8 %all-to-all-done.5.w0_ref = bf16[8,256,128]{2,1,0:T(8,128)(2,1)S(1)} async-done(((bf16[8,256,128]{2,1,0:T(8,128)(2,1)}), bf16[8,256,128]{2,1,0:T(8,128)(2,1)S(1)}, u32[]{:S(2)}, u32[]{:S(2)}) %all-to-all-start.5) | async-done | bytes 524320 | tf_op jit(solution)/shard_map/all_to_all | solution.py:23
  107.7 3.9 %all-to-all-start.4 = ((bf16[32,16,512]{2,1,0:T(8,128)(2,1)}), bf16[32,16,512]{2,1,0:T(8,128)(2,1)S(1)}, u32[]{:S(2)}, u32[]{:S(2)}) async-start(bf16[32,16,512]{2,1,0:T(8,128)(2,1)} %broadcast_in_dim.11), calls=%async_computation.4 | async-start | bytes 1048576 | tf_op jit(solution)/shard_map/all_to_all | solution.py:23
  111.7 2.7 %collective-permute-start.8 = (bf16[8,256,128]{2,1,0:T(8,128)(2,1)S(1)}, bf16[8,256,128]{2,1,0:T(8,128)(2,1)S(1)}, u32[]{:S(2)}, u32[]{:S(2)}) collective-permute-start(bf16[8,256,128]{2,1,0:T(8,128)(2,1)S(1)} %all-to-all-done.5.w0_ref), channel_id=1, source_target_pairs={{0,24},{8,0},{16,8},{24,16},{1,25},{9,1},{17,9},{25,17},{2,26},{10... | collective-permute-start | bytes 1572872 | tf_op jit(solution)/shard_map/ppermute | solution.py:37
  114.3 13.8 %all-to-all-done.4 = bf16[32,16,512]{2,1,0:T(8,128)(2,1)S(1)} async-done(((bf16[32,16,512]{2,1,0:T(8,128)(2,1)}), bf16[32,16,512]{2,1,0:T(8,128)(2,1)S(1)}, u32[]{:S(2)}, u32[]{:S(2)}) %all-to-all-start.4) | async-done | bytes 524320 | tf_op jit(solution)/shard_map/all_to_all | solution.py:23
  128.2 2.1 %collective-permute-start.7 = (bf16[8,64,512]{2,1,0:T(8,128)(2,1)S(1)}, bf16[8,64,512]{2,1,0:T(8,128)(2,1)S(1)}, u32[]{:S(2)}, u32[]{:S(2)}) collective-permute-start(bf16[8,64,512]{2,1,0:T(8,128)(2,1)S(1)} %bitcast.56), channel_id=1, source_target_pairs={{0,1},{1,0},{2,3},{3,2},{4,5},{5,4},{6,7},{7,6},{8,9},{9,8},{10,11... | collective-permute-start | bytes 1572872 | tf_op jit(solution)/shard_map/ppermute | solution.py:41
  130.7 2.7 %collective-permute-start.11 = (bf16[4,256,128]{2,1,0:T(8,128)(2,1)S(1)}, bf16[4,256,128]{2,1,0:T(8,128)(2,1)S(1)}, u32[]{:S(2)}, u32[]{:S(2)}) collective-permute-start(bf16[4,256,128]{2,1,0:T(8,128)(2,1)S(1)} %slice.98), channel_id=1, source_target_pairs={{0,24},{8,0},{16,8},{24,16},{1,25},{9,1},{17,9},{25,17},{2,26},{10... | collective-permute-start | bytes 786440 | tf_op jit(solution)/shard_map/ppermute | solution.py:37
  133.4 6.3 %collective-permute-done.10.w2a_ref = bf16[4,256,128]{2,1,0:T(8,128)(2,1)S(1)} collective-permute-done((bf16[4,256,128]{2,1,0:T(8,128)(2,1)S(1)}, bf16[4,256,128]{2,1,0:T(8,128)(2,1)S(1)}, u32[]{:S(2)}, u32[]{:S(2)}) %collective-permute-start.10) | collective-permute-done | bytes 262176 | tf_op jit(solution)/shard_map/ppermute | solution.py:37
  141.9 3.4 %hidden.1 = bf16[8,128,256]{2,1,0:T(8,128)(2,1)} custom-call(bf16[8,64,512]{2,1,0:T(8,128)(2,1)} %bitcast.57, bf16[8,64,512]{2,1,0:T(8,128)(2,1)} %copy-done.7, bf16[8,256,128]{2,1,0:T(8,128)(2,1)} %copy-done, bf16[8,256,128]{2,1,0:T(8,128)(2,1)} %copy-done.4, bf16[4,256,128]{2,1,0:T(8,128)(2,1)} %copy-done.10, bf16[4,256,128]{2,1,0:T(8,128)(2,1)} %copy-done.11, ...), custom_call_target="tpu_custom_call" | custom-call | tf_op jit(solution)/shard_map/hidden/pallas_call | solution.py:230
  145.3 3.5 %all-to-all-start.6 = ((bf16[8,128,256]{2,1,0:T(8,128)(2,1)}), bf16[8,128,256]{2,1,0:T(8,128)(2,1)S(1)}, u32[]{:S(2)}, u32[]{:S(2)}) async-start(bf16[8,128,256]{2,1,0:T(8,128)(2,1)} %hidden.1), calls=%async_computation.6 | async-start | bytes 1048576 | tf_op jit(solution)/shard_map/all_to_all | solution.py:23
  148.9 2.7 %collective-permute-start.12 = (bf16[2048,128]{1,0:T(8,128)(2,1)S(1)}, bf16[2048,128]{1,0:T(8,128)(2,1)S(1)}, u32[]{:S(2)}, u32[]{:S(2)}) collective-permute-start(bf16[2048,128]{1,0:T(8,128)(2,1)S(1)} %copy-done.9), channel_id=1, source_target_pairs={{0,24},{8,0},{16,8},{24,16},{1,25},{9,1},{17,9},{25,17},{2,26},{10... | collective-permute-start | bytes 1572872 | tf_op jit(solution)/shard_map/ppermute | solution.py:37
  151.6 11.1 %collective-permute-done.13.w3_ref = bf16[2048,128]{1,0:T(8,128)(2,1)S(1)} collective-permute-done((bf16[2048,128]{1,0:T(8,128)(2,1)S(1)}, bf16[2048,128]{1,0:T(8,128)(2,1)S(1)}, u32[]{:S(2)}, u32[]{:S(2)}) %collective-permute-start.13) | collective-permute-done | bytes 524320 | tf_op jit(solution)/shard_map/ppermute | solution.py:37
  162.9 2.7 %collective-permute-start.15 = (bf16[1024,128]{1,0:T(8,128)(2,1)S(1)}, bf16[1024,128]{1,0:T(8,128)(2,1)S(1)}, u32[]{:S(2)}, u32[]{:S(2)}) collective-permute-start(bf16[1024,128]{1,0:T(8,128)(2,1)S(1)} %slice.100), channel_id=1, source_target_pairs={{0,24},{8,0},{16,8},{24,16},{1,25},{9,1},{17,9},{25,17},{2,26},{10... | collective-permute-start | bytes 786440 | tf_op jit(solution)/shard_map/ppermute | solution.py:37
  165.6 4.5 %collective-permute-done.14.w2a_ref = bf16[1024,128]{1,0:T(8,128)(2,1)S(1)} collective-permute-done((bf16[1024,128]{1,0:T(8,128)(2,1)S(1)}, bf16[1024,128]{1,0:T(8,128)(2,1)S(1)}, u32[]{:S(2)}, u32[]{:S(2)}) %collective-permute-start.14) | collective-permute-done | bytes 262176 | tf_op jit(solution)/shard_map/ppermute | solution.py:37
  171.7 3.6 %down.1 = bf16[4,8,16,128]{3,2,1,0:T(8,128)(2,1)} custom-call(bf16[8,128,256]{2,1,0:T(8,128)(2,1)} %copy-done.2, bf16[16,512]{1,0:T(8,128)(2,1)} %copy-done.14, bf16[2048,128]{1,0:T(8,128)(2,1)} %w0_ref.1, bf16[2048,128]{1,0:T(8,128)(2,1)} %copy-done.6, bf16[1024,128]{1,0:T(8,128)(2,1)} %copy-done.12, bf16[1024,128]{1,0:T(8,128)(2,1)} %copy-done.13, ...), custom_call_target="tpu_custom_call" | custom-call | tf_op jit(solution)/shard_map/down/pallas_call | solution.py:243
  175.4 8.8 %all-to-all-start.7 = ((bf16[32,16,128]{2,1,0:T(8,128)(2,1)}), bf16[32,16,128]{2,1,0:T(8,128)(2,1)S(1)}, u32[]{:S(2)}, u32[]{:S(2)}) async-start(bf16[32,16,128]{2,1,0:T(8,128)(2,1)} %bitcast.62), calls=%async_computation.7 | async-start | bytes 262144 | tf_op jit(solution)/shard_map/all_to_all | solution.py:23
  184.2 4.0 %multiply_add_fusion = f32[16,2,128,256]{3,2,1,0:T(8,128)} fusion(f32[16,2,128,256]{3,2,1,0:T(8,128)} %param.15, f32[16,2,256]{2,1,0:T(2,128)S(1)} %reshape.188, f32[16,2,128]{2,1,0:T(2,128)S(1)} %copy.64, f32[2]{0:T(128)S(1)} %exponential_subtract_fusion), kind=kLoop, calls=%fused_computation | loop fusion | flops 3145728 | bytes 8437768 | tf_op jit(solution)/shard_map/add | solution.py:212
  188.1 3.6 %all-to-all-done.7 = bf16[32,16,128]{2,1,0:T(8,128)(2,1)S(1)} async-done(((bf16[32,16,128]{2,1,0:T(8,128)(2,1)}), bf16[32,16,128]{2,1,0:T(8,128)(2,1)S(1)}, u32[]{:S(2)}, u32[]{:S(2)}) %all-to-all-start.7) | async-done | bytes 131104 | tf_op jit(solution)/shard_map/all_to_all | solution.py:23
  (114 shorter events, 19.7 us)
Async XLA Ops:
  2.0 16.2 %all-to-all-start = ((bf16[32,16,128]{2,1,0:T(8,128)(2,1)}), bf16[32,16,128]{2,1,0:T(8,128)(2,1)S(1)}, u32[]{:S(2)}, u32[]{:S(2)}) async-start(bf16[32,16,128]{2,1,0:T(8,128)(2,1)} %bitcast.1), calls=%async_computation | async-start | bytes 262144 | tf_op jit(solution)/shard_map/all_to_all | solution.py:23
  11.7 14.8 %collective-permute-start = (bf16[128,1536]{1,0:T(8,128)(2,1)S(1)}, bf16[128,1536]{1,0:T(8,128)(2,1)S(1)}, u32[]{:S(2)}, u32[]{:S(2)}) collective-permute-start(bf16[128,1536]{1,0:T(8,128)(2,1)S(1)} %multiply_convert_fusion.1), channel_id=1, source_target_pairs={{0,8},{8,16},{16,24},{24,0},{1,9},{9,17},{17,25},{25,1},{2,10},{10... | collective-permute-start | bytes 1179656 | tf_op jit(solution)/shard_map/ppermute | solution.py:37
  13.2 10.8 %collective-permute-start.1 = (bf16[128,1536]{1,0:T(8,128)(2,1)S(1)}, bf16[128,1536]{1,0:T(8,128)(2,1)S(1)}, u32[]{:S(2)}, u32[]{:S(2)}) collective-permute-start(bf16[128,1536]{1,0:T(8,128)(2,1)S(1)} %multiply_convert_fusion.1), channel_id=1, source_target_pairs={{0,24},{8,0},{16,8},{24,16},{1,25},{9,1},{17,9},{25,17},{2,26},{10... | collective-permute-start | bytes 1179656 | tf_op jit(solution)/shard_map/ppermute | solution.py:37
  19.0 23.4 %copy-start.15 = (bf16[512,128]{1,0:T(8,128)(2,1)S(1)}, bf16[512,128]{1,0:T(8,128)(2,1)}, u32[]{:S(2)}) copy-start(bf16[512,128]{1,0:T(8,128)(2,1)} %param.22) | copy-start | bytes 393220
  19.0 26.2 %copy-start.18 = (s32[16]{0:T(128)S(1)}, s32[16]{0:T(128)}, u32[]{:S(2)}) copy-start(s32[16]{0:T(128)} %param.14) | copy-start | bytes 196
  24.0 5.7 %collective-permute-start.3 = (bf16[128,768]{1,0:T(8,128)(2,1)S(1)}, bf16[128,768]{1,0:T(8,128)(2,1)S(1)}, u32[]{:S(2)}, u32[]{:S(2)}) collective-permute-start(bf16[128,768]{1,0:T(8,128)(2,1)S(1)} %slice.86), channel_id=1, source_target_pairs={{0,24},{8,0},{16,8},{24,16},{1,25},{9,1},{17,9},{25,17},{2,26},{10... | collective-permute-start | bytes 589832 | tf_op jit(solution)/shard_map/ppermute | solution.py:37
  26.5 6.4 %collective-permute-start.2 = (bf16[128,768]{1,0:T(8,128)(2,1)S(1)}, bf16[128,768]{1,0:T(8,128)(2,1)S(1)}, u32[]{:S(2)}, u32[]{:S(2)}) collective-permute-start(bf16[128,768]{1,0:T(8,128)(2,1)S(1)} %slice.85), channel_id=1, source_target_pairs={{0,8},{8,16},{16,24},{24,0},{1,9},{9,17},{17,25},{25,1},{2,10},{10... | collective-permute-start | bytes 589832 | tf_op jit(solution)/shard_map/ppermute | solution.py:37
  33.4 25.6 %copy-start.16 = (f32[512]{0:T(512)S(1)}, f32[512]{0:T(512)}, u32[]{:S(2)}) copy-start(f32[512]{0:T(512)} %param.21) | copy-start | bytes 6148
  34.2 20.9 %all-to-all-start.1 = ((bf16[8,16,1538]{2,1,0:T(8,128)(2,1)}), bf16[8,16,1538]{2,1,0:T(8,128)(2,1)S(1)}, u32[]{:S(2)}, u32[]{:S(2)}) async-start(bf16[8,16,1538]{2,1,0:T(8,128)(2,1)} %concatenate.28), calls=%async_computation.1 | async-start | bytes 851968 | tf_op jit(solution)/shard_map/all_to_all | solution.py:23
  42.4 20.7 %collective-permute-start.6 = (bf16[512,128]{1,0:T(8,128)(2,1)S(1)}, bf16[512,128]{1,0:T(8,128)(2,1)S(1)}, u32[]{:S(2)}, u32[]{:S(2)}) collective-permute-start(bf16[512,128]{1,0:T(8,128)(2,1)S(1)} %copy-done.15), channel_id=1, source_target_pairs={{0,8},{8,16},{16,24},{24,0},{1,9},{9,17},{17,25},{25,1},{2,10},{10... | collective-permute-start | bytes 393224 | tf_op jit(solution)/shard_map/ppermute | solution.py:37
  42.5 20.6 %collective-permute-start.5 = (bf16[512,128]{1,0:T(8,128)(2,1)S(1)}, bf16[512,128]{1,0:T(8,128)(2,1)S(1)}, u32[]{:S(2)}, u32[]{:S(2)}) collective-permute-start(bf16[512,128]{1,0:T(8,128)(2,1)S(1)} %copy-done.15), channel_id=1, source_target_pairs={{0,16},{8,24},{16,0},{24,8},{1,17},{9,25},{17,1},{25,9},{2,18},{10... | collective-permute-start | bytes 393224 | tf_op jit(solution)/shard_map/ppermute | solution.py:37
  44.1 19.1 %collective-permute-start.4 = (bf16[512,128]{1,0:T(8,128)(2,1)S(1)}, bf16[512,128]{1,0:T(8,128)(2,1)S(1)}, u32[]{:S(2)}, u32[]{:S(2)}) collective-permute-start(bf16[512,128]{1,0:T(8,128)(2,1)S(1)} %copy-done.15), channel_id=1, source_target_pairs={{0,24},{8,0},{16,8},{24,16},{1,25},{9,1},{17,9},{25,17},{2,26},{10... | collective-permute-start | bytes 393224 | tf_op jit(solution)/shard_map/ppermute | solution.py:37
  45.4 34.5 %copy-start.8 = (bf16[128,2048]{1,0:T(8,128)(2,1)S(1)}, bf16[128,2048]{1,0:T(8,128)(2,1)}, u32[]{:S(2)}) copy-start(bf16[128,2048]{1,0:T(8,128)(2,1)} %param.24) | copy-start | bytes 1572868
  45.4 34.5 %copy-start.17 = (f32[128]{0:T(128)S(1)}, f32[128]{0:T(128)}, u32[]{:S(2)}) copy-start(f32[128]{0:T(128)} %param.23) | copy-start | bytes 1540
  59.8 11.3 %all-to-all-start.2 = ((bf16[8,16,512]{2,1,0:T(8,128)(2,1)}), bf16[8,16,512]{2,1,0:T(8,128)(2,1)S(1)}, u32[]{:S(2)}, u32[]{:S(2)}) async-start(bf16[8,16,512]{2,1,0:T(8,128)(2,1)} %broadcast_in_dim.10), calls=%async_computation.2 | async-start | bytes 262144 | tf_op jit(solution)/shard_map/all_to_all | solution.py:23
  71.9 13.3 %all-to-all-start.3 = ((bf16[8,16,512]{2,1,0:T(8,128)(2,1)}), bf16[8,16,512]{2,1,0:T(8,128)(2,1)S(1)}, u32[]{:S(2)}, u32[]{:S(2)}) async-start(bf16[8,16,512]{2,1,0:T(8,128)(2,1)} %bitcast.12), calls=%async_computation.3 | async-start | bytes 262144 | tf_op jit(solution)/shard_map/all_to_all | solution.py:23
  85.2 63.6 %copy-start.9 = (bf16[2048,128]{1,0:T(8,128)(2,1)S(1)}, bf16[2048,128]{1,0:T(8,128)(2,1)}, u32[]{:S(2)}) copy-start(bf16[2048,128]{1,0:T(8,128)(2,1)} %w0_ref.1) | copy-start | bytes 1572868
  85.2 21.5 %all-to-all-start.5 = ((bf16[8,256,128]{2,1,0:T(8,128)(2,1)}), bf16[8,256,128]{2,1,0:T(8,128)(2,1)S(1)}, u32[]{:S(2)}, u32[]{:S(2)}) async-start(bf16[8,256,128]{2,1,0:T(8,128)(2,1)} %bitcast.15), calls=%async_computation.5 | async-start | bytes 1048576 | tf_op jit(solution)/shard_map/all_to_all | solution.py:23
  88.9 74.0 %copy-start.14 = (bf16[16,512]{1,0:T(8,128)(2,1)}, bf16[16,512]{1,0:T(8,128)(2,1)S(1)}, u32[]{:S(2)}) copy-start(bf16[16,512]{1,0:T(8,128)(2,1)S(1)} %fusion.3.resid_ref) | copy-start | bytes 49156
  106.7 34.3 %copy-start = (bf16[8,256,128]{2,1,0:T(8,128)(2,1)}, bf16[8,256,128]{2,1,0:T(8,128)(2,1)S(1)}, u32[]{:S(2)}) copy-start(bf16[8,256,128]{2,1,0:T(8,128)(2,1)S(1)} %all-to-all-done.5.w0_ref) | copy-start | bytes 1572868
  107.7 20.5 %all-to-all-start.4 = ((bf16[32,16,512]{2,1,0:T(8,128)(2,1)}), bf16[32,16,512]{2,1,0:T(8,128)(2,1)S(1)}, u32[]{:S(2)}, u32[]{:S(2)}) async-start(bf16[32,16,512]{2,1,0:T(8,128)(2,1)} %broadcast_in_dim.11), calls=%async_computation.4 | async-start | bytes 1048576 | tf_op jit(solution)/shard_map/all_to_all | solution.py:23
  111.6 18.7 %collective-permute-start.9 = (bf16[8,256,128]{2,1,0:T(8,128)(2,1)S(1)}, bf16[8,256,128]{2,1,0:T(8,128)(2,1)S(1)}, u32[]{:S(2)}, u32[]{:S(2)}) collective-permute-start(bf16[8,256,128]{2,1,0:T(8,128)(2,1)S(1)} %all-to-all-done.5.w0_ref), channel_id=1, source_target_pairs={{0,8},{8,16},{16,24},{24,0},{1,9},{9,17},{17,25},{25,1},{2,10},{10... | collective-permute-start | bytes 1572872 | tf_op jit(solution)/shard_map/ppermute | solution.py:37
  111.7 18.9 %collective-permute-start.8 = (bf16[8,256,128]{2,1,0:T(8,128)(2,1)S(1)}, bf16[8,256,128]{2,1,0:T(8,128)(2,1)S(1)}, u32[]{:S(2)}, u32[]{:S(2)}) collective-permute-start(bf16[8,256,128]{2,1,0:T(8,128)(2,1)S(1)} %all-to-all-done.5.w0_ref), channel_id=1, source_target_pairs={{0,24},{8,0},{16,8},{24,16},{1,25},{9,1},{17,9},{25,17},{2,26},{10... | collective-permute-start | bytes 1572872 | tf_op jit(solution)/shard_map/ppermute | solution.py:37
  128.2 12.9 %collective-permute-start.7 = (bf16[8,64,512]{2,1,0:T(8,128)(2,1)S(1)}, bf16[8,64,512]{2,1,0:T(8,128)(2,1)S(1)}, u32[]{:S(2)}, u32[]{:S(2)}) collective-permute-start(bf16[8,64,512]{2,1,0:T(8,128)(2,1)S(1)} %bitcast.56), channel_id=1, source_target_pairs={{0,1},{1,0},{2,3},{3,2},{4,5},{5,4},{6,7},{7,6},{8,9},{9,8},{10,11... | collective-permute-start | bytes 1572872 | tf_op jit(solution)/shard_map/ppermute | solution.py:41
  130.3 9.3 %collective-permute-start.10 = (bf16[4,256,128]{2,1,0:T(8,128)(2,1)S(1)}, bf16[4,256,128]{2,1,0:T(8,128)(2,1)S(1)}, u32[]{:S(2)}, u32[]{:S(2)}) collective-permute-start(bf16[4,256,128]{2,1,0:T(8,128)(2,1)S(1)} %slice.97), channel_id=1, source_target_pairs={{0,8},{8,16},{16,24},{24,0},{1,9},{9,17},{17,25},{25,1},{2,10},{10... | collective-permute-start | bytes 786440 | tf_op jit(solution)/shard_map/ppermute | solution.py:37
  130.7 9.7 %collective-permute-start.11 = (bf16[4,256,128]{2,1,0:T(8,128)(2,1)S(1)}, bf16[4,256,128]{2,1,0:T(8,128)(2,1)S(1)}, u32[]{:S(2)}, u32[]{:S(2)}) collective-permute-start(bf16[4,256,128]{2,1,0:T(8,128)(2,1)S(1)} %slice.98), channel_id=1, source_target_pairs={{0,24},{8,0},{16,8},{24,16},{1,25},{9,1},{17,9},{25,17},{2,26},{10... | collective-permute-start | bytes 786440 | tf_op jit(solution)/shard_map/ppermute | solution.py:37
  145.3 24.9 %all-to-all-start.6 = ((bf16[8,128,256]{2,1,0:T(8,128)(2,1)}), bf16[8,128,256]{2,1,0:T(8,128)(2,1)S(1)}, u32[]{:S(2)}, u32[]{:S(2)}) async-start(bf16[8,128,256]{2,1,0:T(8,128)(2,1)} %hidden.1), calls=%async_computation.6 | async-start | bytes 1048576 | tf_op jit(solution)/shard_map/all_to_all | solution.py:23
  148.8 13.9 %collective-permute-start.13 = (bf16[2048,128]{1,0:T(8,128)(2,1)S(1)}, bf16[2048,128]{1,0:T(8,128)(2,1)S(1)}, u32[]{:S(2)}, u32[]{:S(2)}) collective-permute-start(bf16[2048,128]{1,0:T(8,128)(2,1)S(1)} %copy-done.9), channel_id=1, source_target_pairs={{0,8},{8,16},{16,24},{24,0},{1,9},{9,17},{17,25},{25,1},{2,10},{10... | collective-permute-start | bytes 1572872 | tf_op jit(solution)/shard_map/ppermute | solution.py:37
  148.9 13.9 %collective-permute-start.12 = (bf16[2048,128]{1,0:T(8,128)(2,1)S(1)}, bf16[2048,128]{1,0:T(8,128)(2,1)S(1)}, u32[]{:S(2)}, u32[]{:S(2)}) collective-permute-start(bf16[2048,128]{1,0:T(8,128)(2,1)S(1)} %copy-done.9), channel_id=1, source_target_pairs={{0,24},{8,0},{16,8},{24,16},{1,25},{9,1},{17,9},{25,17},{2,26},{10... | collective-permute-start | bytes 1572872 | tf_op jit(solution)/shard_map/ppermute | solution.py:37
  162.7 7.4 %collective-permute-start.14 = (bf16[1024,128]{1,0:T(8,128)(2,1)S(1)}, bf16[1024,128]{1,0:T(8,128)(2,1)S(1)}, u32[]{:S(2)}, u32[]{:S(2)}) collective-permute-start(bf16[1024,128]{1,0:T(8,128)(2,1)S(1)} %slice.99), channel_id=1, source_target_pairs={{0,8},{8,16},{16,24},{24,0},{1,9},{9,17},{17,25},{25,1},{2,10},{10... | collective-permute-start | bytes 786440 | tf_op jit(solution)/shard_map/ppermute | solution.py:37
  162.9 7.3 %collective-permute-start.15 = (bf16[1024,128]{1,0:T(8,128)(2,1)S(1)}, bf16[1024,128]{1,0:T(8,128)(2,1)S(1)}, u32[]{:S(2)}, u32[]{:S(2)}) collective-permute-start(bf16[1024,128]{1,0:T(8,128)(2,1)S(1)} %slice.100), channel_id=1, source_target_pairs={{0,24},{8,0},{16,8},{24,16},{1,25},{9,1},{17,9},{25,17},{2,26},{10... | collective-permute-start | bytes 786440 | tf_op jit(solution)/shard_map/ppermute | solution.py:37
  175.4 16.4 %all-to-all-start.7 = ((bf16[32,16,128]{2,1,0:T(8,128)(2,1)}), bf16[32,16,128]{2,1,0:T(8,128)(2,1)S(1)}, u32[]{:S(2)}, u32[]{:S(2)}) async-start(bf16[32,16,128]{2,1,0:T(8,128)(2,1)} %bitcast.62), calls=%async_computation.7 | async-start | bytes 262144 | tf_op jit(solution)/shard_map/all_to_all | solution.py:23
  (11 other events, 53.5 us)

commit v7 on v6

--- a/solution.py
+++ b/solution.py
@@ -12,7 +12,7 @@
 DV = 256
 KV = ("z", "y")
 TP = ("x", "c")
-ZX = ("z", "x")
+XZ = ("x", "z")
 NZ, NY, NX, NC = (8, 4, 4, 2)
 
 
@@ -66,8 +66,8 @@
     for k in range(NZ // STEP):
         at = pl.ds(STEP * k, STEP)
         parts = [
-            pltpu.make_async_copy(own_ref.at[at], x_ref.at[me, at], x_sem.at[k, 0]),
-            pltpu.make_async_copy(other_ref.at[at], x_ref.at[1 - me, at], x_sem.at[k, 1]),
+            pltpu.make_async_copy(own_ref.at[:, at], x_ref.at[me, :, at], x_sem.at[k, 0]),
+            pltpu.make_async_copy(other_ref.at[:, at], x_ref.at[1 - me, :, at], x_sem.at[k, 1]),
         ]
         half = NZ // STEP // 2
         far = w2a_ref.at[at] if k < half else w2b_ref.at[pl.ds(STEP * (k - half), STEP)]
@@ -76,20 +76,21 @@
         for copy in parts:
             copy.start()
         copies.append(parts)
-    rows = own_ref.shape[1]
-    hidden = jnp.zeros((2 * rows, 256), jnp.float32)
-    squares = jnp.zeros((2 * rows, 1), jnp.float32)
+    hidden = jnp.zeros((128, 256), jnp.float32)
+    squares = jnp.zeros((128, 128), jnp.float32)
     for z in range(NZ):
         if z % STEP == 0:
             for copy in copies[z // STEP]:
                 copy.wait()
-        left = x_ref[:, z].reshape(2 * rows, 512)
+        left = x_ref[:, :, z].reshape(128, 512)
         wide = left.astype(jnp.float32)
-        squares = squares + jnp.sum(wide * wide, axis=1, keepdims=True)
+        wide = wide * wide
+        for j in range(4):
+            squares = squares + wide[:, 128 * j : 128 * (j + 1)]
         right = [w_ref[:, z, 128 * j : 128 * (j + 1), :].reshape(512, 128) for j in range(2)]
         right = jnp.concatenate(right, axis=1)
         hidden = hidden + jnp.dot(left, right, preferred_element_type=jnp.float32)
-    scale = lax.rsqrt(squares / D + EPS)
+    scale = lax.rsqrt(jnp.sum(squares, axis=1, keepdims=True) / D + EPS)
     positive = jnp.maximum(hidden * scale, 0.0)
     active = (positive * positive).astype(jnp.bfloat16)
     for z in range(NZ):
@@ -224,7 +225,7 @@
     down_low = shifted(down_below[:1024], "y", 1)
     down_high = shifted(down_above[1024:], "y", -1)
 
-    own = copy_for_each(resid, ZX).reshape(NZ, 64, 512)
+    own = copy_for_each(resid, XZ).reshape(NX, NZ, 16, 512)
     other = swapped(own)
     anywhere = pl.BlockSpec(memory_space=pl.ANY)
     active = pl.pallas_call(
@@ -232,7 +233,7 @@
         out_shape=jax.ShapeDtypeStruct((NZ, 128, 256), jnp.bfloat16),
         in_specs=[anywhere] * 7,
         scratch_shapes=[
-            pltpu.VMEM((NC, NZ, 64, 512), jnp.bfloat16),
+            pltpu.VMEM((NC, NX, NZ, 16, 512), jnp.bfloat16),
             pltpu.VMEM((NY, NZ, 256, 128), jnp.bfloat16),
             pltpu.SemaphoreType.DMA((NZ // STEP, 2)),
             pltpu.SemaphoreType.DMA((NZ // STEP, NY)),

time: 193 us -> 192 us (level)
  waiting for transfers between devices: 93 us -> 89.9 us
    all_to_all x8, waiting for transfers between devices: 60.2 us -> 57.6 us  [exchanged(): return lax.all_to_all(blocks, axis, split_axis=0, concat_axis=0, tiled=True)]
where the time goes in v7:
time: 192 us; the launch traced here: 191 us
  waiting for transfers between devices  89.9 us (47%)
  starting transfers between devices  71.1 us (37%)
  local copies, waits for them, and re-layouts  9.92 us (5%)
  other arithmetic  9.73 us (5%)
  Pallas kernels  6.99 us (4%)
  matrix products  2.01 us (1%)
    all_to_all x8, waiting for transfers between devices, exchanged(): return lax.all_to_all(blocks, axis, split_axis=0, concat_axis=0, tiled=True)  57.6 us
    all_to_all x8, starting transfers between devices, exchanged(): return lax.all_to_all(blocks, axis, split_axis=0, concat_axis=0, tiled=True)  48 us
    ppermute x15, waiting for transfers between devices, shifted(): lax.ppermute(array, axis, [(i, (i + by) % size) for i in range(size)])  32.2 us
    ppermute x15, starting transfers between devices, shifted(): lax.ppermute(array, axis, [(i, (i + by) % size) for i in range(size)])  19.4 us
    unnamed x44, local copies, waits for them, and re-layouts  3.99 us
    add x1, other arithmetic, local(): new_state = decay[..., None] * old + left[..., None] * right[:, :, None, :]  3.96 us
  transfers between devices with their start and end apart: 24, of which 13 were waited for; matrix products, arithmetic and copies ran while one was open for 7% of the time, Pallas kernels for 0%

profile of v7, /device:TPU:1, one launch (start us, length us, event | category | flops | bytes accessed | tf_op | source)
XLA Modules:
  0.0 190.8 jit_solution(5709925292506525557)
XLA Ops:
  2.0 8.6 %all-to-all-start = ((bf16[32,16,128]{2,1,0:T(8,128)(2,1)}), bf16[32,16,128]{2,1,0:T(8,128)(2,1)S(1)}, u32[]{:S(2)}, u32[]{:S(2)}) async-start(bf16[32,16,128]{2,1,0:T(8,128)(2,1)} %bitcast.1), calls=%async_computation | async-start | bytes 262144 | tf_op jit(solution)/shard_map/all_to_all | solution.py:23
  14.5 3.7 %all-to-all-done = bf16[32,16,128]{2,1,0:T(8,128)(2,1)S(1)} async-done(((bf16[32,16,128]{2,1,0:T(8,128)(2,1)}), bf16[32,16,128]{2,1,0:T(8,128)(2,1)S(1)}, u32[]{:S(2)}, u32[]{:S(2)}) %all-to-all-start) | async-done | bytes 131104 | tf_op jit(solution)/shard_map/all_to_all | solution.py:23
  19.0 5.0 %collective-permute-done.1 = bf16[128,1536]{1,0:T(8,128)(2,1)S(1)} collective-permute-done((bf16[128,1536]{1,0:T(8,128)(2,1)S(1)}, bf16[128,1536]{1,0:T(8,128)(2,1)S(1)}, u32[]{:S(2)}, u32[]{:S(2)}) %collective-permute-start.1) | collective-permute-done | bytes 393248 | tf_op jit(solution)/shard_map/ppermute | solution.py:37
  24.0 2.5 %collective-permute-start.3 = (bf16[128,768]{1,0:T(8,128)(2,1)S(1)}, bf16[128,768]{1,0:T(8,128)(2,1)S(1)}, u32[]{:S(2)}, u32[]{:S(2)}) collective-permute-start(bf16[128,768]{1,0:T(8,128)(2,1)S(1)} %slice.86), channel_id=1, source_target_pairs={{0,24},{8,0},{16,8},{24,16},{1,25},{9,1},{17,9},{25,17},{2,26},{10... | collective-permute-start | bytes 589832 | tf_op jit(solution)/shard_map/ppermute | solution.py:37
  26.9 2.8 %collective-permute-done.3 = bf16[128,768]{1,0:T(8,128)(2,1)S(1)} collective-permute-done((bf16[128,768]{1,0:T(8,128)(2,1)S(1)}, bf16[128,768]{1,0:T(8,128)(2,1)S(1)}, u32[]{:S(2)}, u32[]{:S(2)}) %collective-permute-start.3) | collective-permute-done | bytes 196640 | tf_op jit(solution)/shard_map/ppermute | solution.py:37
  29.9 3.0 %collective-permute-done.2 = bf16[128,768]{1,0:T(8,128)(2,1)S(1)} collective-permute-done((bf16[128,768]{1,0:T(8,128)(2,1)S(1)}, bf16[128,768]{1,0:T(8,128)(2,1)S(1)}, u32[]{:S(2)}, u32[]{:S(2)}) %collective-permute-start.2) | collective-permute-done | bytes 196640 | tf_op jit(solution)/shard_map/ppermute | solution.py:37
  34.2 8.2 %all-to-all-start.1 = ((bf16[8,16,1538]{2,1,0:T(8,128)(2,1)}), bf16[8,16,1538]{2,1,0:T(8,128)(2,1)S(1)}, u32[]{:S(2)}, u32[]{:S(2)}) async-start(bf16[8,16,1538]{2,1,0:T(8,128)(2,1)} %concatenate.28), calls=%async_computation.1 | async-start | bytes 851968 | tf_op jit(solution)/shard_map/all_to_all | solution.py:23
  42.5 1.6 collective-permute-start.5
  45.5 9.7 %all-to-all-done.1 = bf16[8,16,1538]{2,1,0:T(8,128)(2,1)S(1)} async-done(((bf16[8,16,1538]{2,1,0:T(8,128)(2,1)}), bf16[8,16,1538]{2,1,0:T(8,128)(2,1)S(1)}, u32[]{:S(2)}, u32[]{:S(2)}) %all-to-all-start.1) | async-done | bytes 393760 | tf_op jit(solution)/shard_map/all_to_all | solution.py:23
  56.0 2.6 %multiply_reduce_fusion = f32[16,2,256]{2,1,0:T(2,128)S(1)} fusion(f32[16,2,128,256]{3,2,1,0:T(8,128)} %param.15, f32[16,2,128]{2,1,0:T(2,128)S(1)} %copy.59), kind=kLoop, calls=%fused_computation.1 | loop fusion | flops 2088960 | bytes 4243456 | tf_op jit(solution)/shard_map/reduce_sum | solution.py:207
  59.8 3.4 %all-to-all-start.2 = ((bf16[8,16,512]{2,1,0:T(8,128)(2,1)}), bf16[8,16,512]{2,1,0:T(8,128)(2,1)S(1)}, u32[]{:S(2)}, u32[]{:S(2)}) async-start(bf16[8,16,512]{2,1,0:T(8,128)(2,1)} %broadcast_in_dim.10), calls=%async_computation.2 | async-start | bytes 262144 | tf_op jit(solution)/shard_map/all_to_all | solution.py:23
  63.3 7.8 %all-to-all-done.2 = bf16[8,16,512]{2,1,0:T(8,128)(2,1)S(1)} async-done(((bf16[8,16,512]{2,1,0:T(8,128)(2,1)}), bf16[8,16,512]{2,1,0:T(8,128)(2,1)S(1)}, u32[]{:S(2)}, u32[]{:S(2)}) %all-to-all-start.2) | async-done | bytes 131104 | tf_op jit(solution)/shard_map/all_to_all | solution.py:23
  71.9 8.1 %all-to-all-start.3 = ((bf16[8,16,512]{2,1,0:T(8,128)(2,1)}), bf16[8,16,512]{2,1,0:T(8,128)(2,1)S(1)}, u32[]{:S(2)}, u32[]{:S(2)}) async-start(bf16[8,16,512]{2,1,0:T(8,128)(2,1)} %bitcast.12), calls=%async_computation.3 | async-start | bytes 262144 | tf_op jit(solution)/shard_map/all_to_all | solution.py:23
  81.4 3.8 %all-to-all-done.3 = bf16[8,16,512]{2,1,0:T(8,128)(2,1)S(1)} async-done(((bf16[8,16,512]{2,1,0:T(8,128)(2,1)}), bf16[8,16,512]{2,1,0:T(8,128)(2,1)S(1)}, u32[]{:S(2)}, u32[]{:S(2)}) %all-to-all-start.3) | async-done | bytes 131104 | tf_op jit(solution)/shard_map/all_to_all | solution.py:23
  85.2 3.6 %all-to-all-start.5 = ((bf16[8,256,128]{2,1,0:T(8,128)(2,1)}), bf16[8,256,128]{2,1,0:T(8,128)(2,1)S(1)}, u32[]{:S(2)}, u32[]{:S(2)}) async-start(bf16[8,256,128]{2,1,0:T(8,128)(2,1)} %bitcast.15), calls=%async_computation.5 | async-start | bytes 1048576 | tf_op jit(solution)/shard_map/all_to_all | solution.py:23
  88.9 17.8 %all-to-all-done.5.w0_ref = bf16[8,256,128]{2,1,0:T(8,128)(2,1)S(1)} async-done(((bf16[8,256,128]{2,1,0:T(8,128)(2,1)}), bf16[8,256,128]{2,1,0:T(8,128)(2,1)S(1)}, u32[]{:S(2)}, u32[]{:S(2)}) %all-to-all-start.5) | async-done | bytes 524320 | tf_op jit(solution)/shard_map/all_to_all | solution.py:23
  107.7 3.9 %all-to-all-start.4 = ((bf16[32,16,512]{2,1,0:T(8,128)(2,1)}), bf16[32,16,512]{2,1,0:T(8,128)(2,1)S(1)}, u32[]{:S(2)}, u32[]{:S(2)}) async-start(bf16[32,16,512]{2,1,0:T(8,128)(2,1)} %broadcast_in_dim.11), calls=%async_computation.4 | async-start | bytes 1048576 | tf_op jit(solution)/shard_map/all_to_all | solution.py:23
  111.7 2.7 %collective-permute-start.8 = (bf16[8,256,128]{2,1,0:T(8,128)(2,1)S(1)}, bf16[8,256,128]{2,1,0:T(8,128)(2,1)S(1)}, u32[]{:S(2)}, u32[]{:S(2)}) collective-permute-start(bf16[8,256,128]{2,1,0:T(8,128)(2,1)S(1)} %all-to-all-done.5.w0_ref), channel_id=1, source_target_pairs={{0,24},{8,0},{16,8},{24,16},{1,25},{9,1},{17,9},{25,17},{2,26},{10... | collective-permute-start | bytes 1572872 | tf_op jit(solution)/shard_map/ppermute | solution.py:37
  114.3 11.3 %all-to-all-done.4 = bf16[32,16,512]{2,1,0:T(8,128)(2,1)S(1)} async-done(((bf16[32,16,512]{2,1,0:T(8,128)(2,1)}), bf16[32,16,512]{2,1,0:T(8,128)(2,1)S(1)}, u32[]{:S(2)}, u32[]{:S(2)}) %all-to-all-start.4) | async-done | bytes 524320 | tf_op jit(solution)/shard_map/all_to_all | solution.py:23
  125.6 3.7 %collective-permute-start.7 = (bf16[4,8,16,512]{3,2,1,0:T(8,128)(2,1)S(1)}, bf16[4,8,16,512]{3,2,1,0:T(8,128)(2,1)S(1)}, u32[]{:S(2)}, u32[]{:S(2)}) collective-permute-start(bf16[4,8,16,512]{3,2,1,0:T(8,128)(2,1)S(1)} %bitcast.56), channel_id=1, source_target_pairs={{0,1},{1,0},{2,3},{3,2},{4,5},{5,4},{6,7},{7,6},{8,9},{9,8},{10,11... | collective-permute-start | bytes 1572872 | tf_op jit(solution)/shard_map/ppermute | solution.py:41
  129.6 2.7 %collective-permute-start.11 = (bf16[4,256,128]{2,1,0:T(8,128)(2,1)S(1)}, bf16[4,256,128]{2,1,0:T(8,128)(2,1)S(1)}, u32[]{:S(2)}, u32[]{:S(2)}) collective-permute-start(bf16[4,256,128]{2,1,0:T(8,128)(2,1)S(1)} %slice.98), channel_id=1, source_target_pairs={{0,24},{8,0},{16,8},{24,16},{1,25},{9,1},{17,9},{25,17},{2,26},{10... | collective-permute-start | bytes 786440 | tf_op jit(solution)/shard_map/ppermute | solution.py:37
  132.3 6.3 %collective-permute-done.10.w2a_ref = bf16[4,256,128]{2,1,0:T(8,128)(2,1)S(1)} collective-permute-done((bf16[4,256,128]{2,1,0:T(8,128)(2,1)S(1)}, bf16[4,256,128]{2,1,0:T(8,128)(2,1)S(1)}, u32[]{:S(2)}, u32[]{:S(2)}) %collective-permute-start.10) | collective-permute-done | bytes 262176 | tf_op jit(solution)/shard_map/ppermute | solution.py:37
  140.9 3.4 %hidden.1 = bf16[8,128,256]{2,1,0:T(8,128)(2,1)} custom-call(bf16[4,8,16,512]{3,2,1,0:T(8,128)(2,1)} %bitcast.57, bf16[4,8,16,512]{3,2,1,0:T(8,128)(2,1)} %copy-done.7, bf16[8,256,128]{2,1,0:T(8,128)(2,1)} %copy-done, bf16[8,256,128]{2,1,0:T(8,128)(2,1)} %copy-done.4, bf16[4,256,128]{2,1,0:T(8,128)(2,1)} %copy-done.10, bf16[4,256,128]{2,1,0:T(8,128)(2,1)} %copy-done.11, ...), custom_call_target="tpu_custom_call" | custom-call | tf_op jit(solution)/shard_map/hidden/pallas_call | solution.py:231
  144.2 4.2 %all-to-all-start.6 = ((bf16[8,128,256]{2,1,0:T(8,128)(2,1)}), bf16[8,128,256]{2,1,0:T(8,128)(2,1)S(1)}, u32[]{:S(2)}, u32[]{:S(2)}) async-start(bf16[8,128,256]{2,1,0:T(8,128)(2,1)} %hidden.1), calls=%async_computation.6 | async-start | bytes 1048576 | tf_op jit(solution)/shard_map/all_to_all | solution.py:23
  148.5 2.7 %collective-permute-start.12 = (bf16[2048,128]{1,0:T(8,128)(2,1)S(1)}, bf16[2048,128]{1,0:T(8,128)(2,1)S(1)}, u32[]{:S(2)}, u32[]{:S(2)}) collective-permute-start(bf16[2048,128]{1,0:T(8,128)(2,1)S(1)} %copy-done.9), channel_id=1, source_target_pairs={{0,24},{8,0},{16,8},{24,16},{1,25},{9,1},{17,9},{25,17},{2,26},{10... | collective-permute-start | bytes 1572872 | tf_op jit(solution)/shard_map/ppermute | solution.py:37
  151.2 10.9 %collective-permute-done.13.w3_ref = bf16[2048,128]{1,0:T(8,128)(2,1)S(1)} collective-permute-done((bf16[2048,128]{1,0:T(8,128)(2,1)S(1)}, bf16[2048,128]{1,0:T(8,128)(2,1)S(1)}, u32[]{:S(2)}, u32[]{:S(2)}) %collective-permute-start.13) | collective-permute-done | bytes 524320 | tf_op jit(solution)/shard_map/ppermute | solution.py:37
  162.2 2.7 %collective-permute-start.15 = (bf16[1024,128]{1,0:T(8,128)(2,1)S(1)}, bf16[1024,128]{1,0:T(8,128)(2,1)S(1)}, u32[]{:S(2)}, u32[]{:S(2)}) collective-permute-start(bf16[1024,128]{1,0:T(8,128)(2,1)S(1)} %slice.100), channel_id=1, source_target_pairs={{0,24},{8,0},{16,8},{24,16},{1,25},{9,1},{17,9},{25,17},{2,26},{10... | collective-permute-start | bytes 786440 | tf_op jit(solution)/shard_map/ppermute | solution.py:37
  165.0 4.3 %collective-permute-done.14.w2a_ref = bf16[1024,128]{1,0:T(8,128)(2,1)S(1)} collective-permute-done((bf16[1024,128]{1,0:T(8,128)(2,1)S(1)}, bf16[1024,128]{1,0:T(8,128)(2,1)S(1)}, u32[]{:S(2)}, u32[]{:S(2)}) %collective-permute-start.14) | collective-permute-done | bytes 262176 | tf_op jit(solution)/shard_map/ppermute | solution.py:37
  170.8 3.6 %down.1 = bf16[4,8,16,128]{3,2,1,0:T(8,128)(2,1)} custom-call(bf16[8,128,256]{2,1,0:T(8,128)(2,1)} %copy-done.2, bf16[16,512]{1,0:T(8,128)(2,1)} %copy-done.14, bf16[2048,128]{1,0:T(8,128)(2,1)} %w0_ref.1, bf16[2048,128]{1,0:T(8,128)(2,1)} %copy-done.6, bf16[1024,128]{1,0:T(8,128)(2,1)} %copy-done.12, bf16[1024,128]{1,0:T(8,128)(2,1)} %copy-done.13, ...), custom_call_target="tpu_custom_call" | custom-call | tf_op jit(solution)/shard_map/down/pallas_call | solution.py:244
  174.4 8.1 %all-to-all-start.7 = ((bf16[32,16,128]{2,1,0:T(8,128)(2,1)}), bf16[32,16,128]{2,1,0:T(8,128)(2,1)S(1)}, u32[]{:S(2)}, u32[]{:S(2)}) async-start(bf16[32,16,128]{2,1,0:T(8,128)(2,1)} %bitcast.62), calls=%async_computation.7 | async-start | bytes 262144 | tf_op jit(solution)/shard_map/all_to_all | solution.py:23
  182.6 4.0 %multiply_add_fusion = f32[16,2,128,256]{3,2,1,0:T(8,128)} fusion(f32[16,2,128,256]{3,2,1,0:T(8,128)} %param.15, f32[16,2,256]{2,1,0:T(2,128)S(1)} %reshape.188, f32[16,2,128]{2,1,0:T(2,128)S(1)} %copy.64, f32[2]{0:T(128)S(1)} %exponential_subtract_fusion), kind=kLoop, calls=%fused_computation | loop fusion | flops 3145728 | bytes 8437768 | tf_op jit(solution)/shard_map/add | solution.py:213
  186.5 3.6 %all-to-all-done.7 = bf16[32,16,128]{2,1,0:T(8,128)(2,1)S(1)} async-done(((bf16[32,16,128]{2,1,0:T(8,128)(2,1)}), bf16[32,16,128]{2,1,0:T(8,128)(2,1)S(1)}, u32[]{:S(2)}, u32[]{:S(2)}) %all-to-all-start.7) | async-done | bytes 131104 | tf_op jit(solution)/shard_map/all_to_all | solution.py:23
  (114 shorter events, 19.7 us)
Async XLA Ops:
  2.0 16.2 %all-to-all-start = ((bf16[32,16,128]{2,1,0:T(8,128)(2,1)}), bf16[32,16,128]{2,1,0:T(8,128)(2,1)S(1)}, u32[]{:S(2)}, u32[]{:S(2)}) async-start(bf16[32,16,128]{2,1,0:T(8,128)(2,1)} %bitcast.1), calls=%async_computation | async-start | bytes 262144 | tf_op jit(solution)/shard_map/all_to_all | solution.py:23
  11.7 14.8 %collective-permute-start = (bf16[128,1536]{1,0:T(8,128)(2,1)S(1)}, bf16[128,1536]{1,0:T(8,128)(2,1)S(1)}, u32[]{:S(2)}, u32[]{:S(2)}) collective-permute-start(bf16[128,1536]{1,0:T(8,128)(2,1)S(1)} %multiply_convert_fusion.1), channel_id=1, source_target_pairs={{0,8},{8,16},{16,24},{24,0},{1,9},{9,17},{17,25},{25,1},{2,10},{10... | collective-permute-start | bytes 1179656 | tf_op jit(solution)/shard_map/ppermute | solution.py:37
  13.2 10.8 %collective-permute-start.1 = (bf16[128,1536]{1,0:T(8,128)(2,1)S(1)}, bf16[128,1536]{1,0:T(8,128)(2,1)S(1)}, u32[]{:S(2)}, u32[]{:S(2)}) collective-permute-start(bf16[128,1536]{1,0:T(8,128)(2,1)S(1)} %multiply_convert_fusion.1), channel_id=1, source_target_pairs={{0,24},{8,0},{16,8},{24,16},{1,25},{9,1},{17,9},{25,17},{2,26},{10... | collective-permute-start | bytes 1179656 | tf_op jit(solution)/shard_map/ppermute | solution.py:37
  19.0 23.4 %copy-start.15 = (bf16[512,128]{1,0:T(8,128)(2,1)S(1)}, bf16[512,128]{1,0:T(8,128)(2,1)}, u32[]{:S(2)}) copy-start(bf16[512,128]{1,0:T(8,128)(2,1)} %param.22) | copy-start | bytes 393220
  19.0 26.2 %copy-start.18 = (s32[16]{0:T(128)S(1)}, s32[16]{0:T(128)}, u32[]{:S(2)}) copy-start(s32[16]{0:T(128)} %param.14) | copy-start | bytes 196
  24.0 5.7 %collective-permute-start.3 = (bf16[128,768]{1,0:T(8,128)(2,1)S(1)}, bf16[128,768]{1,0:T(8,128)(2,1)S(1)}, u32[]{:S(2)}, u32[]{:S(2)}) collective-permute-start(bf16[128,768]{1,0:T(8,128)(2,1)S(1)} %slice.86), channel_id=1, source_target_pairs={{0,24},{8,0},{16,8},{24,16},{1,25},{9,1},{17,9},{25,17},{2,26},{10... | collective-permute-start | bytes 589832 | tf_op jit(solution)/shard_map/ppermute | solution.py:37
  26.5 6.4 %collective-permute-start.2 = (bf16[128,768]{1,0:T(8,128)(2,1)S(1)}, bf16[128,768]{1,0:T(8,128)(2,1)S(1)}, u32[]{:S(2)}, u32[]{:S(2)}) collective-permute-start(bf16[128,768]{1,0:T(8,128)(2,1)S(1)} %slice.85), channel_id=1, source_target_pairs={{0,8},{8,16},{16,24},{24,0},{1,9},{9,17},{17,25},{25,1},{2,10},{10... | collective-permute-start | bytes 589832 | tf_op jit(solution)/shard_map/ppermute | solution.py:37
  33.4 25.6 %copy-start.16 = (f32[512]{0:T(512)S(1)}, f32[512]{0:T(512)}, u32[]{:S(2)}) copy-start(f32[512]{0:T(512)} %param.21) | copy-start | bytes 6148
  34.2 20.9 %all-to-all-start.1 = ((bf16[8,16,1538]{2,1,0:T(8,128)(2,1)}), bf16[8,16,1538]{2,1,0:T(8,128)(2,1)S(1)}, u32[]{:S(2)}, u32[]{:S(2)}) async-start(bf16[8,16,1538]{2,1,0:T(8,128)(2,1)} %concatenate.28), calls=%async_computation.1 | async-start | bytes 851968 | tf_op jit(solution)/shard_map/all_to_all | solution.py:23
  42.4 20.7 %collective-permute-start.6 = (bf16[512,128]{1,0:T(8,128)(2,1)S(1)}, bf16[512,128]{1,0:T(8,128)(2,1)S(1)}, u32[]{:S(2)}, u32[]{:S(2)}) collective-permute-start(bf16[512,128]{1,0:T(8,128)(2,1)S(1)} %copy-done.15), channel_id=1, source_target_pairs={{0,8},{8,16},{16,24},{24,0},{1,9},{9,17},{17,25},{25,1},{2,10},{10... | collective-permute-start | bytes 393224 | tf_op jit(solution)/shard_map/ppermute | solution.py:37
  42.5 20.6 %collective-permute-start.5 = (bf16[512,128]{1,0:T(8,128)(2,1)S(1)}, bf16[512,128]{1,0:T(8,128)(2,1)S(1)}, u32[]{:S(2)}, u32[]{:S(2)}) collective-permute-start(bf16[512,128]{1,0:T(8,128)(2,1)S(1)} %copy-done.15), channel_id=1, source_target_pairs={{0,16},{8,24},{16,0},{24,8},{1,17},{9,25},{17,1},{25,9},{2,18},{10... | collective-permute-start | bytes 393224 | tf_op jit(solution)/shard_map/ppermute | solution.py:37
  44.1 19.1 %collective-permute-start.4 = (bf16[512,128]{1,0:T(8,128)(2,1)S(1)}, bf16[512,128]{1,0:T(8,128)(2,1)S(1)}, u32[]{:S(2)}, u32[]{:S(2)}) collective-permute-start(bf16[512,128]{1,0:T(8,128)(2,1)S(1)} %copy-done.15), channel_id=1, source_target_pairs={{0,24},{8,0},{16,8},{24,16},{1,25},{9,1},{17,9},{25,17},{2,26},{10... | collective-permute-start | bytes 393224 | tf_op jit(solution)/shard_map/ppermute | solution.py:37
  45.4 34.5 %copy-start.8 = (bf16[128,2048]{1,0:T(8,128)(2,1)S(1)}, bf16[128,2048]{1,0:T(8,128)(2,1)}, u32[]{:S(2)}) copy-start(bf16[128,2048]{1,0:T(8,128)(2,1)} %param.24) | copy-start | bytes 1572868
  45.4 34.5 %copy-start.17 = (f32[128]{0:T(128)S(1)}, f32[128]{0:T(128)}, u32[]{:S(2)}) copy-start(f32[128]{0:T(128)} %param.23) | copy-start | bytes 1540
  59.8 11.3 %all-to-all-start.2 = ((bf16[8,16,512]{2,1,0:T(8,128)(2,1)}), bf16[8,16,512]{2,1,0:T(8,128)(2,1)S(1)}, u32[]{:S(2)}, u32[]{:S(2)}) async-start(bf16[8,16,512]{2,1,0:T(8,128)(2,1)} %broadcast_in_dim.10), calls=%async_computation.2 | async-start | bytes 262144 | tf_op jit(solution)/shard_map/all_to_all | solution.py:23
  71.9 13.3 %all-to-all-start.3 = ((bf16[8,16,512]{2,1,0:T(8,128)(2,1)}), bf16[8,16,512]{2,1,0:T(8,128)(2,1)S(1)}, u32[]{:S(2)}, u32[]{:S(2)}) async-start(bf16[8,16,512]{2,1,0:T(8,128)(2,1)} %bitcast.12), calls=%async_computation.3 | async-start | bytes 262144 | tf_op jit(solution)/shard_map/all_to_all | solution.py:23
  85.2 63.2 %copy-start.9 = (bf16[2048,128]{1,0:T(8,128)(2,1)S(1)}, bf16[2048,128]{1,0:T(8,128)(2,1)}, u32[]{:S(2)}) copy-start(bf16[2048,128]{1,0:T(8,128)(2,1)} %w0_ref.1) | copy-start | bytes 1572868
  85.2 21.5 %all-to-all-start.5 = ((bf16[8,256,128]{2,1,0:T(8,128)(2,1)}), bf16[8,256,128]{2,1,0:T(8,128)(2,1)S(1)}, u32[]{:S(2)}, u32[]{:S(2)}) async-start(bf16[8,256,128]{2,1,0:T(8,128)(2,1)} %bitcast.15), calls=%async_computation.5 | async-start | bytes 1048576 | tf_op jit(solution)/shard_map/all_to_all | solution.py:23
  88.9 73.3 %copy-start.14 = (bf16[16,512]{1,0:T(8,128)(2,1)}, bf16[16,512]{1,0:T(8,128)(2,1)S(1)}, u32[]{:S(2)}) copy-start(bf16[16,512]{1,0:T(8,128)(2,1)S(1)} %fusion.3.resid_ref) | copy-start | bytes 49156
  106.7 33.3 %copy-start = (bf16[8,256,128]{2,1,0:T(8,128)(2,1)}, bf16[8,256,128]{2,1,0:T(8,128)(2,1)S(1)}, u32[]{:S(2)}) copy-start(bf16[8,256,128]{2,1,0:T(8,128)(2,1)S(1)} %all-to-all-done.5.w0_ref) | copy-start | bytes 1572868
  107.7 17.9 %all-to-all-start.4 = ((bf16[32,16,512]{2,1,0:T(8,128)(2,1)}), bf16[32,16,512]{2,1,0:T(8,128)(2,1)S(1)}, u32[]{:S(2)}, u32[]{:S(2)}) async-start(bf16[32,16,512]{2,1,0:T(8,128)(2,1)} %broadcast_in_dim.11), calls=%async_computation.4 | async-start | bytes 1048576 | tf_op jit(solution)/shard_map/all_to_all | solution.py:23
  111.6 17.7 %collective-permute-start.9 = (bf16[8,256,128]{2,1,0:T(8,128)(2,1)S(1)}, bf16[8,256,128]{2,1,0:T(8,128)(2,1)S(1)}, u32[]{:S(2)}, u32[]{:S(2)}) collective-permute-start(bf16[8,256,128]{2,1,0:T(8,128)(2,1)S(1)} %all-to-all-done.5.w0_ref), channel_id=1, source_target_pairs={{0,8},{8,16},{16,24},{24,0},{1,9},{9,17},{17,25},{25,1},{2,10},{10... | collective-permute-start | bytes 1572872 | tf_op jit(solution)/shard_map/ppermute | solution.py:37
  111.7 17.9 %collective-permute-start.8 = (bf16[8,256,128]{2,1,0:T(8,128)(2,1)S(1)}, bf16[8,256,128]{2,1,0:T(8,128)(2,1)S(1)}, u32[]{:S(2)}, u32[]{:S(2)}) collective-permute-start(bf16[8,256,128]{2,1,0:T(8,128)(2,1)S(1)} %all-to-all-done.5.w0_ref), channel_id=1, source_target_pairs={{0,24},{8,0},{16,8},{24,16},{1,25},{9,1},{17,9},{25,17},{2,26},{10... | collective-permute-start | bytes 1572872 | tf_op jit(solution)/shard_map/ppermute | solution.py:37
  125.6 14.4 %collective-permute-start.7 = (bf16[4,8,16,512]{3,2,1,0:T(8,128)(2,1)S(1)}, bf16[4,8,16,512]{3,2,1,0:T(8,128)(2,1)S(1)}, u32[]{:S(2)}, u32[]{:S(2)}) collective-permute-start(bf16[4,8,16,512]{3,2,1,0:T(8,128)(2,1)S(1)} %bitcast.56), channel_id=1, source_target_pairs={{0,1},{1,0},{2,3},{3,2},{4,5},{5,4},{6,7},{7,6},{8,9},{9,8},{10,11... | collective-permute-start | bytes 1572872 | tf_op jit(solution)/shard_map/ppermute | solution.py:41
  129.3 9.3 %collective-permute-start.10 = (bf16[4,256,128]{2,1,0:T(8,128)(2,1)S(1)}, bf16[4,256,128]{2,1,0:T(8,128)(2,1)S(1)}, u32[]{:S(2)}, u32[]{:S(2)}) collective-permute-start(bf16[4,256,128]{2,1,0:T(8,128)(2,1)S(1)} %slice.97), channel_id=1, source_target_pairs={{0,8},{8,16},{16,24},{24,0},{1,9},{9,17},{17,25},{25,1},{2,10},{10... | collective-permute-start | bytes 786440 | tf_op jit(solution)/shard_map/ppermute | solution.py:37
  129.6 9.7 %collective-permute-start.11 = (bf16[4,256,128]{2,1,0:T(8,128)(2,1)S(1)}, bf16[4,256,128]{2,1,0:T(8,128)(2,1)S(1)}, u32[]{:S(2)}, u32[]{:S(2)}) collective-permute-start(bf16[4,256,128]{2,1,0:T(8,128)(2,1)S(1)} %slice.98), channel_id=1, source_target_pairs={{0,24},{8,0},{16,8},{24,16},{1,25},{9,1},{17,9},{25,17},{2,26},{10... | collective-permute-start | bytes 786440 | tf_op jit(solution)/shard_map/ppermute | solution.py:37
  144.2 25.0 %all-to-all-start.6 = ((bf16[8,128,256]{2,1,0:T(8,128)(2,1)}), bf16[8,128,256]{2,1,0:T(8,128)(2,1)S(1)}, u32[]{:S(2)}, u32[]{:S(2)}) async-start(bf16[8,128,256]{2,1,0:T(8,128)(2,1)} %hidden.1), calls=%async_computation.6 | async-start | bytes 1048576 | tf_op jit(solution)/shard_map/all_to_all | solution.py:23
  148.4 13.6 %collective-permute-start.13 = (bf16[2048,128]{1,0:T(8,128)(2,1)S(1)}, bf16[2048,128]{1,0:T(8,128)(2,1)S(1)}, u32[]{:S(2)}, u32[]{:S(2)}) collective-permute-start(bf16[2048,128]{1,0:T(8,128)(2,1)S(1)} %copy-done.9), channel_id=1, source_target_pairs={{0,8},{8,16},{16,24},{24,0},{1,9},{9,17},{17,25},{25,1},{2,10},{10... | collective-permute-start | bytes 1572872 | tf_op jit(solution)/shard_map/ppermute | solution.py:37
  148.5 13.6 %collective-permute-start.12 = (bf16[2048,128]{1,0:T(8,128)(2,1)S(1)}, bf16[2048,128]{1,0:T(8,128)(2,1)S(1)}, u32[]{:S(2)}, u32[]{:S(2)}) collective-permute-start(bf16[2048,128]{1,0:T(8,128)(2,1)S(1)} %copy-done.9), channel_id=1, source_target_pairs={{0,24},{8,0},{16,8},{24,16},{1,25},{9,1},{17,9},{25,17},{2,26},{10... | collective-permute-start | bytes 1572872 | tf_op jit(solution)/shard_map/ppermute | solution.py:37
  162.1 7.1 %collective-permute-start.14 = (bf16[1024,128]{1,0:T(8,128)(2,1)S(1)}, bf16[1024,128]{1,0:T(8,128)(2,1)S(1)}, u32[]{:S(2)}, u32[]{:S(2)}) collective-permute-start(bf16[1024,128]{1,0:T(8,128)(2,1)S(1)} %slice.99), channel_id=1, source_target_pairs={{0,8},{8,16},{16,24},{24,0},{1,9},{9,17},{17,25},{25,1},{2,10},{10... | collective-permute-start | bytes 786440 | tf_op jit(solution)/shard_map/ppermute | solution.py:37
  162.2 7.0 %collective-permute-start.15 = (bf16[1024,128]{1,0:T(8,128)(2,1)S(1)}, bf16[1024,128]{1,0:T(8,128)(2,1)S(1)}, u32[]{:S(2)}, u32[]{:S(2)}) collective-permute-start(bf16[1024,128]{1,0:T(8,128)(2,1)S(1)} %slice.100), channel_id=1, source_target_pairs={{0,24},{8,0},{16,8},{24,16},{1,25},{9,1},{17,9},{25,17},{2,26},{10... | collective-permute-start | bytes 786440 | tf_op jit(solution)/shard_map/ppermute | solution.py:37
  174.4 15.7 %all-to-all-start.7 = ((bf16[32,16,128]{2,1,0:T(8,128)(2,1)}), bf16[32,16,128]{2,1,0:T(8,128)(2,1)S(1)}, u32[]{:S(2)}, u32[]{:S(2)}) async-start(bf16[32,16,128]{2,1,0:T(8,128)(2,1)} %bitcast.62), calls=%async_computation.7 | async-start | bytes 262144 | tf_op jit(solution)/shard_map/all_to_all | solution.py:23
  (11 other events, 54.4 us)

commit v8 on v7

--- a/solution.py
+++ b/solution.py
@@ -57,7 +57,7 @@
     return 1.0 - jnp.exp2(-2.0 - 6.0 * head_ids / (H - 1))
 
 
-STEP = 2
+STEP = 4
 
 
 def hidden_kernel(own_ref, other_ref, w0_ref, w1_ref, w2a_ref, w2b_ref, w3_ref, out_ref, x_ref, w_ref, x_sem, w_sem):
@@ -93,8 +93,7 @@
     scale = lax.rsqrt(jnp.sum(squares, axis=1, keepdims=True) / D + EPS)
     positive = jnp.maximum(hidden * scale, 0.0)
     active = (positive * positive).astype(jnp.bfloat16)
-    for z in range(NZ):
-        out_ref[z] = active
+    out_ref[...] = active
 
 
 def down_kernel(act_ref, resid_ref, w0_ref, w1_ref, w2a_ref, w2b_ref, w3_ref, out_ref, a_ref, w_ref, a_sem, w_sem):
@@ -209,8 +208,6 @@
     mixed = (
         read.reshape(local_rows, heads_dev * DV) * head_gain[None, :] * jax.nn.silu(gates)
     ).astype(jnp.bfloat16)
-    mixed, old, left, right = lax.optimization_barrier((mixed, state, turned_keys, values))
-    new_state = decay[..., None] * old + left[..., None] * right[:, :, None, :]
     mixed_all = copy_for_each(mixed, "z").reshape(128, heads_dev * DV)
     attn_terms = term(mixed_all, out_wide).astype(jnp.bfloat16)
     attn = summed_on_arrival(attn_terms.reshape(NX * NC, 16, 512), TP)
@@ -230,7 +227,7 @@
     anywhere = pl.BlockSpec(memory_space=pl.ANY)
     active = pl.pallas_call(
         hidden_kernel,
-        out_shape=jax.ShapeDtypeStruct((NZ, 128, 256), jnp.bfloat16),
+        out_shape=jax.ShapeDtypeStruct((128, 256), jnp.bfloat16),
         in_specs=[anywhere] * 7,
         scratch_shapes=[
             pltpu.VMEM((NC, NX, NZ, 16, 512), jnp.bfloat16),
@@ -240,7 +237,8 @@
         ],
         name="hidden",
     )(own, other, mixer, mix_above, far_low, far_high, mix_below)
-    active = exchanged(active, "z")
+    active, down_low, down_high = lax.optimization_barrier((active, down_low, down_high))
+    active = copy_for_each(active, "z").reshape(NZ, 128, 256)
     partial = pl.pallas_call(
         down_kernel,
         out_shape=jax.ShapeDtypeStruct((NY, NX * NC, 16, 128), jnp.bfloat16),
@@ -253,6 +251,8 @@
         ],
         name="down",
     )(active, resid, down_weight, down_above, down_low, down_high, down_below)
+    partial, old, left, right = lax.optimization_barrier((partial, state, turned_keys, values))
+    new_state = decay[..., None] * old + left[..., None] * right[:, :, None, :]
     partial = exchanged(partial.reshape(NY * NX * NC, 16, 128), ("y", "x", "c"))
     output = jnp.sum(partial.reshape(NY, NX * NC, 16, 128).astype(jnp.float32), axis=1)
     output = output.astype(jnp.bfloat16).reshape(64, 128)

time: 192 us -> 195 us (1.016)
  blocking collectives: 0 us -> 20.1 us
  waiting for transfers between devices: 89.9 us -> 78.3 us
  starting transfers between devices: 71.1 us -> 68.2 us
    all_to_all x0 -> x1, blocking collectives: none -> 20.1 us  [exchanged(): return lax.all_to_all(blocks, axis, split_axis=0, concat_axis=0, tiled=True)]
    ppermute x15, waiting for transfers between devices: 32.2 us -> 22.2 us  [shifted(): lax.ppermute(array, axis, [(i, (i + by) % size) for i in range(size)])]
    unnamed x44 -> x30, local copies, waits for them, and re-layouts: 3.99 us -> 0.23 us
    all_to_all x8 -> x7, waiting for transfers between devices: 57.6 us -> 56.1 us  [exchanged(): return lax.all_to_all(blocks, axis, split_axis=0, concat_axis=0, tiled=True)]
    all_to_all x8 -> x7, starting transfers between devices: 48 us -> 46.8 us  [exchanged(): return lax.all_to_all(blocks, axis, split_axis=0, concat_axis=0, tiled=True)]
  transfers between devices with their start and end apart: 24 -> 23, of which waited for: 13 -> 13; matrix products, arithmetic and copies ran while one was open for 7% -> 7% of each run, Pallas kernels for 0% -> 2%
where the time goes in v8:
time: 195 us
  waiting for transfers between devices  78.3 us (40%)
  starting transfers between devices  68.2 us (35%)
  blocking collectives  20.1 us (10%)
  other arithmetic  9.73 us (5%)
  local copies, waits for them, and re-layouts  8.55 us (4%)
  Pallas kernels  6.51 us (3%)
  matrix products  2 us (1%)
    all_to_all x7, waiting for transfers between devices, exchanged(): return lax.all_to_all(blocks, axis, split_axis=0, concat_axis=0, tiled=True)  56.1 us
    all_to_all x7, starting transfers between devices, exchanged(): return lax.all_to_all(blocks, axis, split_axis=0, concat_axis=0, tiled=True)  46.8 us
    ppermute x15, waiting for transfers between devices, shifted(): lax.ppermute(array, axis, [(i, (i + by) % size) for i in range(size)])  22.2 us
    all_to_all x1, blocking collectives, exchanged(): return lax.all_to_all(blocks, axis, split_axis=0, concat_axis=0, tiled=True)  20.1 us
    ppermute x15, starting transfers between devices, shifted(): lax.ppermute(array, axis, [(i, (i + by) % size) for i in range(size)])  17.8 us
    add x1, other arithmetic, local(): new_state = decay[..., None] * old + left[..., None] * right[:, :, None, :]  3.96 us
  transfers between devices with their start and end apart: 23, of which 13 were waited for; matrix products, arithmetic and copies ran while one was open for 7% of the time, Pallas kernels for 2%

profile of v8, /device:TPU:1, one launch (start us, length us, event | category | flops | bytes accessed | tf_op | source)
XLA Modules:
  0.0 194.6 jit_solution(10396720825115396201)
XLA Ops:
  2.0 8.6 %all-to-all-start = ((bf16[32,16,128]{2,1,0:T(8,128)(2,1)}), bf16[32,16,128]{2,1,0:T(8,128)(2,1)S(1)}, u32[]{:S(2)}, u32[]{:S(2)}) async-start(bf16[32,16,128]{2,1,0:T(8,128)(2,1)} %bitcast.1), calls=%async_computation | async-start | bytes 262144 | tf_op jit(solution)/shard_map/all_to_all | solution.py:23
  11.7 1.4 collective-permute-start
  14.5 3.7 %all-to-all-done = bf16[32,16,128]{2,1,0:T(8,128)(2,1)S(1)} async-done(((bf16[32,16,128]{2,1,0:T(8,128)(2,1)}), bf16[32,16,128]{2,1,0:T(8,128)(2,1)S(1)}, u32[]{:S(2)}, u32[]{:S(2)}) %all-to-all-start) | async-done | bytes 131104 | tf_op jit(solution)/shard_map/all_to_all | solution.py:23
  19.0 5.0 %collective-permute-done.1 = bf16[128,1536]{1,0:T(8,128)(2,1)S(1)} collective-permute-done((bf16[128,1536]{1,0:T(8,128)(2,1)S(1)}, bf16[128,1536]{1,0:T(8,128)(2,1)S(1)}, u32[]{:S(2)}, u32[]{:S(2)}) %collective-permute-start.1) | collective-permute-done | bytes 393248 | tf_op jit(solution)/shard_map/ppermute | solution.py:37
  24.0 2.5 %collective-permute-start.3 = (bf16[128,768]{1,0:T(8,128)(2,1)S(1)}, bf16[128,768]{1,0:T(8,128)(2,1)S(1)}, u32[]{:S(2)}, u32[]{:S(2)}) collective-permute-start(bf16[128,768]{1,0:T(8,128)(2,1)S(1)} %slice.86), channel_id=1, source_target_pairs={{0,24},{8,0},{16,8},{24,16},{1,25},{9,1},{17,9},{25,17},{2,26},{10... | collective-permute-start | bytes 589832 | tf_op jit(solution)/shard_map/ppermute | solution.py:37
  26.9 2.8 %collective-permute-done.3 = bf16[128,768]{1,0:T(8,128)(2,1)S(1)} collective-permute-done((bf16[128,768]{1,0:T(8,128)(2,1)S(1)}, bf16[128,768]{1,0:T(8,128)(2,1)S(1)}, u32[]{:S(2)}, u32[]{:S(2)}) %collective-permute-start.3) | collective-permute-done | bytes 196640 | tf_op jit(solution)/shard_map/ppermute | solution.py:37
  29.9 3.0 %collective-permute-done.2 = bf16[128,768]{1,0:T(8,128)(2,1)S(1)} collective-permute-done((bf16[128,768]{1,0:T(8,128)(2,1)S(1)}, bf16[128,768]{1,0:T(8,128)(2,1)S(1)}, u32[]{:S(2)}, u32[]{:S(2)}) %collective-permute-start.2) | collective-permute-done | bytes 196640 | tf_op jit(solution)/shard_map/ppermute | solution.py:37
  34.2 8.2 %all-to-all-start.1 = ((bf16[8,16,1538]{2,1,0:T(8,128)(2,1)}), bf16[8,16,1538]{2,1,0:T(8,128)(2,1)S(1)}, u32[]{:S(2)}, u32[]{:S(2)}) async-start(bf16[8,16,1538]{2,1,0:T(8,128)(2,1)} %concatenate.28), calls=%async_computation.1 | async-start | bytes 851968 | tf_op jit(solution)/shard_map/all_to_all | solution.py:23
  42.5 1.6 collective-permute-start.5
  45.5 9.7 %all-to-all-done.1 = bf16[8,16,1538]{2,1,0:T(8,128)(2,1)S(1)} async-done(((bf16[8,16,1538]{2,1,0:T(8,128)(2,1)}), bf16[8,16,1538]{2,1,0:T(8,128)(2,1)S(1)}, u32[]{:S(2)}, u32[]{:S(2)}) %all-to-all-start.1) | async-done | bytes 393760 | tf_op jit(solution)/shard_map/all_to_all | solution.py:23
  56.0 2.6 %multiply_reduce_fusion = f32[16,2,256]{2,1,0:T(2,128)S(1)} fusion(f32[16,2,128,256]{3,2,1,0:T(8,128)} %param.15, f32[16,2,128]{2,1,0:T(2,128)S(1)} %copy.59), kind=kLoop, calls=%fused_computation.1 | loop fusion | flops 2088960 | bytes 4243456 | tf_op jit(solution)/shard_map/reduce_sum | solution.py:206
  59.8 3.4 %all-to-all-start.2 = ((bf16[8,16,512]{2,1,0:T(8,128)(2,1)}), bf16[8,16,512]{2,1,0:T(8,128)(2,1)S(1)}, u32[]{:S(2)}, u32[]{:S(2)}) async-start(bf16[8,16,512]{2,1,0:T(8,128)(2,1)} %broadcast_in_dim.12), calls=%async_computation.2 | async-start | bytes 262144 | tf_op jit(solution)/shard_map/all_to_all | solution.py:23
  63.3 7.8 %all-to-all-done.2 = bf16[8,16,512]{2,1,0:T(8,128)(2,1)S(1)} async-done(((bf16[8,16,512]{2,1,0:T(8,128)(2,1)}), bf16[8,16,512]{2,1,0:T(8,128)(2,1)S(1)}, u32[]{:S(2)}, u32[]{:S(2)}) %all-to-all-start.2) | async-done | bytes 131104 | tf_op jit(solution)/shard_map/all_to_all | solution.py:23
  71.9 8.1 %all-to-all-start.3 = ((bf16[8,16,512]{2,1,0:T(8,128)(2,1)}), bf16[8,16,512]{2,1,0:T(8,128)(2,1)S(1)}, u32[]{:S(2)}, u32[]{:S(2)}) async-start(bf16[8,16,512]{2,1,0:T(8,128)(2,1)} %bitcast.12), calls=%async_computation.3 | async-start | bytes 262144 | tf_op jit(solution)/shard_map/all_to_all | solution.py:23
  81.4 3.8 %all-to-all-done.3 = bf16[8,16,512]{2,1,0:T(8,128)(2,1)S(1)} async-done(((bf16[8,16,512]{2,1,0:T(8,128)(2,1)}), bf16[8,16,512]{2,1,0:T(8,128)(2,1)S(1)}, u32[]{:S(2)}, u32[]{:S(2)}) %all-to-all-start.3) | async-done | bytes 131104 | tf_op jit(solution)/shard_map/all_to_all | solution.py:23
  85.2 3.5 %all-to-all-start.5 = ((bf16[8,256,128]{2,1,0:T(8,128)(2,1)}), bf16[8,256,128]{2,1,0:T(8,128)(2,1)S(1)}, u32[]{:S(2)}, u32[]{:S(2)}) async-start(bf16[8,256,128]{2,1,0:T(8,128)(2,1)} %bitcast.15), calls=%async_computation.5 | async-start | bytes 1048576 | tf_op jit(solution)/shard_map/all_to_all | solution.py:23
  88.8 17.8 %all-to-all-done.5.w0_ref = bf16[8,256,128]{2,1,0:T(8,128)(2,1)S(1)} async-done(((bf16[8,256,128]{2,1,0:T(8,128)(2,1)}), bf16[8,256,128]{2,1,0:T(8,128)(2,1)S(1)}, u32[]{:S(2)}, u32[]{:S(2)}) %all-to-all-start.5) | async-done | bytes 524320 | tf_op jit(solution)/shard_map/all_to_all | solution.py:23
  107.6 3.9 %all-to-all-start.4 = ((bf16[32,16,512]{2,1,0:T(8,128)(2,1)}), bf16[32,16,512]{2,1,0:T(8,128)(2,1)S(1)}, u32[]{:S(2)}, u32[]{:S(2)}) async-start(bf16[32,16,512]{2,1,0:T(8,128)(2,1)} %broadcast_in_dim.13), calls=%async_computation.4 | async-start | bytes 1048576 | tf_op jit(solution)/shard_map/all_to_all | solution.py:23
  111.6 2.7 %collective-permute-start.8 = (bf16[8,256,128]{2,1,0:T(8,128)(2,1)S(1)}, bf16[8,256,128]{2,1,0:T(8,128)(2,1)S(1)}, u32[]{:S(2)}, u32[]{:S(2)}) collective-permute-start(bf16[8,256,128]{2,1,0:T(8,128)(2,1)S(1)} %all-to-all-done.5.w0_ref), channel_id=1, source_target_pairs={{0,24},{8,0},{16,8},{24,16},{1,25},{9,1},{17,9},{25,17},{2,26},{10... | collective-permute-start | bytes 1572872 | tf_op jit(solution)/shard_map/ppermute | solution.py:37
  115.7 9.8 %all-to-all-done.4 = bf16[32,16,512]{2,1,0:T(8,128)(2,1)S(1)} async-done(((bf16[32,16,512]{2,1,0:T(8,128)(2,1)}), bf16[32,16,512]{2,1,0:T(8,128)(2,1)S(1)}, u32[]{:S(2)}, u32[]{:S(2)}) %all-to-all-start.4) | async-done | bytes 524320 | tf_op jit(solution)/shard_map/all_to_all | solution.py:23
  125.5 3.7 %collective-permute-start.7 = (bf16[4,8,16,512]{3,2,1,0:T(8,128)(2,1)S(1)}, bf16[4,8,16,512]{3,2,1,0:T(8,128)(2,1)}, u32[]{:S(2)}, u32[]{:S(2)}) collective-permute-start(bf16[4,8,16,512]{3,2,1,0:T(8,128)(2,1)S(1)} %bitcast.56), channel_id=1, source_target_pairs={{0,1},{1,0},{2,3},{3,2},{4,5},{5,4},{6,7},{7,6},{8,9},{9,8},{10,11... | collective-permute-start | bytes 1572872 | tf_op jit(solution)/shard_map/ppermute | solution.py:41
  129.9 7.3 %collective-permute-done.9.w3_ref = bf16[8,256,128]{2,1,0:T(8,128)(2,1)S(1)} collective-permute-done((bf16[8,256,128]{2,1,0:T(8,128)(2,1)S(1)}, bf16[8,256,128]{2,1,0:T(8,128)(2,1)S(1)}, u32[]{:S(2)}, u32[]{:S(2)}) %collective-permute-start.9) | collective-permute-done | bytes 524320 | tf_op jit(solution)/shard_map/ppermute | solution.py:37
  137.4 2.7 %collective-permute-start.11 = (bf16[4,256,128]{2,1,0:T(8,128)(2,1)S(1)}, bf16[4,256,128]{2,1,0:T(8,128)(2,1)}, u32[]{:S(2)}, u32[]{:S(2)}) collective-permute-start(bf16[4,256,128]{2,1,0:T(8,128)(2,1)S(1)} %slice.98), channel_id=1, source_target_pairs={{0,24},{8,0},{16,8},{24,16},{1,25},{9,1},{17,9},{25,17},{2,26},{10... | collective-permute-start | bytes 786440 | tf_op jit(solution)/shard_map/ppermute | solution.py:37
  140.9 2.7 %collective-permute-start.15 = (bf16[1024,128]{1,0:T(8,128)(2,1)}, bf16[1024,128]{1,0:T(8,128)(2,1)}, u32[]{:S(2)}, u32[]{:S(2)}) collective-permute-start(bf16[1024,128]{1,0:T(8,128)(2,1)} %slice.100), channel_id=1, source_target_pairs={{0,24},{8,0},{16,8},{24,16},{1,25},{9,1},{17,9},{25,17},{2,26},{10... | collective-permute-start | bytes 786440 | tf_op jit(solution)/shard_map/ppermute | solution.py:37
  143.5 1.6 collective-permute-done.10.w2a_ref
  145.2 3.1 %hidden.1 = bf16[128,256]{1,0:T(8,128)(2,1)} custom-call(bf16[4,8,16,512]{3,2,1,0:T(8,128)(2,1)} %bitcast.57, bf16[4,8,16,512]{3,2,1,0:T(8,128)(2,1)} %collective-permute-done.7.other_ref, bf16[8,256,128]{2,1,0:T(8,128)(2,1)} %copy-done, bf16[8,256,128]{2,1,0:T(8,128)(2,1)} %copy-done.3, bf16[4,256,128]{2,1,0:T(8,128)(2,1)} %collective-permute-done.10.w2a_ref, ...), custom_call_target="tpu_custom_call" | custom-call | tf_op jit(solution)/shard_map/hidden/pallas_call | solution.py:228
  148.3 2.5 %collective-permute-done.13.w2a_ref = bf16[1024,128]{1,0:T(8,128)(2,1)} collective-permute-done((bf16[1024,128]{1,0:T(8,128)(2,1)}, bf16[1024,128]{1,0:T(8,128)(2,1)}, u32[]{:S(2)}, u32[]{:S(2)}) %collective-permute-start.13) | collective-permute-done | bytes 262176 | tf_op jit(solution)/shard_map/ppermute | solution.py:37
  151.6 20.1 %all_to_all.40.act_ref = bf16[8,128,256]{2,1,0:T(8,128)(2,1)} all-to-all(bf16[8,128,256]{2,1,0:T(8,128)(2,1)S(1)} %broadcast_in_dim.14), channel_id=1, replica_groups=mesh['z'=8,'y'=4,'x'=4,'c'=2] {'z'}, dimensions={0} | all-to-all | bytes 1048576 | tf_op jit(solution)/shard_map/all_to_all | solution.py:23
  171.7 3.4 %down.1 = bf16[4,8,16,128]{3,2,1,0:T(8,128)(2,1)} custom-call(bf16[8,128,256]{2,1,0:T(8,128)(2,1)} %all_to_all.40.act_ref, bf16[16,512]{1,0:T(8,128)(2,1)} %copy-done.7, bf16[2048,128]{1,0:T(8,128)(2,1)} %w0_ref.1, bf16[2048,128]{1,0:T(8,128)(2,1)} %copy-done.5, bf16[1024,128]{1,0:T(8,128)(2,1)} %collective-permute-done.13.w2a_ref, ...), custom_call_target="tpu_custom_call" | custom-call | tf_op jit(solution)/shard_map/down/pallas_call | solution.py:242
  175.1 11.2 %all-to-all-start.7 = ((bf16[32,16,128]{2,1,0:T(8,128)(2,1)}), bf16[32,16,128]{2,1,0:T(8,128)(2,1)S(1)}, u32[]{:S(2)}, u32[]{:S(2)}) async-start(bf16[32,16,128]{2,1,0:T(8,128)(2,1)} %bitcast.62), calls=%async_computation.7 | async-start | bytes 262144 | tf_op jit(solution)/shard_map/all_to_all | solution.py:23
  186.4 4.0 %multiply_add_fusion = f32[16,2,128,256]{3,2,1,0:T(8,128)} fusion(f32[16,2,128,256]{3,2,1,0:T(8,128)} %param.15, f32[16,2,256]{2,1,0:T(2,128)S(1)} %reshape.188, f32[16,2,128]{2,1,0:T(2,128)S(1)} %copy.64, f32[2]{0:T(128)S(1)} %exponential_subtract_fusion), kind=kLoop, calls=%fused_computation | loop fusion | flops 3145728 | bytes 8437768 | tf_op jit(solution)/shard_map/add | solution.py:255
  190.3 3.6 %all-to-all-done.7 = bf16[32,16,128]{2,1,0:T(8,128)(2,1)S(1)} async-done(((bf16[32,16,128]{2,1,0:T(8,128)(2,1)}), bf16[32,16,128]{2,1,0:T(8,128)(2,1)S(1)}, u32[]{:S(2)}, u32[]{:S(2)}) %all-to-all-start.7) | async-done | bytes 131104 | tf_op jit(solution)/shard_map/all_to_all | solution.py:23
  (100 shorter events, 18.0 us)
Async XLA Ops:
  2.0 16.2 %all-to-all-start = ((bf16[32,16,128]{2,1,0:T(8,128)(2,1)}), bf16[32,16,128]{2,1,0:T(8,128)(2,1)S(1)}, u32[]{:S(2)}, u32[]{:S(2)}) async-start(bf16[32,16,128]{2,1,0:T(8,128)(2,1)} %bitcast.1), calls=%async_computation | async-start | bytes 262144 | tf_op jit(solution)/shard_map/all_to_all | solution.py:23
  11.7 14.8 %collective-permute-start = (bf16[128,1536]{1,0:T(8,128)(2,1)S(1)}, bf16[128,1536]{1,0:T(8,128)(2,1)S(1)}, u32[]{:S(2)}, u32[]{:S(2)}) collective-permute-start(bf16[128,1536]{1,0:T(8,128)(2,1)S(1)} %multiply_convert_fusion.1), channel_id=1, source_target_pairs={{0,8},{8,16},{16,24},{24,0},{1,9},{9,17},{17,25},{25,1},{2,10},{10... | collective-permute-start | bytes 1179656 | tf_op jit(solution)/shard_map/ppermute | solution.py:37
  13.2 10.8 %collective-permute-start.1 = (bf16[128,1536]{1,0:T(8,128)(2,1)S(1)}, bf16[128,1536]{1,0:T(8,128)(2,1)S(1)}, u32[]{:S(2)}, u32[]{:S(2)}) collective-permute-start(bf16[128,1536]{1,0:T(8,128)(2,1)S(1)} %multiply_convert_fusion.1), channel_id=1, source_target_pairs={{0,24},{8,0},{16,8},{24,16},{1,25},{9,1},{17,9},{25,17},{2,26},{10... | collective-permute-start | bytes 1179656 | tf_op jit(solution)/shard_map/ppermute | solution.py:37
  19.0 23.4 %copy-start.8 = (bf16[512,128]{1,0:T(8,128)(2,1)S(1)}, bf16[512,128]{1,0:T(8,128)(2,1)}, u32[]{:S(2)}) copy-start(bf16[512,128]{1,0:T(8,128)(2,1)} %param.22) | copy-start | bytes 393220
  19.0 26.2 %copy-start.11 = (s32[16]{0:T(128)S(1)}, s32[16]{0:T(128)}, u32[]{:S(2)}) copy-start(s32[16]{0:T(128)} %param.14) | copy-start | bytes 196
  24.0 5.7 %collective-permute-start.3 = (bf16[128,768]{1,0:T(8,128)(2,1)S(1)}, bf16[128,768]{1,0:T(8,128)(2,1)S(1)}, u32[]{:S(2)}, u32[]{:S(2)}) collective-permute-start(bf16[128,768]{1,0:T(8,128)(2,1)S(1)} %slice.86), channel_id=1, source_target_pairs={{0,24},{8,0},{16,8},{24,16},{1,25},{9,1},{17,9},{25,17},{2,26},{10... | collective-permute-start | bytes 589832 | tf_op jit(solution)/shard_map/ppermute | solution.py:37
  26.5 6.4 %collective-permute-start.2 = (bf16[128,768]{1,0:T(8,128)(2,1)S(1)}, bf16[128,768]{1,0:T(8,128)(2,1)S(1)}, u32[]{:S(2)}, u32[]{:S(2)}) collective-permute-start(bf16[128,768]{1,0:T(8,128)(2,1)S(1)} %slice.85), channel_id=1, source_target_pairs={{0,8},{8,16},{16,24},{24,0},{1,9},{9,17},{17,25},{25,1},{2,10},{10... | collective-permute-start | bytes 589832 | tf_op jit(solution)/shard_map/ppermute | solution.py:37
  33.4 25.6 %copy-start.9 = (f32[512]{0:T(512)S(1)}, f32[512]{0:T(512)}, u32[]{:S(2)}) copy-start(f32[512]{0:T(512)} %param.21) | copy-start | bytes 6148
  34.2 20.9 %all-to-all-start.1 = ((bf16[8,16,1538]{2,1,0:T(8,128)(2,1)}), bf16[8,16,1538]{2,1,0:T(8,128)(2,1)S(1)}, u32[]{:S(2)}, u32[]{:S(2)}) async-start(bf16[8,16,1538]{2,1,0:T(8,128)(2,1)} %concatenate.28), calls=%async_computation.1 | async-start | bytes 851968 | tf_op jit(solution)/shard_map/all_to_all | solution.py:23
  42.4 20.7 %collective-permute-start.6 = (bf16[512,128]{1,0:T(8,128)(2,1)S(1)}, bf16[512,128]{1,0:T(8,128)(2,1)S(1)}, u32[]{:S(2)}, u32[]{:S(2)}) collective-permute-start(bf16[512,128]{1,0:T(8,128)(2,1)S(1)} %copy-done.8), channel_id=1, source_target_pairs={{0,8},{8,16},{16,24},{24,0},{1,9},{9,17},{17,25},{25,1},{2,10},{10... | collective-permute-start | bytes 393224 | tf_op jit(solution)/shard_map/ppermute | solution.py:37
  42.5 20.6 %collective-permute-start.5 = (bf16[512,128]{1,0:T(8,128)(2,1)S(1)}, bf16[512,128]{1,0:T(8,128)(2,1)S(1)}, u32[]{:S(2)}, u32[]{:S(2)}) collective-permute-start(bf16[512,128]{1,0:T(8,128)(2,1)S(1)} %copy-done.8), channel_id=1, source_target_pairs={{0,16},{8,24},{16,0},{24,8},{1,17},{9,25},{17,1},{25,9},{2,18},{10... | collective-permute-start | bytes 393224 | tf_op jit(solution)/shard_map/ppermute | solution.py:37
  44.1 19.1 %collective-permute-start.4 = (bf16[512,128]{1,0:T(8,128)(2,1)S(1)}, bf16[512,128]{1,0:T(8,128)(2,1)S(1)}, u32[]{:S(2)}, u32[]{:S(2)}) collective-permute-start(bf16[512,128]{1,0:T(8,128)(2,1)S(1)} %copy-done.8), channel_id=1, source_target_pairs={{0,24},{8,0},{16,8},{24,16},{1,25},{9,1},{17,9},{25,17},{2,26},{10... | collective-permute-start | bytes 393224 | tf_op jit(solution)/shard_map/ppermute | solution.py:37
  45.4 34.5 %copy-start.6 = (bf16[128,2048]{1,0:T(8,128)(2,1)S(1)}, bf16[128,2048]{1,0:T(8,128)(2,1)}, u32[]{:S(2)}) copy-start(bf16[128,2048]{1,0:T(8,128)(2,1)} %param.24) | copy-start | bytes 1572868
  45.4 34.5 %copy-start.10 = (f32[128]{0:T(128)S(1)}, f32[128]{0:T(128)}, u32[]{:S(2)}) copy-start(f32[128]{0:T(128)} %param.23) | copy-start | bytes 1540
  59.8 11.3 %all-to-all-start.2 = ((bf16[8,16,512]{2,1,0:T(8,128)(2,1)}), bf16[8,16,512]{2,1,0:T(8,128)(2,1)S(1)}, u32[]{:S(2)}, u32[]{:S(2)}) async-start(bf16[8,16,512]{2,1,0:T(8,128)(2,1)} %broadcast_in_dim.12), calls=%async_computation.2 | async-start | bytes 262144 | tf_op jit(solution)/shard_map/all_to_all | solution.py:23
  71.9 13.3 %all-to-all-start.3 = ((bf16[8,16,512]{2,1,0:T(8,128)(2,1)}), bf16[8,16,512]{2,1,0:T(8,128)(2,1)S(1)}, u32[]{:S(2)}, u32[]{:S(2)}) async-start(bf16[8,16,512]{2,1,0:T(8,128)(2,1)} %bitcast.12), calls=%async_computation.3 | async-start | bytes 262144 | tf_op jit(solution)/shard_map/all_to_all | solution.py:23
  85.2 21.4 %all-to-all-start.5 = ((bf16[8,256,128]{2,1,0:T(8,128)(2,1)}), bf16[8,256,128]{2,1,0:T(8,128)(2,1)S(1)}, u32[]{:S(2)}, u32[]{:S(2)}) async-start(bf16[8,256,128]{2,1,0:T(8,128)(2,1)} %bitcast.15), calls=%async_computation.5 | async-start | bytes 1048576 | tf_op jit(solution)/shard_map/all_to_all | solution.py:23
  88.8 82.9 %copy-start.7 = (bf16[16,512]{1,0:T(8,128)(2,1)}, bf16[16,512]{1,0:T(8,128)(2,1)S(1)}, u32[]{:S(2)}) copy-start(bf16[16,512]{1,0:T(8,128)(2,1)S(1)} %fusion.3.resid_ref) | copy-start | bytes 49156
  106.6 38.5 %copy-start = (bf16[8,256,128]{2,1,0:T(8,128)(2,1)}, bf16[8,256,128]{2,1,0:T(8,128)(2,1)S(1)}, u32[]{:S(2)}) copy-start(bf16[8,256,128]{2,1,0:T(8,128)(2,1)S(1)} %all-to-all-done.5.w0_ref) | copy-start | bytes 1572868
  107.6 17.9 %all-to-all-start.4 = ((bf16[32,16,512]{2,1,0:T(8,128)(2,1)}), bf16[32,16,512]{2,1,0:T(8,128)(2,1)S(1)}, u32[]{:S(2)}, u32[]{:S(2)}) async-start(bf16[32,16,512]{2,1,0:T(8,128)(2,1)} %broadcast_in_dim.13), calls=%async_computation.4 | async-start | bytes 1048576 | tf_op jit(solution)/shard_map/all_to_all | solution.py:23
  111.5 17.7 %collective-permute-start.12 = (bf16[2048,128]{1,0:T(8,128)(2,1)}, bf16[2048,128]{1,0:T(8,128)(2,1)S(1)}, u32[]{:S(2)}, u32[]{:S(2)}) collective-permute-start(bf16[2048,128]{1,0:T(8,128)(2,1)} %w0_ref.1), channel_id=1, source_target_pairs={{0,8},{8,16},{16,24},{24,0},{1,9},{9,17},{17,25},{25,1},{2,10},{10... | collective-permute-start | bytes 1572872 | tf_op jit(solution)/shard_map/ppermute | solution.py:37
  111.6 25.6 %collective-permute-start.9 = (bf16[8,256,128]{2,1,0:T(8,128)(2,1)S(1)}, bf16[8,256,128]{2,1,0:T(8,128)(2,1)S(1)}, u32[]{:S(2)}, u32[]{:S(2)}) collective-permute-start(bf16[8,256,128]{2,1,0:T(8,128)(2,1)S(1)} %all-to-all-done.5.w0_ref), channel_id=1, source_target_pairs={{0,8},{8,16},{16,24},{24,0},{1,9},{9,17},{17,25},{25,1},{2,10},{10... | collective-permute-start | bytes 1572872 | tf_op jit(solution)/shard_map/ppermute | solution.py:37
  111.6 25.7 %collective-permute-start.8 = (bf16[8,256,128]{2,1,0:T(8,128)(2,1)S(1)}, bf16[8,256,128]{2,1,0:T(8,128)(2,1)S(1)}, u32[]{:S(2)}, u32[]{:S(2)}) collective-permute-start(bf16[8,256,128]{2,1,0:T(8,128)(2,1)S(1)} %all-to-all-done.5.w0_ref), channel_id=1, source_target_pairs={{0,24},{8,0},{16,8},{24,16},{1,25},{9,1},{17,9},{25,17},{2,26},{10... | collective-permute-start | bytes 1572872 | tf_op jit(solution)/shard_map/ppermute | solution.py:37
  114.3 25.8 %collective-permute-start.14 = (bf16[2048,128]{1,0:T(8,128)(2,1)}, bf16[2048,128]{1,0:T(8,128)(2,1)S(1)}, u32[]{:S(2)}, u32[]{:S(2)}) collective-permute-start(bf16[2048,128]{1,0:T(8,128)(2,1)} %w0_ref.1), channel_id=1, source_target_pairs={{0,24},{8,0},{16,8},{24,16},{1,25},{9,1},{17,9},{25,17},{2,26},{10... | collective-permute-start | bytes 1572872 | tf_op jit(solution)/shard_map/ppermute | solution.py:37
  125.5 19.6 %collective-permute-start.7 = (bf16[4,8,16,512]{3,2,1,0:T(8,128)(2,1)S(1)}, bf16[4,8,16,512]{3,2,1,0:T(8,128)(2,1)}, u32[]{:S(2)}, u32[]{:S(2)}) collective-permute-start(bf16[4,8,16,512]{3,2,1,0:T(8,128)(2,1)S(1)} %bitcast.56), channel_id=1, source_target_pairs={{0,1},{1,0},{2,3},{3,2},{4,5},{5,4},{6,7},{7,6},{8,9},{9,8},{10,11... | collective-permute-start | bytes 1572872 | tf_op jit(solution)/shard_map/ppermute | solution.py:41
  129.2 42.5 %copy-start.4 = (bf16[2048,128]{1,0:T(8,128)(2,1)}, bf16[2048,128]{1,0:T(8,128)(2,1)S(1)}, u32[]{:S(2)}) copy-start(bf16[2048,128]{1,0:T(8,128)(2,1)S(1)} %collective-permute-done.12.w3_ref) | copy-start | bytes 1572868
  137.2 7.9 %collective-permute-start.10 = (bf16[4,256,128]{2,1,0:T(8,128)(2,1)S(1)}, bf16[4,256,128]{2,1,0:T(8,128)(2,1)}, u32[]{:S(2)}, u32[]{:S(2)}) collective-permute-start(bf16[4,256,128]{2,1,0:T(8,128)(2,1)S(1)} %slice.97), channel_id=1, source_target_pairs={{0,8},{8,16},{16,24},{24,0},{1,9},{9,17},{17,25},{25,1},{2,10},{10... | collective-permute-start | bytes 786440 | tf_op jit(solution)/shard_map/ppermute | solution.py:37
  137.4 7.8 %collective-permute-start.11 = (bf16[4,256,128]{2,1,0:T(8,128)(2,1)S(1)}, bf16[4,256,128]{2,1,0:T(8,128)(2,1)}, u32[]{:S(2)}, u32[]{:S(2)}) collective-permute-start(bf16[4,256,128]{2,1,0:T(8,128)(2,1)S(1)} %slice.98), channel_id=1, source_target_pairs={{0,24},{8,0},{16,8},{24,16},{1,25},{9,1},{17,9},{25,17},{2,26},{10... | collective-permute-start | bytes 786440 | tf_op jit(solution)/shard_map/ppermute | solution.py:37
  140.1 10.7 %collective-permute-start.13 = (bf16[1024,128]{1,0:T(8,128)(2,1)}, bf16[1024,128]{1,0:T(8,128)(2,1)}, u32[]{:S(2)}, u32[]{:S(2)}) collective-permute-start(bf16[1024,128]{1,0:T(8,128)(2,1)} %slice.99), channel_id=1, source_target_pairs={{0,8},{8,16},{16,24},{24,0},{1,9},{9,17},{17,25},{25,1},{2,10},{10... | collective-permute-start | bytes 786440 | tf_op jit(solution)/shard_map/ppermute | solution.py:37
  140.1 31.6 %copy-start.5 = (bf16[2048,128]{1,0:T(8,128)(2,1)}, bf16[2048,128]{1,0:T(8,128)(2,1)S(1)}, u32[]{:S(2)}) copy-start(bf16[2048,128]{1,0:T(8,128)(2,1)S(1)} %collective-permute-done.14.w1_ref) | copy-start | bytes 1572868
  140.9 9.9 %collective-permute-start.15 = (bf16[1024,128]{1,0:T(8,128)(2,1)}, bf16[1024,128]{1,0:T(8,128)(2,1)}, u32[]{:S(2)}, u32[]{:S(2)}) collective-permute-start(bf16[1024,128]{1,0:T(8,128)(2,1)} %slice.100), channel_id=1, source_target_pairs={{0,24},{8,0},{16,8},{24,16},{1,25},{9,1},{17,9},{25,17},{2,26},{10... | collective-permute-start | bytes 786440 | tf_op jit(solution)/shard_map/ppermute | solution.py:37
  175.1 18.8 %all-to-all-start.7 = ((bf16[32,16,128]{2,1,0:T(8,128)(2,1)}), bf16[32,16,128]{2,1,0:T(8,128)(2,1)S(1)}, u32[]{:S(2)}, u32[]{:S(2)}) async-start(bf16[32,16,128]{2,1,0:T(8,128)(2,1)} %bitcast.62), calls=%async_computation.7 | async-start | bytes 262144 | tf_op jit(solution)/shard_map/all_to_all | solution.py:23
  (3 other events, 35.5 us)
